TPU v7x, 512 devices: a whole 4x8x8 slice. The times are simulated.
512 devices in a mesh: sp: 32 (over z, x), tp: 16 (over y, core).
Axes of the slice: x: 4, y: 8, z: 8, core: 2. Of those that a mesh axis runs over, the one named last changes fastest.
Arguments:
- target: bfloat16 [4096, 4096], P('sp', 'tp'), may hold values from -300 to 300
- gain: float32 [4096], P('tp'), may hold values from 0.1 to 1.9
- w_query: bfloat16 [4096, 4096], P('tp'), may hold values from -0.09375 to 0.09375
- queries: bfloat16 [4096, 4096], P('sp', 'tp'), may hold values from -13 to 13
- keys: bfloat16 [16384, 1024], P('sp'), may hold values from -4 to 4
- values: bfloat16 [16384, 1024], P('sp'), may hold values from -4 to 4
- attn_out: bfloat16 [4096, 4096], P('sp', 'tp'), may hold values from -4 to 4
- grad_out: bfloat16 [4096, 4096], P('sp', 'tp'), may hold values from -64 to 64
Outputs:
- grad_rows: bfloat16 [4096, 4096], P('sp', 'tp')
- grad_weight: float32 [4096, 4096], P(('tp', 'sp'))
- grad_keys: float32 [16384, 1024], P(('sp', 'tp'))
- grad_values: float32 [16384, 1024], P(('sp', 'tp'))
All inputs are finite; a program needn't handle non-finite values.
Results may differ from a plain program's by a relative error of at most 0.018.
Values may be sent and summed in bfloat16 or wider, within the bound.
No kernel may reach another device: no remote copies, remote signals or barrier semaphores. Data moves between devices by JAX's collectives and lax.ppermute only.
A program may use at most 64 MiB of HBM per device.

v0:
```python
import jax
import jax.numpy as jnp
from jax import lax
from jax.experimental.layout import Layout, with_layout_constraint
from jax.sharding import Mesh
from jax.sharding import PartitionSpec as P

WIDTH = 4096
HEADS = 16
KV_HEADS = 4
HEAD_DIM = 256
EPS = 1e-06
SCALE = HEAD_DIM ** (-0.5)
F32 = jnp.float32
BF16 = jnp.bfloat16


def shifted(value, axis, by):
    n = lax.axis_size(axis)
    return lax.ppermute(value, axis, [(i, (i + by) % n) for i in range(n)])


def exchanged(value, axis):
    return lax.all_to_all(value, axis, split_axis=0, concat_axis=0, tiled=True)


def told_all(value, axis):
    n = lax.axis_size(axis)
    return exchanged(jnp.broadcast_to(value[None], (n, *value.shape)), axis)


def dot(a, b, ca, cb):
    return lax.dot_general(a, b, (((ca,), (cb,)), ((), ())), preferred_element_type=F32)


def row_major(value):
    return with_layout_constraint(value, Layout(major_to_minor=tuple(range(value.ndim))))


def terms(value):
    high = lax.reduce_precision(value, 8, 7)
    rest = value - high
    mid = lax.reduce_precision(rest, 8, 7)
    return [t.astype(BF16) for t in (high, mid, rest - mid)]


def local(target, gain, w_query, queries, keys, values, attn_out, grad_out):
    nz, nx, ny = lax.axis_size("z"), lax.axis_size("x"), lax.axis_size("y")
    rows, cols = queries.shape
    part = cols // nx
    src = keys.shape[0]
    bit = src // (2 * ny)
    core = lax.axis_index("c")
    x_at = lax.axis_index("x")
    kv = lax.axis_index("y") // 2
    n_rows = nz * rows

    delta_own = jnp.sum(attn_out.astype(F32) * grad_out.astype(F32), axis=1)
    line = jnp.concatenate(terms(delta_own) + [jnp.zeros((rows,), BF16)])[None]
    both = jnp.concatenate([queries, grad_out], axis=1)
    both = jnp.concatenate([both, line, jnp.zeros((7, 2 * cols), BF16)], axis=0)
    both = told_all(both, "z")

    def half_of(v):
        v = v.reshape(ny, 2, bit, v.shape[1])
        v = lax.dynamic_slice(v, (0, core, 0, kv * HEAD_DIM), (ny, 1, bit, HEAD_DIM))
        return v.reshape(src // 2, HEAD_DIM)

    pack = row_major(jnp.concatenate([half_of(keys), half_of(values), target], axis=0))
    blocks = [pack] + [shifted(pack, "x", by) for by in (1, -1, 2)]
    target_all = jnp.zeros((nx * rows, cols), BF16)
    for block, off in zip(blocks, (0, 3, 1, 2)):
        target_all = lax.dynamic_update_slice(target_all, block[src:], (lax.rem(x_at + off, nx) * rows, 0))

    w_parts = lax.dynamic_slice(
        w_query.reshape(cols, HEADS // 2, 2, nx, part), (0, 0, 0, x_at, 0), (cols, HEADS // 2, 2, 1, part)
    )
    w_even = w_parts[:, :, 0].reshape(cols, -1)
    w_odd = w_parts[:, :, 1].reshape(cols, -1)
    w_mine = jnp.where(core == 0, w_even, w_odd)
    w_theirs = jnp.where(core == 0, w_odd, w_even)
    swap = [b[:src] for b in blocks] + [target_all, w_theirs[:, :cols], w_theirs[:, cols:]]
    swap = shifted(row_major(jnp.concatenate(swap, axis=0)), "c", 1)
    blocks = [b[:src] for b in blocks] + [swap[src * k : src * (k + 1)] for k in range(nx)]
    key_all = row_major(jnp.concatenate([b[: src // 2] for b in blocks], axis=0))
    value_all = row_major(jnp.concatenate([b[src // 2 :] for b in blocks], axis=0))
    target_other = swap[nx * src : nx * src + nx * rows]
    w_other = swap[nx * src + nx * rows :]
    w_other = jnp.concatenate([w_other[:cols], w_other[cols:]], axis=1)

    both = both.reshape(nz, rows + 8, 2 * cols)
    query_all = both[:, :rows, :cols].reshape(n_rows, cols)
    grad_all = both[:, :rows, cols:].reshape(n_rows, cols)
    deltas = both[:, rows].astype(F32).reshape(nz, 4, rows).sum(axis=1).reshape(n_rows)
    scores = dot(key_all, query_all, 1, 1) * SCALE
    peak = jnp.max(scores, axis=0)
    weights = jnp.exp(scores - peak[None])
    total = jnp.sum(weights, axis=0)
    stats = told_all(jnp.concatenate([peak, total]).reshape(2 * nz, rows), "z").reshape(nz, 2, n_rows)
    grad_weights = dot(value_all, grad_all, 1, 1)
    grad_scores = (weights * ((grad_weights - deltas[None]) * SCALE)).astype(BF16)
    query_t = dot(key_all, grad_scores, 0, 0)
    query_t, stats = lax.optimization_barrier((query_t, stats))
    top = jnp.max(stats[:, 0], axis=0)
    log_totals = top + jnp.log(jnp.sum(stats[:, 1] * jnp.exp(stats[:, 0] - top[None]), axis=0))
    share = jnp.exp(peak - log_totals)

    sent = (query_t * share[None]).astype(BF16).reshape(nx, part, nz, rows).transpose(2, 0, 1, 3)
    sent = sent.reshape(nz * nx, part, rows)
    got = exchanged(sent, ("z", "x")).reshape(nz, nx, part, rows)
    part_t = got.astype(F32).sum(axis=0)
    part_t = part_t.transpose(1, 0, 2).reshape(part, nx * rows).astype(BF16)

    query_share, grad_share, _ = lax.optimization_barrier(
        ((query_all * share[:, None]).astype(BF16), (grad_all * share[:, None]).astype(BF16), sent)
    )
    key_sum = dot(grad_scores, query_share, 1, 0)
    value_sum = dot(weights.astype(BF16), grad_share, 1, 0)
    half = nx * src // 2
    theirs = jnp.concatenate([key_sum[half:], value_sum[half:]], axis=1).astype(BF16)
    mine = jnp.concatenate([key_sum[:half], value_sum[:half]], axis=1)
    mine = row_major((mine + shifted(row_major(theirs), "c", 1).astype(F32)).astype(BF16))
    own, left, right, far = (mine[src // 2 * k : src // 2 * (k + 1)] for k in range(nx))
    own = own.astype(F32)
    for block, by in ((far, 2), (right, 1), (left, -1)):
        own = own + shifted(block, "x", by).astype(F32)
    mine = own.astype(BF16)

    def by_core(mine, theirs):
        return jnp.where(core == 0, jnp.stack([mine, theirs]), jnp.stack([theirs, mine]))

    target_both = by_core(target_all.T, target_other.T).astype(F32)
    w_both = by_core(w_mine, w_other).reshape(2 * cols, -1)
    squares = jnp.sum(target_both * target_both, axis=(0, 1))
    high = lax.reduce_precision(squares, 8, 7)
    extra = jnp.stack([high, squares - high]).astype(BF16)
    piece = jnp.concatenate([part_t, extra, jnp.zeros((6, nx * rows), BF16)], axis=0)
    every = told_all(piece, "y").reshape(HEADS // 2, part + 8, nx * rows)
    every, mine = lax.optimization_barrier((every, mine))
    grad_t = every[:, :part].reshape(HEADS // 2 * part, nx * rows)
    squares_all = every[:, part : part + 2].astype(F32).sum(axis=(0, 1))
    inverse = lax.rsqrt(squares_all / WIDTH + EPS)
    normed_t = (target_both * inverse[None, None]).astype(BF16)
    weight_part = dot(normed_t.reshape(2 * cols, -1), grad_t, 1, 1).astype(BF16)

    weight_sent = weight_part.reshape(2, nz * nx, 8, -1).transpose(1, 0, 2, 3).reshape(nz * nx * 2, 8, -1)
    weight_got = exchanged(weight_sent, ("z", "x", "c"))
    weight_sum = weight_got.reshape(nz, nx * 2, 8, HEADS // 2 * part).astype(F32).sum(axis=0)
    gain_at = (lax.axis_index("z") * nx + x_at) * 8
    weight_sum = weight_sum * lax.dynamic_slice_in_dim(gain, gain_at, 8, 0)[None, :, None]
    weight_sum = lax.optimization_barrier(weight_sum).reshape(nx, 2, 8, HEADS // 2, part)
    grad_weight = weight_sum.transpose(2, 3, 1, 0, 4).reshape(8, WIDTH)

    grad_t, _ = lax.optimization_barrier((grad_t, weight_sent))
    rows_t = dot(w_both, grad_t, 1, 0)

    def rows_at(off):
        return lax.dynamic_slice_in_dim(rows_t, lax.rem(x_at + off, nx) * rows, rows, 1)

    rows_sum = rows_at(0)
    for off, by in ((1, 1), (3, -1), (2, 2)):
        rows_sum = rows_sum + shifted(rows_at(off).astype(BF16), "x", by).astype(F32)
    low, high = rows_sum[:cols], rows_sum[cols:]
    rows_in = shifted(jnp.where(core == 0, high, low).astype(BF16), "c", 1)
    grad_rows = (jnp.where(core == 0, low, high) + rows_in.astype(F32)).T.astype(BF16)

    mine, _ = lax.optimization_barrier((mine, weight_got))
    sums = exchanged(mine.reshape(ny, bit, 2 * HEAD_DIM), "y")
    sums = sums.reshape(KV_HEADS, 2, bit, 2, HEAD_DIM).astype(F32).sum(axis=1)
    sums = sums.transpose(2, 1, 0, 3).reshape(2, bit, KV_HEADS * HEAD_DIM)
    return (grad_rows, grad_weight, sums[0], sums[1])


def solution(mesh):
    finer = Mesh(mesh.devices.reshape(8, 4, 8, 2), ("z", "x", "y", "c"))
    sp, tp = ("z", "x"), ("y", "c")
    placed = (
        P(sp, tp),
        P(tp),
        P(tp, None),
        P(sp, tp),
        P(sp, None),
        P(sp, None),
        P(sp, tp),
        P(sp, tp),
    )

    return jax.shard_map(
        local,
        mesh=finer,
        in_specs=placed,
        out_specs=(P(sp, tp), P(tp + sp, None), P(sp + tp, None), P(sp + tp, None)),
        check_vma=False,
    )
```

profile of v0, /device:TPU:3, one launch (start us, length us, event | category | flops | bytes accessed | tf_op | source)
XLA Modules:
  0.0 200.6 jit_solution(13693992492375325349)
XLA Ops:
  0.6 1.0 constant_dynamic-slice_fusion
  1.7 1.6 pad_maximum_fusion.1
  3.3 3.1 %collective-permute-start = (bf16[640,256]{1,0:T(8,128)(2,1)}, bf16[640,256]{1,0:T(8,128)(2,1)S(1)}, u32[]{:S(2)}, u32[]{:S(2)}) collective-permute-start(bf16[640,256]{1,0:T(8,128)(2,1)} %pad_maximum_fusion.1), channel_id=1, source_target_pairs={{0,16},{16,32},{32,48},{48,0},{1,17},{17,33},{33,49},{49,1},{2,18}... | collective-permute-start | bytes 983048 | tf_op jit(solution)/shard_map/ppermute | solution.py:20
  6.4 2.6 %collective-permute-start.2 = (bf16[640,256]{1,0:T(8,128)(2,1)}, bf16[640,256]{1,0:T(8,128)(2,1)S(1)}, u32[]{:S(2)}, u32[]{:S(2)}) collective-permute-start(bf16[640,256]{1,0:T(8,128)(2,1)} %pad_maximum_fusion.1), channel_id=1, source_target_pairs={{0,32},{16,48},{32,0},{48,16},{1,33},{17,49},{33,1},{49,17},{2,34}... | collective-permute-start | bytes 983048 | tf_op jit(solution)/shard_map/ppermute | solution.py:20
  8.9 4.0 %collective-permute-start.1 = (bf16[640,256]{1,0:T(8,128)(2,1)}, bf16[640,256]{1,0:T(8,128)(2,1)S(1)}, u32[]{:S(2)}, u32[]{:S(2)}) collective-permute-start(bf16[640,256]{1,0:T(8,128)(2,1)} %pad_maximum_fusion.1), channel_id=1, source_target_pairs={{0,48},{16,0},{32,16},{48,32},{1,49},{17,1},{33,17},{49,33},{2,50}... | collective-permute-start | bytes 983048 | tf_op jit(solution)/shard_map/ppermute | solution.py:20
  12.9 3.3 %copy.188 = bf16[256,4096]{0,1:T(8,128)(2,1)S(1)} copy(bf16[256,4096]{1,0:T(8,128)(2,1)} %param.10) | data formatting | bytes 4194304 | tf_op args[2]
  18.9 5.1 %collective-permute-done.1 = bf16[640,256]{1,0:T(8,128)(2,1)S(1)} collective-permute-done((bf16[640,256]{1,0:T(8,128)(2,1)}, bf16[640,256]{1,0:T(8,128)(2,1)S(1)}, u32[]{:S(2)}, u32[]{:S(2)}) %collective-permute-start.1) | collective-permute-done | bytes 327712 | tf_op jit(solution)/shard_map/ppermute | solution.py:20
  27.5 5.1 %collective-permute-start.3 = (bf16[3072,256]{1,0:T(8,128)(2,1)}, bf16[3072,256]{1,0:T(8,128)(2,1)}, u32[]{:S(2)}, u32[]{:S(2)}) collective-permute-start(bf16[3072,256]{1,0:T(8,128)(2,1)} %constant_dynamic-update-slice_fusion), channel_id=1, source_target_pairs={{0,1},{1,0},{2,3},{3,2},{4,5},{5,4},{6,7},{7,6},{8,9},{9,8},{10,11... | collective-permute-start | bytes 4718600 | tf_op jit(solution)/shard_map/ppermute | solution.py:20
  33.0 1.1 broadcast_in_dim.20
  34.1 10.0 %all-to-all-start = ((bf16[8,136,512]{2,1,0:T(8,128)(2,1)}), bf16[8,136,512]{2,1,0:T(8,128)(2,1)S(1)}, u32[]{:S(2)}, u32[]{:S(2)}) async-start(bf16[8,136,512]{2,1,0:T(8,128)(2,1)} %broadcast_in_dim.20), calls=%async_computation | async-start | bytes 2228224 | tf_op jit(solution)/shard_map/all_to_all | solution.py:24
  44.8 1.6 slice_dynamic-update-slice_fusion.9
  46.4 1.6 slice_dynamic-update-slice_fusion.8
  48.7 1.6 slice_dynamic-update-slice_fusion.6
  50.3 1.6 slice_dynamic-update-slice_fusion.5
  52.0 1.6 slice_dynamic-update-slice_fusion.4
  53.6 1.8 slice_dynamic-update-slice_fusion.3
  55.4 19.3 %all-to-all-done = bf16[8,136,512]{2,1,0:T(8,128)(2,1)S(1)} async-done(((bf16[8,136,512]{2,1,0:T(8,128)(2,1)}), bf16[8,136,512]{2,1,0:T(8,128)(2,1)S(1)}, u32[]{:S(2)}, u32[]{:S(2)}) %all-to-all-start) | async-done | bytes 1114144 | tf_op jit(solution)/shard_map/all_to_all | solution.py:24
  74.9 1.3 multiply_reduce_fusion
  76.2 1.4 fusion.1
  77.6 1.8 copy-done
  80.1 3.4 %all-to-all-start.1 = ((f32[8,16,128]{2,1,0:T(8,128)}), f32[8,16,128]{2,1,0:T(8,128)S(1)}, u32[]{:S(2)}, u32[]{:S(2)}) async-start(f32[8,16,128]{2,1,0:T(8,128)} %broadcast_in_dim.21), calls=%async_computation.1 | async-start | bytes 131072 | tf_op jit(solution)/shard_map/all_to_all | solution.py:24
  83.5 5.0 %multiply_convert_fusion = bf16[2048,1024]{1,0:T(8,128)(2,1)S(1)} fusion(f32[2048,1024]{1,0:T(8,128)} %copy-done, bf16[2048,256]{1,0:T(8,128)(2,1)} %get-tuple-element.62, bf16[1024,256]{1,0:T(8,128)(2,1)S(1)} %bitcast.108, f32[1024]{0:T(1024)S(1)} %bitcast.122, f32[1024]{0:T(1024)S(1)} %get-tuple-element.97), kind=kOutput, calls=%fused_computation | convolution fusion | flops 1086324736 | bytes 14163968 | tf_op jit(solution)/shard_map/dot_general | solution.py:33
  88.5 2.0 copy-done.12
  90.4 1.3 fusion.20
  93.4 8.5 %all-to-all-start.2 = ((bf16[32,64,128]{2,1,0:T(8,128)(2,1)}), bf16[32,64,128]{2,1,0:T(8,128)(2,1)S(1)}, u32[]{:S(2)}, u32[]{:S(2)}) async-start(bf16[32,64,128]{2,1,0:T(8,128)(2,1)} %bitcast.17), calls=%async_computation.2 | async-start | bytes 1048576 | tf_op jit(solution)/shard_map/all_to_all | solution.py:24
  102.0 5.1 %fusion.2 = f32[2048,256]{1,0:T(8,128)S(1)} fusion(bf16[1024,256]{1,0:T(8,128)(2,1)S(1)} %get-tuple-element.15, f32[2048,1024]{1,0:T(8,128)} %copy-done, f32[1024]{0:T(1024)S(1)} %get-tuple-element.97), kind=kOutput, calls=%fused_computation.5 | convolution fusion | flops 1080033280 | bytes 11014144 | tf_op jit(solution)/shard_map/dot_general | solution.py:33
  107.1 1.3 fusion.21
  108.5 1.2 pad_maximum_fusion
  109.7 3.2 %collective-permute-start.4 = (bf16[1024,512]{1,0:T(8,128)(2,1)}, bf16[1024,512]{1,0:T(8,128)(2,1)}, u32[]{:S(2)}, u32[]{:S(2)}) collective-permute-start(bf16[1024,512]{1,0:T(8,128)(2,1)} %pad_maximum_fusion), channel_id=1, source_target_pairs={{0,1},{1,0},{2,3},{3,2},{4,5},{5,4},{6,7},{7,6},{8,9},{9,8},{10,11... | collective-permute-start | bytes 3145736 | tf_op jit(solution)/shard_map/ppermute | solution.py:20
  113.0 1.0 slice_bitcast_fusion
  114.3 1.0 slice.263
  115.3 2.7 %all-to-all-done.2 = bf16[32,64,128]{2,1,0:T(8,128)(2,1)S(1)} async-done(((bf16[32,64,128]{2,1,0:T(8,128)(2,1)}), bf16[32,64,128]{2,1,0:T(8,128)(2,1)S(1)}, u32[]{:S(2)}, u32[]{:S(2)}) %all-to-all-start.2) | async-done | bytes 524320 | tf_op jit(solution)/shard_map/all_to_all | solution.py:24
  119.1 6.8 %all-to-all-start.3 = ((bf16[8,72,512]{2,1,0:T(8,128)(2,1)}), bf16[8,72,512]{2,1,0:T(8,128)(2,1)S(1)}, u32[]{:S(2)}, u32[]{:S(2)}) async-start(bf16[8,72,512]{2,1,0:T(8,128)(2,1)} %broadcast_in_dim.46), calls=%async_computation.3 | async-start | bytes 1179648 | tf_op jit(solution)/shard_map/all_to_all | solution.py:24
  126.0 1.9 fusion.6
  128.8 3.4 %collective-permute-start.5 = (bf16[256,512]{1,0:T(8,128)(2,1)}, bf16[256,512]{1,0:T(8,128)(2,1)}, u32[]{:S(2)}, u32[]{:S(2)}) collective-permute-start(bf16[256,512]{1,0:T(8,128)(2,1)} %get-tuple-element.77), channel_id=1, source_target_pairs={{0,32},{16,48},{32,0},{48,16},{1,33},{17,49},{33,1},{49,17},{2,34}... | collective-permute-start | bytes 786440 | tf_op jit(solution)/shard_map/ppermute | solution.py:20
  132.2 1.9 collective-permute-start.6
  134.2 3.4 %collective-permute-start.7 = (bf16[256,512]{1,0:T(8,128)(2,1)}, bf16[256,512]{1,0:T(8,128)(2,1)}, u32[]{:S(2)}, u32[]{:S(2)}) collective-permute-start(bf16[256,512]{1,0:T(8,128)(2,1)} %get-tuple-element.79), channel_id=1, source_target_pairs={{0,48},{16,0},{32,16},{48,32},{1,49},{17,1},{33,17},{49,33},{2,50}... | collective-permute-start | bytes 786440 | tf_op jit(solution)/shard_map/ppermute | solution.py:20
  138.1 6.4 %collective-permute-done.6 = bf16[256,512]{1,0:T(8,128)(2,1)} collective-permute-done((bf16[256,512]{1,0:T(8,128)(2,1)}, bf16[256,512]{1,0:T(8,128)(2,1)}, u32[]{:S(2)}, u32[]{:S(2)}) %collective-permute-start.6) | collective-permute-done | bytes 262176 | tf_op jit(solution)/shard_map/ppermute | solution.py:20
  144.6 2.0 add_convert_fusion
  148.6 9.9 %all-to-all-start.4 = ((bf16[64,8,512]{2,1,0:T(8,128)(2,1)}), bf16[64,8,512]{2,1,0:T(8,128)(2,1)S(1)}, u32[]{:S(2)}, u32[]{:S(2)}) async-start(bf16[64,8,512]{2,1,0:T(8,128)(2,1)} %bitcast.32), calls=%async_computation.4 | async-start | bytes 1048576 | tf_op jit(solution)/shard_map/all_to_all | solution.py:24
  159.0 3.1 %collective-permute-start.8 = (bf16[512,128]{1,0:T(8,128)(2,1)S(1)}, bf16[512,128]{1,0:T(8,128)(2,1)S(1)}, u32[]{:S(2)}, u32[]{:S(2)}) collective-permute-start(bf16[512,128]{1,0:T(8,128)(2,1)S(1)} %get-tuple-element.74), channel_id=1, source_target_pairs={{0,16},{16,32},{32,48},{48,0},{1,17},{17,33},{33,49},{49,1},{2,18}... | collective-permute-start | bytes 393224 | tf_op jit(solution)/shard_map/ppermute | solution.py:20
  162.1 2.6 %collective-permute-start.10 = (bf16[512,128]{1,0:T(8,128)(2,1)S(1)}, bf16[512,128]{1,0:T(8,128)(2,1)S(1)}, u32[]{:S(2)}, u32[]{:S(2)}) collective-permute-start(bf16[512,128]{1,0:T(8,128)(2,1)S(1)} %get-tuple-element.75), channel_id=1, source_target_pairs={{0,32},{16,48},{32,0},{48,16},{1,33},{17,49},{33,1},{49,17},{2,34}... | collective-permute-start | bytes 393224 | tf_op jit(solution)/shard_map/ppermute | solution.py:20
  164.8 3.9 %collective-permute-start.9 = (bf16[512,128]{1,0:T(8,128)(2,1)S(1)}, bf16[512,128]{1,0:T(8,128)(2,1)S(1)}, u32[]{:S(2)}, u32[]{:S(2)}) collective-permute-start(bf16[512,128]{1,0:T(8,128)(2,1)S(1)} %get-tuple-element.76), channel_id=1, source_target_pairs={{0,48},{16,0},{32,16},{48,32},{1,49},{17,1},{33,17},{49,33},{2,50}... | collective-permute-start | bytes 393224 | tf_op jit(solution)/shard_map/ppermute | solution.py:20
  168.7 3.5 %collective-permute-done.10 = bf16[512,128]{1,0:T(8,128)(2,1)S(1)} collective-permute-done((bf16[512,128]{1,0:T(8,128)(2,1)S(1)}, bf16[512,128]{1,0:T(8,128)(2,1)S(1)}, u32[]{:S(2)}, u32[]{:S(2)}) %collective-permute-start.10) | collective-permute-done | bytes 131104 | tf_op jit(solution)/shard_map/ppermute | solution.py:20
  172.2 4.3 %collective-permute-done.9 = bf16[512,128]{1,0:T(8,128)(2,1)S(1)} collective-permute-done((bf16[512,128]{1,0:T(8,128)(2,1)S(1)}, bf16[512,128]{1,0:T(8,128)(2,1)S(1)}, u32[]{:S(2)}, u32[]{:S(2)}) %collective-permute-start.9) | collective-permute-done | bytes 131104 | tf_op jit(solution)/shard_map/ppermute | solution.py:20
  176.6 2.4 %collective-permute-start.11 = (bf16[256,128]{1,0:T(8,128)(2,1)S(1)}, bf16[256,128]{1,0:T(8,128)(2,1)S(1)}, u32[]{:S(2)}, u32[]{:S(2)}) collective-permute-start(bf16[256,128]{1,0:T(8,128)(2,1)S(1)} %select_convert_fusion), channel_id=1, source_target_pairs={{0,1},{1,0},{2,3},{3,2},{4,5},{5,4},{6,7},{7,6},{8,9},{9,8},{10,11... | collective-permute-start | bytes 196616 | tf_op jit(solution)/shard_map/ppermute | solution.py:20
  179.1 6.6 %all-to-all-start.5 = ((bf16[8,32,512]{2,1,0:T(8,128)(2,1)}), bf16[8,32,512]{2,1,0:T(8,128)(2,1)S(1)}, u32[]{:S(2)}, u32[]{:S(2)}) async-start(bf16[8,32,512]{2,1,0:T(8,128)(2,1)} %bitcast.37), calls=%async_computation.5 | async-start | bytes 524288 | tf_op jit(solution)/shard_map/all_to_all | solution.py:24
  187.8 10.2 %all-to-all-done.5 = bf16[8,32,512]{2,1,0:T(8,128)(2,1)S(1)} async-done(((bf16[8,32,512]{2,1,0:T(8,128)(2,1)}), bf16[8,32,512]{2,1,0:T(8,128)(2,1)S(1)}, u32[]{:S(2)}, u32[]{:S(2)}) %all-to-all-start.5) | async-done | bytes 262176 | tf_op jit(solution)/shard_map/all_to_all | solution.py:24
  (124 shorter events, 20.3 us)
Async XLA Ops:
  3.3 14.8 %collective-permute-start = (bf16[640,256]{1,0:T(8,128)(2,1)}, bf16[640,256]{1,0:T(8,128)(2,1)S(1)}, u32[]{:S(2)}, u32[]{:S(2)}) collective-permute-start(bf16[640,256]{1,0:T(8,128)(2,1)} %pad_maximum_fusion.1), channel_id=1, source_target_pairs={{0,16},{16,32},{32,48},{48,0},{1,17},{17,33},{33,49},{49,1},{2,18}... | collective-permute-start | bytes 983048 | tf_op jit(solution)/shard_map/ppermute | solution.py:20
  6.4 18.3 %collective-permute-start.2 = (bf16[640,256]{1,0:T(8,128)(2,1)}, bf16[640,256]{1,0:T(8,128)(2,1)S(1)}, u32[]{:S(2)}, u32[]{:S(2)}) collective-permute-start(bf16[640,256]{1,0:T(8,128)(2,1)} %pad_maximum_fusion.1), channel_id=1, source_target_pairs={{0,32},{16,48},{32,0},{48,16},{1,33},{17,49},{33,1},{49,17},{2,34}... | collective-permute-start | bytes 983048 | tf_op jit(solution)/shard_map/ppermute | solution.py:20
  8.9 15.0 %collective-permute-start.1 = (bf16[640,256]{1,0:T(8,128)(2,1)}, bf16[640,256]{1,0:T(8,128)(2,1)S(1)}, u32[]{:S(2)}, u32[]{:S(2)}) collective-permute-start(bf16[640,256]{1,0:T(8,128)(2,1)} %pad_maximum_fusion.1), channel_id=1, source_target_pairs={{0,48},{16,0},{32,16},{48,32},{1,49},{17,1},{33,17},{49,33},{2,50}... | collective-permute-start | bytes 983048 | tf_op jit(solution)/shard_map/ppermute | solution.py:20
  16.2 1.1 copy-start.7
  17.1 15.5 %copy-start.8 = (bf16[128,256]{1,0:T(8,128)(2,1)S(1)}, bf16[128,256]{1,0:T(8,128)(2,1)}, u32[]{:S(2)}) copy-start(bf16[128,256]{1,0:T(8,128)(2,1)} %param.15) | copy-start | bytes 196612
  17.1 15.5 %copy-start.9 = (bf16[128,256]{1,0:T(8,128)(2,1)S(1)}, bf16[128,256]{1,0:T(8,128)(2,1)}, u32[]{:S(2)}) copy-start(bf16[128,256]{1,0:T(8,128)(2,1)} %param.14) | copy-start | bytes 196612
  17.2 15.6 %copy-start.10 = (bf16[128,256]{1,0:T(8,128)(2,1)S(1)}, bf16[128,256]{1,0:T(8,128)(2,1)}, u32[]{:S(2)}) copy-start(bf16[128,256]{1,0:T(8,128)(2,1)} %param.11) | copy-start | bytes 196612
  18.1 16.0 %copy-start.2 = (bf16[640,256]{1,0:T(8,128)(2,1)}, bf16[640,256]{1,0:T(8,128)(2,1)S(1)}, u32[]{:S(2)}) copy-start(bf16[640,256]{1,0:T(8,128)(2,1)S(1)} %collective-permute-done) | copy-start | bytes 983044
  23.9 10.1 %copy-start.3 = (bf16[640,256]{1,0:T(8,128)(2,1)}, bf16[640,256]{1,0:T(8,128)(2,1)S(1)}, u32[]{:S(2)}) copy-start(bf16[640,256]{1,0:T(8,128)(2,1)S(1)} %collective-permute-done.1) | copy-start | bytes 983044
  27.5 21.2 %collective-permute-start.3 = (bf16[3072,256]{1,0:T(8,128)(2,1)}, bf16[3072,256]{1,0:T(8,128)(2,1)}, u32[]{:S(2)}, u32[]{:S(2)}) collective-permute-start(bf16[3072,256]{1,0:T(8,128)(2,1)} %constant_dynamic-update-slice_fusion), channel_id=1, source_target_pairs={{0,1},{1,0},{2,3},{3,2},{4,5},{5,4},{6,7},{7,6},{8,9},{9,8},{10,11... | collective-permute-start | bytes 4718600 | tf_op jit(solution)/shard_map/ppermute | solution.py:20
  34.1 40.7 %all-to-all-start = ((bf16[8,136,512]{2,1,0:T(8,128)(2,1)}), bf16[8,136,512]{2,1,0:T(8,128)(2,1)S(1)}, u32[]{:S(2)}, u32[]{:S(2)}) async-start(bf16[8,136,512]{2,1,0:T(8,128)(2,1)} %broadcast_in_dim.20), calls=%async_computation | async-start | bytes 2228224 | tf_op jit(solution)/shard_map/all_to_all | solution.py:24
  76.2 3.3 %copy-start = (f32[2048,1024]{1,0:T(8,128)}, f32[2048,1024]{1,0:T(8,128)S(1)}, u32[]{:S(2)}) copy-start(f32[2048,1024]{1,0:T(8,128)S(1)} %get-tuple-element.98) | copy-start | bytes 25165828
  80.1 11.6 %all-to-all-start.1 = ((f32[8,16,128]{2,1,0:T(8,128)}), f32[8,16,128]{2,1,0:T(8,128)S(1)}, u32[]{:S(2)}, u32[]{:S(2)}) async-start(f32[8,16,128]{2,1,0:T(8,128)} %broadcast_in_dim.21), calls=%async_computation.1 | async-start | bytes 131072 | tf_op jit(solution)/shard_map/all_to_all | solution.py:24
  88.5 2.0 copy-start.12
  93.4 24.6 %all-to-all-start.2 = ((bf16[32,64,128]{2,1,0:T(8,128)(2,1)}), bf16[32,64,128]{2,1,0:T(8,128)(2,1)S(1)}, u32[]{:S(2)}, u32[]{:S(2)}) async-start(bf16[32,64,128]{2,1,0:T(8,128)(2,1)} %bitcast.17), calls=%async_computation.2 | async-start | bytes 1048576 | tf_op jit(solution)/shard_map/all_to_all | solution.py:24
  102.0 5.1 %copy-start.13 = (bf16[2048,1024]{1,0:T(8,128)(2,1)S(1)}, bf16[2048,1024]{1,0:T(8,128)(2,1)}, u32[]{:S(2)}) copy-start(bf16[2048,1024]{1,0:T(8,128)(2,1)} %copy-done.12) | copy-start | bytes 12582916
  108.4 5.9 %copy-start.1 = (f32[2048,256]{1,0:T(8,128)}, f32[2048,256]{1,0:T(8,128)S(1)}, u32[]{:S(2)}) copy-start(f32[2048,256]{1,0:T(8,128)S(1)} %fusion.21) | copy-start | bytes 6291460
  109.7 16.2 %collective-permute-start.4 = (bf16[1024,512]{1,0:T(8,128)(2,1)}, bf16[1024,512]{1,0:T(8,128)(2,1)}, u32[]{:S(2)}, u32[]{:S(2)}) collective-permute-start(bf16[1024,512]{1,0:T(8,128)(2,1)} %pad_maximum_fusion), channel_id=1, source_target_pairs={{0,1},{1,0},{2,3},{3,2},{4,5},{5,4},{6,7},{7,6},{8,9},{9,8},{10,11... | collective-permute-start | bytes 3145736 | tf_op jit(solution)/shard_map/ppermute | solution.py:20
  114.2 11.7 %slice-start = ((f32[2048,256]{1,0:T(8,128)}), f32[1024,256]{1,0:T(8,128)S(1)}, s32[]{:S(2)}) async-start(f32[2048,256]{1,0:T(8,128)} %copy-done.1), calls=%async_computation.6 | async-start | bytes 2097152 | tf_op jit(solution)/shard_map/slice | solution.py:121
  119.1 27.4 %all-to-all-start.3 = ((bf16[8,72,512]{2,1,0:T(8,128)(2,1)}), bf16[8,72,512]{2,1,0:T(8,128)(2,1)S(1)}, u32[]{:S(2)}, u32[]{:S(2)}) async-start(bf16[8,72,512]{2,1,0:T(8,128)(2,1)} %broadcast_in_dim.46), calls=%async_computation.3 | async-start | bytes 1179648 | tf_op jit(solution)/shard_map/all_to_all | solution.py:24
  125.9 11.6 %copy-start.6 = (bf16[256,256]{1,0:T(8,128)(2,1)S(1)}, bf16[256,256]{1,0:T(8,128)(2,1)}, u32[]{:S(2)}) copy-start(bf16[256,256]{1,0:T(8,128)(2,1)} %get-tuple-element.63) | copy-start | bytes 393220
  125.9 11.7 %copy-start.5 = (bf16[256,256]{1,0:T(8,128)(2,1)S(1)}, bf16[256,256]{1,0:T(8,128)(2,1)}, u32[]{:S(2)}) copy-start(bf16[256,256]{1,0:T(8,128)(2,1)} %get-tuple-element.65) | copy-start | bytes 393220
  127.9 9.9 %copy-start.4 = (bf16[256,8,1,1,64]{0,4,3,2,1:T(8,128)(2,1)S(1)}, bf16[256,8,1,1,64]{0,4,3,2,1:T(8,128)(2,1)}, u32[]{:S(2)}) copy-start(bf16[256,8,1,1,64]{0,4,3,2,1:T(8,128)(2,1)} %get-tuple-element.60) | copy-start | bytes 786436
  128.8 9.3 %collective-permute-start.5 = (bf16[256,512]{1,0:T(8,128)(2,1)}, bf16[256,512]{1,0:T(8,128)(2,1)}, u32[]{:S(2)}, u32[]{:S(2)}) collective-permute-start(bf16[256,512]{1,0:T(8,128)(2,1)} %get-tuple-element.77), channel_id=1, source_target_pairs={{0,32},{16,48},{32,0},{48,16},{1,33},{17,49},{33,1},{49,17},{2,34}... | collective-permute-start | bytes 786440 | tf_op jit(solution)/shard_map/ppermute | solution.py:20
  132.2 12.3 %collective-permute-start.6 = (bf16[256,512]{1,0:T(8,128)(2,1)}, bf16[256,512]{1,0:T(8,128)(2,1)}, u32[]{:S(2)}, u32[]{:S(2)}) collective-permute-start(bf16[256,512]{1,0:T(8,128)(2,1)} %get-tuple-element.78), channel_id=1, source_target_pairs={{0,16},{16,32},{32,48},{48,0},{1,17},{17,33},{33,49},{49,1},{2,18}... | collective-permute-start | bytes 786440 | tf_op jit(solution)/shard_map/ppermute | solution.py:20
  134.2 10.4 %collective-permute-start.7 = (bf16[256,512]{1,0:T(8,128)(2,1)}, bf16[256,512]{1,0:T(8,128)(2,1)}, u32[]{:S(2)}, u32[]{:S(2)}) collective-permute-start(bf16[256,512]{1,0:T(8,128)(2,1)} %get-tuple-element.79), channel_id=1, source_target_pairs={{0,48},{16,0},{32,16},{48,32},{1,49},{17,1},{33,17},{49,33},{2,50}... | collective-permute-start | bytes 786440 | tf_op jit(solution)/shard_map/ppermute | solution.py:20
  148.6 30.5 %all-to-all-start.4 = ((bf16[64,8,512]{2,1,0:T(8,128)(2,1)}), bf16[64,8,512]{2,1,0:T(8,128)(2,1)S(1)}, u32[]{:S(2)}, u32[]{:S(2)}) async-start(bf16[64,8,512]{2,1,0:T(8,128)(2,1)} %bitcast.32), calls=%async_computation.4 | async-start | bytes 1048576 | tf_op jit(solution)/shard_map/all_to_all | solution.py:24
  158.5 20.5 %copy-start.11 = (f32[256]{0:T(256)S(1)}, f32[256]{0:T(256)}, u32[]{:S(2)}) copy-start(f32[256]{0:T(256)} %param.9) | copy-start | bytes 3076
  159.0 9.6 %collective-permute-start.8 = (bf16[512,128]{1,0:T(8,128)(2,1)S(1)}, bf16[512,128]{1,0:T(8,128)(2,1)S(1)}, u32[]{:S(2)}, u32[]{:S(2)}) collective-permute-start(bf16[512,128]{1,0:T(8,128)(2,1)S(1)} %get-tuple-element.74), channel_id=1, source_target_pairs={{0,16},{16,32},{32,48},{48,0},{1,17},{17,33},{33,49},{49,1},{2,18}... | collective-permute-start | bytes 393224 | tf_op jit(solution)/shard_map/ppermute | solution.py:20
  162.1 10.1 %collective-permute-start.10 = (bf16[512,128]{1,0:T(8,128)(2,1)S(1)}, bf16[512,128]{1,0:T(8,128)(2,1)S(1)}, u32[]{:S(2)}, u32[]{:S(2)}) collective-permute-start(bf16[512,128]{1,0:T(8,128)(2,1)S(1)} %get-tuple-element.75), channel_id=1, source_target_pairs={{0,32},{16,48},{32,0},{48,16},{1,33},{17,49},{33,1},{49,17},{2,34}... | collective-permute-start | bytes 393224 | tf_op jit(solution)/shard_map/ppermute | solution.py:20
  164.8 11.7 %collective-permute-start.9 = (bf16[512,128]{1,0:T(8,128)(2,1)S(1)}, bf16[512,128]{1,0:T(8,128)(2,1)S(1)}, u32[]{:S(2)}, u32[]{:S(2)}) collective-permute-start(bf16[512,128]{1,0:T(8,128)(2,1)S(1)} %get-tuple-element.76), channel_id=1, source_target_pairs={{0,48},{16,0},{32,16},{48,32},{1,49},{17,1},{33,17},{49,33},{2,50}... | collective-permute-start | bytes 393224 | tf_op jit(solution)/shard_map/ppermute | solution.py:20
  176.6 9.1 %collective-permute-start.11 = (bf16[256,128]{1,0:T(8,128)(2,1)S(1)}, bf16[256,128]{1,0:T(8,128)(2,1)S(1)}, u32[]{:S(2)}, u32[]{:S(2)}) collective-permute-start(bf16[256,128]{1,0:T(8,128)(2,1)S(1)} %select_convert_fusion), channel_id=1, source_target_pairs={{0,1},{1,0},{2,3},{3,2},{4,5},{5,4},{6,7},{7,6},{8,9},{9,8},{10,11... | collective-permute-start | bytes 196616 | tf_op jit(solution)/shard_map/ppermute | solution.py:20
  179.1 19.0 %all-to-all-start.5 = ((bf16[8,32,512]{2,1,0:T(8,128)(2,1)}), bf16[8,32,512]{2,1,0:T(8,128)(2,1)S(1)}, u32[]{:S(2)}, u32[]{:S(2)}) async-start(bf16[8,32,512]{2,1,0:T(8,128)(2,1)} %bitcast.37), calls=%async_computation.5 | async-start | bytes 524288 | tf_op jit(solution)/shard_map/all_to_all | solution.py:24
where the time goes:
time: 202 us; the launch traced here: 201 us
  starting transfers between devices  83.9 us (42%)
  waiting for transfers between devices  51.7 us (26%)
  local copies, waits for them, and re-layouts  37 us (18%)
  matrix products  14.8 us (7%)
  other arithmetic  11.6 us (6%)
    all_to_all x6, starting transfers between devices, exchanged(): return lax.all_to_all(value, axis, split_axis=0, concat_axis=0, tiled=True)  45.3 us
    ppermute x12, starting transfers between devices, shifted(): return lax.ppermute(value, axis, [(i, (i + by) % n) for i in range(n)])  38.6 us
    all_to_all x6, waiting for transfers between devices, exchanged(): return lax.all_to_all(value, axis, split_axis=0, concat_axis=0, tiled=True)  32.3 us
    unnamed x50, local copies, waits for them, and re-layouts  22.9 us
    ppermute x12, waiting for transfers between devices, shifted(): return lax.ppermute(value, axis, [(i, (i + by) % n) for i in range(n)])  19.4 us
    dot_general x7, matrix products, dot(): lax.dot_general(a, b, (((ca,), (cb,)), ((), ())), preferred_element_type=...  14.8 us
  transfers between devices with their start and end apart: 18, of which 7 were waited for; matrix products, arithmetic and copies ran while one was open for 22% of the time, Pallas kernels for 0%

commit v1 on v0

--- a/solution.py
+++ b/solution.py
@@ -66,11 +66,17 @@
         v = lax.dynamic_slice(v, (0, core, 0, kv * HEAD_DIM), (ny, 1, bit, HEAD_DIM))
         return v.reshape(src // 2, HEAD_DIM)
 
-    pack = row_major(jnp.concatenate([half_of(keys), half_of(values), target], axis=0))
-    blocks = [pack] + [shifted(pack, "x", by) for by in (1, -1, 2)]
+    halves = (target[: rows // 2], target[rows // 2 :])
+    pack = jnp.concatenate([half_of(keys), half_of(values)], axis=1)
+    pack = row_major(jnp.concatenate([pack, jnp.concatenate(halves, axis=1)], axis=0))
+    blocks = [pack] + [row_major(shifted(pack, "x", by)) for by in (1, -1, 2)]
+    half = nx * src // 2
+    mine = row_major(jnp.concatenate([b[: src // 2] for b in blocks], axis=0))
     target_all = jnp.zeros((nx * rows, cols), BF16)
     for block, off in zip(blocks, (0, 3, 1, 2)):
-        target_all = lax.dynamic_update_slice(target_all, block[src:], (lax.rem(x_at + off, nx) * rows, 0))
+        block = jnp.concatenate([block[src // 2 :, :cols], block[src // 2 :, cols:]], axis=0)
+        target_all = lax.dynamic_update_slice(target_all, block, (lax.rem(x_at + off, nx) * rows, 0))
+    target_t = row_major(row_major(target_all).T)
 
     w_parts = lax.dynamic_slice(
         w_query.reshape(cols, HEADS // 2, 2, nx, part), (0, 0, 0, x_at, 0), (cols, HEADS // 2, 2, 1, part)
@@ -79,27 +85,33 @@
     w_odd = w_parts[:, :, 1].reshape(cols, -1)
     w_mine = jnp.where(core == 0, w_even, w_odd)
     w_theirs = jnp.where(core == 0, w_odd, w_even)
-    swap = [b[:src] for b in blocks] + [target_all, w_theirs[:, :cols], w_theirs[:, cols:]]
-    swap = shifted(row_major(jnp.concatenate(swap, axis=0)), "c", 1)
-    blocks = [b[:src] for b in blocks] + [swap[src * k : src * (k + 1)] for k in range(nx)]
-    key_all = row_major(jnp.concatenate([b[: src // 2] for b in blocks], axis=0))
-    value_all = row_major(jnp.concatenate([b[src // 2 :] for b in blocks], axis=0))
-    target_other = swap[nx * src : nx * src + nx * rows]
-    w_other = swap[nx * src + nx * rows :]
-    w_other = jnp.concatenate([w_other[:cols], w_other[cols:]], axis=1)
+    swap = shifted(row_major(jnp.concatenate([mine, target_t, w_theirs], axis=0)), "c", 1)
+    theirs, target_other, w_other = swap[:half], swap[half : half + cols], swap[half + cols :]
+    key_one, value_one = mine[:, :HEAD_DIM], mine[:, HEAD_DIM:]
+    key_two, value_two = theirs[:, :HEAD_DIM], theirs[:, HEAD_DIM:]
 
     both = both.reshape(nz, rows + 8, 2 * cols)
     query_all = both[:, :rows, :cols].reshape(n_rows, cols)
     grad_all = both[:, :rows, cols:].reshape(n_rows, cols)
     deltas = both[:, rows].astype(F32).reshape(nz, 4, rows).sum(axis=1).reshape(n_rows)
-    scores = dot(key_all, query_all, 1, 1) * SCALE
-    peak = jnp.max(scores, axis=0)
-    weights = jnp.exp(scores - peak[None])
-    total = jnp.sum(weights, axis=0)
+    score_one = dot(key_one, query_all, 1, 1) * SCALE
+    score_two = dot(key_two, query_all, 1, 1) * SCALE
+    peak = jnp.maximum(jnp.max(score_one, axis=0), jnp.max(score_two, axis=0))
+    weight_one = jnp.exp(score_one - peak[None])
+    weight_two = jnp.exp(score_two - peak[None])
+    total = jnp.sum(weight_one, axis=0) + jnp.sum(weight_two, axis=0)
+    weight_one, weight_two, total = lax.optimization_barrier(
+        (weight_one.astype(BF16), weight_two.astype(BF16), total)
+    )
     stats = told_all(jnp.concatenate([peak, total]).reshape(2 * nz, rows), "z").reshape(nz, 2, n_rows)
-    grad_weights = dot(value_all, grad_all, 1, 1)
-    grad_scores = (weights * ((grad_weights - deltas[None]) * SCALE)).astype(BF16)
-    query_t = dot(key_all, grad_scores, 0, 0)
+
+    def grads_of(weight, value):
+        product = dot(value, grad_all, 1, 1)
+        return (weight.astype(F32) * ((product - deltas[None]) * SCALE)).astype(BF16)
+
+    grad_one = grads_of(weight_one, value_one)
+    grad_two = grads_of(weight_two, value_two)
+    query_t = dot(key_one, grad_one, 0, 0) + dot(key_two, grad_two, 0, 0)
     query_t, stats = lax.optimization_barrier((query_t, stats))
     top = jnp.max(stats[:, 0], axis=0)
     log_totals = top + jnp.log(jnp.sum(stats[:, 1] * jnp.exp(stats[:, 0] - top[None]), axis=0))
@@ -114,29 +126,30 @@
     query_share, grad_share, _ = lax.optimization_barrier(
         ((query_all * share[:, None]).astype(BF16), (grad_all * share[:, None]).astype(BF16), sent)
     )
-    key_sum = dot(grad_scores, query_share, 1, 0)
-    value_sum = dot(weights.astype(BF16), grad_share, 1, 0)
-    half = nx * src // 2
-    theirs = jnp.concatenate([key_sum[half:], value_sum[half:]], axis=1).astype(BF16)
-    mine = jnp.concatenate([key_sum[:half], value_sum[:half]], axis=1)
-    mine = row_major((mine + shifted(row_major(theirs), "c", 1).astype(F32)).astype(BF16))
+
+    def sums_of(grad, weight):
+        return jnp.concatenate([dot(grad, query_share, 1, 0), dot(weight, grad_share, 1, 0)], axis=1)
+
+    swap = shifted(row_major(sums_of(grad_two, weight_two).astype(BF16)), "c", 1)
+    mine = row_major((sums_of(grad_one, weight_one) + swap.astype(F32)).astype(BF16))
     own, left, right, far = (mine[src // 2 * k : src // 2 * (k + 1)] for k in range(nx))
     own = own.astype(F32)
-    for block, by in ((far, 2), (right, 1), (left, -1)):
-        own = own + shifted(block, "x", by).astype(F32)
+    moved = [shifted(block, "x", by) for block, by in ((far, 2), (right, 1), (left, -1))]
+    for block in moved:
+        own = own + block.astype(F32)
     mine = own.astype(BF16)
 
     def by_core(mine, theirs):
         return jnp.where(core == 0, jnp.stack([mine, theirs]), jnp.stack([theirs, mine]))
 
-    target_both = by_core(target_all.T, target_other.T).astype(F32)
+    target_t, target_other, _ = lax.optimization_barrier((target_t, target_other, sent))
+    target_both = by_core(target_t, target_other).astype(F32)
     w_both = by_core(w_mine, w_other).reshape(2 * cols, -1)
     squares = jnp.sum(target_both * target_both, axis=(0, 1))
     high = lax.reduce_precision(squares, 8, 7)
     extra = jnp.stack([high, squares - high]).astype(BF16)
     piece = jnp.concatenate([part_t, extra, jnp.zeros((6, nx * rows), BF16)], axis=0)
     every = told_all(piece, "y").reshape(HEADS // 2, part + 8, nx * rows)
-    every, mine = lax.optimization_barrier((every, mine))
     grad_t = every[:, :part].reshape(HEADS // 2 * part, nx * rows)
     squares_all = every[:, part : part + 2].astype(F32).sum(axis=(0, 1))
     inverse = lax.rsqrt(squares_all / WIDTH + EPS)

time: 202 us -> 189 us (0.936)
  the two profiles are of different devices: /device:TPU:3 before, /device:TPU:1 now
where the time goes in v1:
time: 189 us; the launch traced here: 187 us
  starting transfers between devices  81.3 us (43%)
  waiting for transfers between devices  47.9 us (25%)
  local copies, waits for them, and re-layouts  23.2 us (12%)
  matrix products  18.5 us (10%)
  other arithmetic  14.9 us (8%)
    ppermute x12, starting transfers between devices, shifted(): return lax.ppermute(value, axis, [(i, (i + by) % n) for i in range(n)])  41.3 us
    all_to_all x6, waiting for transfers between devices, exchanged(): return lax.all_to_all(value, axis, split_axis=0, concat_axis=0, tiled=True)  40.8 us
    all_to_all x6, starting transfers between devices, exchanged(): return lax.all_to_all(value, axis, split_axis=0, concat_axis=0, tiled=True)  40 us
    dot_general x12, matrix products, dot(): lax.dot_general(a, b, (((ca,), (cb,)), ((), ())), preferred_element_type=...  18.5 us
    ppermute x12, waiting for transfers between devices, shifted(): return lax.ppermute(value, axis, [(i, (i + by) % n) for i in range(n)])  7.05 us
    unnamed x41, local copies, waits for them, and re-layouts  6.18 us
  transfers between devices with their start and end apart: 18, of which 6 were waited for; matrix products, arithmetic and copies ran while one was open for 21% of the time, Pallas kernels for 0%

profile of v1, /device:TPU:1, one launch (start us, length us, event | category | flops | bytes accessed | tf_op | source)
XLA Modules:
  0.0 187.4 jit_solution(6042532907015643363)
XLA Ops:
  1.4 1.0 constant_dynamic-slice_fusion
  3.8 3.9 %collective-permute-start = (bf16[320,512]{1,0:T(8,128)(2,1)}, bf16[320,512]{1,0:T(8,128)(2,1)}, u32[]{:S(2)}, u32[]{:S(2)}) collective-permute-start(bf16[320,512]{1,0:T(8,128)(2,1)} %maximum_maximum_fusion), channel_id=1, source_target_pairs={{0,16},{16,32},{32,48},{48,0},{1,17},{17,33},{33,49},{49,1},{2,18}... | collective-permute-start | bytes 983048 | tf_op jit(solution)/shard_map/ppermute | solution.py:20
  7.8 4.4 %collective-permute-start.2 = (bf16[320,512]{1,0:T(8,128)(2,1)}, bf16[320,512]{1,0:T(8,128)(2,1)}, u32[]{:S(2)}, u32[]{:S(2)}) collective-permute-start(bf16[320,512]{1,0:T(8,128)(2,1)} %maximum_maximum_fusion), channel_id=1, source_target_pairs={{0,32},{16,48},{32,0},{48,16},{1,33},{17,49},{33,1},{49,17},{2,34}... | collective-permute-start | bytes 983048 | tf_op jit(solution)/shard_map/ppermute | solution.py:20
  12.1 3.1 %collective-permute-start.1 = (bf16[320,512]{1,0:T(8,128)(2,1)}, bf16[320,512]{1,0:T(8,128)(2,1)}, u32[]{:S(2)}, u32[]{:S(2)}) collective-permute-start(bf16[320,512]{1,0:T(8,128)(2,1)} %maximum_maximum_fusion), channel_id=1, source_target_pairs={{0,48},{16,0},{32,16},{48,32},{1,49},{17,1},{33,17},{49,33},{2,50}... | collective-permute-start | bytes 983048 | tf_op jit(solution)/shard_map/ppermute | solution.py:20
  15.2 1.0 multiply_reduce_fusion.2
  16.3 1.0 maximum_maximum_fusion.1
  17.3 1.1 broadcast_in_dim.20
  18.4 10.0 %all-to-all-start = ((bf16[8,136,512]{2,1,0:T(8,128)(2,1)}), bf16[8,136,512]{2,1,0:T(8,128)(2,1)S(1)}, u32[]{:S(2)}, u32[]{:S(2)}) async-start(bf16[8,136,512]{2,1,0:T(8,128)(2,1)} %broadcast_in_dim.20), calls=%async_computation | async-start | bytes 2228224 | tf_op jit(solution)/shard_map/all_to_all | solution.py:24
  28.4 3.3 %copy.170 = bf16[256,4096]{0,1:T(8,128)(2,1)S(1)} copy(bf16[256,4096]{1,0:T(8,128)(2,1)} %param.10) | data formatting | bytes 4194304 | tf_op args[2]
  35.2 1.0 slice.156
  36.2 1.0 slice.158
  37.2 1.0 slice.157
  38.2 2.0 %pad_maximum_fusion = bf16[1536,512]{1,0:T(8,128)(2,1)} fusion(bf16[256,512]{1,0:T(8,128)(2,1)S(1)} %copy.174, bf16[256,512]{1,0:T(8,128)(2,1)S(1)} %bitcast.95, bf16[256,512]{1,0:T(8,128)(2,1)S(1)} %slice.158, bf16[256,512]{1,0:T(8,128)(2,1)S(1)} %slice.157, bf16[256,512]{1,0:T(8,128)(2,1)S(1)} %slice.156, bf16[256,256]{1,0:T(8,128)(2,1)S(1)} %bitcast.103, ...), kind=kLoop, calls=%fused_computation.12 | loop fusion | flops 11010048 | bytes 3145728 | tf_op jit(solution)/shard_map/concatenate | solution.py:88
  40.2 3.7 %collective-permute-start.3 = (bf16[1536,512]{1,0:T(8,128)(2,1)}, bf16[1536,512]{1,0:T(8,128)(2,1)}, u32[]{:S(2)}, u32[]{:S(2)}) collective-permute-start(bf16[1536,512]{1,0:T(8,128)(2,1)} %pad_maximum_fusion), channel_id=1, source_target_pairs={{0,1},{1,0},{2,3},{3,2},{4,5},{5,4},{6,7},{7,6},{8,9},{9,8},{10,11... | collective-permute-start | bytes 4718600 | tf_op jit(solution)/shard_map/ppermute | solution.py:20
  45.0 2.3 %collective-permute-done.3 = bf16[1536,512]{1,0:T(8,128)(2,1)} collective-permute-done((bf16[1536,512]{1,0:T(8,128)(2,1)}, bf16[1536,512]{1,0:T(8,128)(2,1)}, u32[]{:S(2)}, u32[]{:S(2)}) %collective-permute-start.3) | collective-permute-done | bytes 1572896 | tf_op jit(solution)/shard_map/ppermute | solution.py:20
  47.3 1.1 fusion.22
  48.3 10.7 %all-to-all-done = bf16[8,136,512]{2,1,0:T(8,128)(2,1)S(1)} async-done(((bf16[8,136,512]{2,1,0:T(8,128)(2,1)}), bf16[8,136,512]{2,1,0:T(8,128)(2,1)S(1)}, u32[]{:S(2)}, u32[]{:S(2)}) %all-to-all-start) | async-done | bytes 1114144 | tf_op jit(solution)/shard_map/all_to_all | solution.py:24
  59.0 0.9 fusion.23
  60.7 1.8 multiply_reduce_fusion
  62.6 3.1 %fusion.2 = (f32[1024]{0:T(1024)S(1)}, f32[1024]{0:T(1024)S(1)}, bf16[1024,1024]{1,0:T(8,128)(2,1)}, bf16[1024,1024]{1,0:T(8,128)(2,1)}) fusion(f32[1024,1024]{1,0:T(8,128)S(1)} %get-tuple-element.102, f32[1024]{0:T(1024)S(1)} %max.18, f32[1024,1024]{1,0:T(8,128)S(1)} %get-tuple-element.100), kind=kLoop, calls=%fused_computation.8 | loop fusion | flops 8386560 | bytes 12595200 | tf_op jit(solution)/shard_map/reduce_sum | solution.py:102
  66.3 3.4 %all-to-all-start.1 = ((f32[8,16,128]{2,1,0:T(8,128)}), f32[8,16,128]{2,1,0:T(8,128)S(1)}, u32[]{:S(2)}, u32[]{:S(2)}) async-start(f32[8,16,128]{2,1,0:T(8,128)} %broadcast_in_dim.21), calls=%async_computation.1 | async-start | bytes 131072 | tf_op jit(solution)/shard_map/all_to_all | solution.py:24
  69.7 2.6 %multiply_convert_fusion.1 = bf16[1024,1024]{1,0:T(8,128)(2,1)S(1)} fusion(bf16[1024,1024]{1,0:T(8,128)(2,1)} %get-tuple-element.15, bf16[1024,256]{1,0:T(8,128)(2,1)S(1)} %bitcast.112, f32[1024]{0:T(1024)S(1)} %bitcast.128, bf16[1024,512]{1,0:T(8,128)(2,1)S(1)} %pad_maximum_fusion.1), kind=kOutput, calls=%fused_computation.1 | convolution fusion | flops 542113792 | bytes 5246976 | tf_op jit(solution)/shard_map/dot_general | solution.py:33
  72.3 2.3 %multiply_convert_fusion = bf16[1024,1024]{1,0:T(8,128)(2,1)S(1)} fusion(bf16[1024,1024]{1,0:T(8,128)(2,1)S(1)} %copy-done.1, bf16[1024,256]{1,0:T(8,128)(2,1)S(1)} %bitcast.113, f32[1024]{0:T(1024)S(1)} %bitcast.129, bf16[1536,512]{1,0:T(8,128)(2,1)} %collective-permute-done.3), kind=kOutput, calls=%fused_computation | convolution fusion | flops 542113792 | bytes 5246976 | tf_op jit(solution)/shard_map/dot_general | solution.py:33
  74.5 2.1 %fusion.10 = f32[256,1024]{1,0:T(8,128)S(1)} fusion(bf16[1024,1024]{1,0:T(8,128)(2,1)S(1)} %multiply_convert_fusion, bf16[1536,512]{1,0:T(8,128)(2,1)} %collective-permute-done.3), kind=kOutput, calls=%fused_computation.33 | convolution fusion | flops 536870912 | bytes 3670016 | tf_op jit(solution)/shard_map/dot_general | solution.py:33
  76.7 1.8 convolution_add_fusion
  78.7 1.4 multiply_convert_fusion.2
  80.4 0.9 copy.179
  81.4 7.0 %all-to-all-start.2 = ((bf16[32,64,128]{2,1,0:T(8,128)(2,1)}), bf16[32,64,128]{2,1,0:T(8,128)(2,1)S(1)}, u32[]{:S(2)}, u32[]{:S(2)}) async-start(bf16[32,64,128]{2,1,0:T(8,128)(2,1)} %bitcast.18), calls=%async_computation.2 | async-start | bytes 1048576 | tf_op jit(solution)/shard_map/all_to_all | solution.py:24
  88.4 2.4 %convolution_convert_fusion.1 = bf16[1024,256]{1,0:T(8,128)(2,1)S(1)} fusion(bf16[1024,1024]{1,0:T(8,128)(2,1)} %get-tuple-element.16, bf16[1024,256]{1,0:T(8,128)(2,1)S(1)} %get-tuple-element.24), kind=kOutput, calls=%fused_computation.17 | convolution fusion | flops 537133056 | bytes 3145728 | tf_op jit(solution)/shard_map/dot_general | solution.py:33
  91.6 1.1 pad_maximum_fusion.2
  92.6 3.1 %collective-permute-start.8 = (bf16[1024,512]{1,0:T(8,128)(2,1)}, bf16[1024,512]{1,0:T(8,128)(2,1)}, u32[]{:S(2)}, u32[]{:S(2)}) collective-permute-start(bf16[1024,512]{1,0:T(8,128)(2,1)} %pad_maximum_fusion.2), channel_id=1, source_target_pairs={{0,1},{1,0},{2,3},{3,2},{4,5},{5,4},{6,7},{7,6},{8,9},{9,8},{10,11... | collective-permute-start | bytes 3145736 | tf_op jit(solution)/shard_map/ppermute | solution.py:20
  95.9 8.5 %all-to-all-done.2 = bf16[32,64,128]{2,1,0:T(8,128)(2,1)S(1)} async-done(((bf16[32,64,128]{2,1,0:T(8,128)(2,1)}), bf16[32,64,128]{2,1,0:T(8,128)(2,1)S(1)}, u32[]{:S(2)}, u32[]{:S(2)}) %all-to-all-start.2) | async-done | bytes 524320 | tf_op jit(solution)/shard_map/all_to_all | solution.py:24
  105.5 6.8 %all-to-all-start.3 = ((bf16[8,72,512]{2,1,0:T(8,128)(2,1)}), bf16[8,72,512]{2,1,0:T(8,128)(2,1)S(1)}, u32[]{:S(2)}, u32[]{:S(2)}) async-start(bf16[8,72,512]{2,1,0:T(8,128)(2,1)} %broadcast_in_dim.23), calls=%async_computation.3 | async-start | bytes 1179648 | tf_op jit(solution)/shard_map/all_to_all | solution.py:24
  112.4 2.5 %fusion.32 = f32[1024,256]{1,0:T(8,128)S(1)} fusion(bf16[1024,1024]{1,0:T(8,128)(2,1)} %get-tuple-element.15, bf16[1024,256]{1,0:T(8,128)(2,1)S(1)} %copy-done.16), kind=kOutput, calls=%fused_computation.92 | convolution fusion | flops 536870912 | bytes 3670016 | tf_op jit(solution)/shard_map/dot_general | solution.py:33
  115.6 1.5 fusion.4
  117.1 11.6 %all-to-all-done.3 = bf16[8,72,512]{2,1,0:T(8,128)(2,1)S(1)} async-done(((bf16[8,72,512]{2,1,0:T(8,128)(2,1)}), bf16[8,72,512]{2,1,0:T(8,128)(2,1)S(1)}, u32[]{:S(2)}, u32[]{:S(2)}) %all-to-all-start.3) | async-done | bytes 589856 | tf_op jit(solution)/shard_map/all_to_all | solution.py:24
  130.2 9.4 %all-to-all-start.4 = ((bf16[64,8,512]{2,1,0:T(8,128)(2,1)}), bf16[64,8,512]{2,1,0:T(8,128)(2,1)S(1)}, u32[]{:S(2)}, u32[]{:S(2)}) async-start(bf16[64,8,512]{2,1,0:T(8,128)(2,1)} %bitcast.29), calls=%async_computation.4 | async-start | bytes 1048576 | tf_op jit(solution)/shard_map/all_to_all | solution.py:24
  140.2 3.3 %collective-permute-start.4 = (bf16[512,128]{1,0:T(8,128)(2,1)S(1)}, bf16[512,128]{1,0:T(8,128)(2,1)S(1)}, u32[]{:S(2)}, u32[]{:S(2)}) collective-permute-start(bf16[512,128]{1,0:T(8,128)(2,1)S(1)} %get-tuple-element.79), channel_id=1, source_target_pairs={{0,16},{16,32},{32,48},{48,0},{1,17},{17,33},{33,49},{49,1},{2,18}... | collective-permute-start | bytes 393224 | tf_op jit(solution)/shard_map/ppermute | solution.py:20
  143.5 4.3 %collective-permute-start.6 = (bf16[512,128]{1,0:T(8,128)(2,1)S(1)}, bf16[512,128]{1,0:T(8,128)(2,1)S(1)}, u32[]{:S(2)}, u32[]{:S(2)}) collective-permute-start(bf16[512,128]{1,0:T(8,128)(2,1)S(1)} %get-tuple-element.80), channel_id=1, source_target_pairs={{0,32},{16,48},{32,0},{48,16},{1,33},{17,49},{33,1},{49,17},{2,34}... | collective-permute-start | bytes 393224 | tf_op jit(solution)/shard_map/ppermute | solution.py:20
  147.8 3.1 %collective-permute-start.5 = (bf16[512,128]{1,0:T(8,128)(2,1)S(1)}, bf16[512,128]{1,0:T(8,128)(2,1)S(1)}, u32[]{:S(2)}, u32[]{:S(2)}) collective-permute-start(bf16[512,128]{1,0:T(8,128)(2,1)S(1)} %get-tuple-element.81), channel_id=1, source_target_pairs={{0,48},{16,0},{32,16},{48,32},{1,49},{17,1},{33,17},{49,33},{2,50}... | collective-permute-start | bytes 393224 | tf_op jit(solution)/shard_map/ppermute | solution.py:20
  151.0 2.0 %collective-permute-start.9 = (bf16[256,512]{1,0:T(8,128)(2,1)S(1)}, bf16[256,512]{1,0:T(8,128)(2,1)S(1)}, u32[]{:S(2)}, u32[]{:S(2)}) collective-permute-start(bf16[256,512]{1,0:T(8,128)(2,1)S(1)} %get-tuple-element.76), channel_id=1, source_target_pairs={{0,32},{16,48},{32,0},{48,16},{1,33},{17,49},{33,1},{49,17},{2,34}... | collective-permute-start | bytes 786440 | tf_op jit(solution)/shard_map/ppermute | solution.py:20
  153.0 2.4 %collective-permute-start.10 = (bf16[256,512]{1,0:T(8,128)(2,1)S(1)}, bf16[256,512]{1,0:T(8,128)(2,1)S(1)}, u32[]{:S(2)}, u32[]{:S(2)}) collective-permute-start(bf16[256,512]{1,0:T(8,128)(2,1)S(1)} %get-tuple-element.77), channel_id=1, source_target_pairs={{0,16},{16,32},{32,48},{48,0},{1,17},{17,33},{33,49},{49,1},{2,18}... | collective-permute-start | bytes 786440 | tf_op jit(solution)/shard_map/ppermute | solution.py:20
  155.4 4.1 %collective-permute-start.11 = (bf16[256,512]{1,0:T(8,128)(2,1)S(1)}, bf16[256,512]{1,0:T(8,128)(2,1)S(1)}, u32[]{:S(2)}, u32[]{:S(2)}) collective-permute-start(bf16[256,512]{1,0:T(8,128)(2,1)S(1)} %get-tuple-element.78), channel_id=1, source_target_pairs={{0,48},{16,0},{32,16},{48,32},{1,49},{17,1},{33,17},{49,33},{2,50}... | collective-permute-start | bytes 786440 | tf_op jit(solution)/shard_map/ppermute | solution.py:20
  159.6 4.0 %collective-permute-start.7 = (bf16[256,128]{1,0:T(8,128)(2,1)S(1)}, bf16[256,128]{1,0:T(8,128)(2,1)S(1)}, u32[]{:S(2)}, u32[]{:S(2)}) collective-permute-start(bf16[256,128]{1,0:T(8,128)(2,1)S(1)} %select_convert_fusion), channel_id=1, source_target_pairs={{0,1},{1,0},{2,3},{3,2},{4,5},{5,4},{6,7},{7,6},{8,9},{9,8},{10,11... | collective-permute-start | bytes 196616 | tf_op jit(solution)/shard_map/ppermute | solution.py:20
  163.7 4.8 %collective-permute-done.10 = bf16[256,512]{1,0:T(8,128)(2,1)S(1)} collective-permute-done((bf16[256,512]{1,0:T(8,128)(2,1)S(1)}, bf16[256,512]{1,0:T(8,128)(2,1)S(1)}, u32[]{:S(2)}, u32[]{:S(2)}) %collective-permute-start.10) | collective-permute-done | bytes 262176 | tf_op jit(solution)/shard_map/ppermute | solution.py:20
  169.3 3.4 %all-to-all-start.5 = ((bf16[8,32,512]{2,1,0:T(8,128)(2,1)}), bf16[8,32,512]{2,1,0:T(8,128)(2,1)S(1)}, u32[]{:S(2)}, u32[]{:S(2)}) async-start(bf16[8,32,512]{2,1,0:T(8,128)(2,1)} %bitcast.34), calls=%async_computation.5 | async-start | bytes 524288 | tf_op jit(solution)/shard_map/all_to_all | solution.py:24
  173.9 0.9 reshape.206
  174.8 10.1 %all-to-all-done.5 = bf16[8,32,512]{2,1,0:T(8,128)(2,1)S(1)} async-done(((bf16[8,32,512]{2,1,0:T(8,128)(2,1)}), bf16[8,32,512]{2,1,0:T(8,128)(2,1)S(1)}, u32[]{:S(2)}, u32[]{:S(2)}) %all-to-all-start.5) | async-done | bytes 262176 | tf_op jit(solution)/shard_map/all_to_all | solution.py:24
  (122 shorter events, 18.1 us)
Async XLA Ops:
  2.4 0.7 copy-start.4
  2.4 1.4 copy-start.6
  3.8 28.8 %collective-permute-start = (bf16[320,512]{1,0:T(8,128)(2,1)}, bf16[320,512]{1,0:T(8,128)(2,1)}, u32[]{:S(2)}, u32[]{:S(2)}) collective-permute-start(bf16[320,512]{1,0:T(8,128)(2,1)} %maximum_maximum_fusion), channel_id=1, source_target_pairs={{0,16},{16,32},{32,48},{48,0},{1,17},{17,33},{33,49},{49,1},{2,18}... | collective-permute-start | bytes 983048 | tf_op jit(solution)/shard_map/ppermute | solution.py:20
  7.8 26.5 %collective-permute-start.2 = (bf16[320,512]{1,0:T(8,128)(2,1)}, bf16[320,512]{1,0:T(8,128)(2,1)}, u32[]{:S(2)}, u32[]{:S(2)}) collective-permute-start(bf16[320,512]{1,0:T(8,128)(2,1)} %maximum_maximum_fusion), channel_id=1, source_target_pairs={{0,32},{16,48},{32,0},{48,16},{1,33},{17,49},{33,1},{49,17},{2,34}... | collective-permute-start | bytes 983048 | tf_op jit(solution)/shard_map/ppermute | solution.py:20
  12.1 21.3 %collective-permute-start.1 = (bf16[320,512]{1,0:T(8,128)(2,1)}, bf16[320,512]{1,0:T(8,128)(2,1)}, u32[]{:S(2)}, u32[]{:S(2)}) collective-permute-start(bf16[320,512]{1,0:T(8,128)(2,1)} %maximum_maximum_fusion), channel_id=1, source_target_pairs={{0,48},{16,0},{32,16},{48,32},{1,49},{17,1},{33,17},{49,33},{2,50}... | collective-permute-start | bytes 983048 | tf_op jit(solution)/shard_map/ppermute | solution.py:20
  18.4 40.6 %all-to-all-start = ((bf16[8,136,512]{2,1,0:T(8,128)(2,1)}), bf16[8,136,512]{2,1,0:T(8,128)(2,1)S(1)}, u32[]{:S(2)}, u32[]{:S(2)}) async-start(bf16[8,136,512]{2,1,0:T(8,128)(2,1)} %broadcast_in_dim.20), calls=%async_computation | async-start | bytes 2228224 | tf_op jit(solution)/shard_map/all_to_all | solution.py:24
  32.5 5.8 %copy-start.5 = (bf16[8,1,32,256]{3,2,1,0:T(8,128)(2,1)S(1)}, bf16[8,1,32,256]{3,2,1,0:T(8,128)(2,1)}, u32[]{:S(2)}) copy-start(bf16[8,1,32,256]{3,2,1,0:T(8,128)(2,1)} %copy-done.4) | copy-start | bytes 393220
  32.5 5.8 %copy-start.7 = (bf16[8,1,32,256]{3,2,1,0:T(8,128)(2,1)S(1)}, bf16[8,1,32,256]{3,2,1,0:T(8,128)(2,1)}, u32[]{:S(2)}) copy-start(bf16[8,1,32,256]{3,2,1,0:T(8,128)(2,1)} %copy-done.6) | copy-start | bytes 393220
  36.2 7.8 %copy-start.11 = (bf16[256,8,1,1,64]{0,4,3,2,1:T(8,128)(2,1)S(1)}, bf16[256,8,1,1,64]{0,4,3,2,1:T(8,128)(2,1)}, u32[]{:S(2)}) copy-start(bf16[256,8,1,1,64]{0,4,3,2,1:T(8,128)(2,1)} %get-tuple-element.70) | copy-start | bytes 786436
  37.2 7.6 %copy-start.17 = (f32[256]{0:T(256)S(1)}, f32[256]{0:T(256)}, u32[]{:S(2)}) copy-start(f32[256]{0:T(256)} %param.9) | copy-start | bytes 3076
  40.2 7.1 %collective-permute-start.3 = (bf16[1536,512]{1,0:T(8,128)(2,1)}, bf16[1536,512]{1,0:T(8,128)(2,1)}, u32[]{:S(2)}, u32[]{:S(2)}) collective-permute-start(bf16[1536,512]{1,0:T(8,128)(2,1)} %pad_maximum_fusion), channel_id=1, source_target_pairs={{0,1},{1,0},{2,3},{3,2},{4,5},{5,4},{6,7},{7,6},{8,9},{9,8},{10,11... | collective-permute-start | bytes 4718600 | tf_op jit(solution)/shard_map/ppermute | solution.py:20
  62.5 7.1 %copy-start.10 = (bf16[8,128,256]{2,1,0:T(8,128)(2,1)S(1)}, bf16[8,128,256]{2,1,0:T(8,128)(2,1)}, u32[]{:S(2)}) copy-start(bf16[8,128,256]{2,1,0:T(8,128)(2,1)} %get-tuple-element.74) | copy-start | bytes 1572868
  66.3 12.2 %all-to-all-start.1 = ((f32[8,16,128]{2,1,0:T(8,128)}), f32[8,16,128]{2,1,0:T(8,128)S(1)}, u32[]{:S(2)}, u32[]{:S(2)}) async-start(f32[8,16,128]{2,1,0:T(8,128)} %broadcast_in_dim.21), calls=%async_computation.1 | async-start | bytes 131072 | tf_op jit(solution)/shard_map/all_to_all | solution.py:24
  69.7 2.6 %copy-start.1 = (bf16[1024,1024]{1,0:T(8,128)(2,1)S(1)}, bf16[1024,1024]{1,0:T(8,128)(2,1)}, u32[]{:S(2)}) copy-start(bf16[1024,1024]{1,0:T(8,128)(2,1)} %get-tuple-element.16) | copy-start | bytes 6291460
  72.3 4.4 %copy-start.8 = (bf16[1024,1024]{1,0:T(8,128)(2,1)}, bf16[1024,1024]{1,0:T(8,128)(2,1)S(1)}, u32[]{:S(2)}) copy-start(bf16[1024,1024]{1,0:T(8,128)(2,1)S(1)} %multiply_convert_fusion.1) | copy-start | bytes 6291460
  74.5 2.2 %copy-start.2 = (bf16[1024,1024]{1,0:T(8,128)(2,1)}, bf16[1024,1024]{1,0:T(8,128)(2,1)S(1)}, u32[]{:S(2)}) copy-start(bf16[1024,1024]{1,0:T(8,128)(2,1)S(1)} %multiply_convert_fusion) | copy-start | bytes 6291460
  78.5 1.6 copy-start
  80.2 8.2 %copy-start.15 = (bf16[1024,256]{1,0:T(8,128)(2,1)}, bf16[1024,256]{1,0:T(8,128)(2,1)S(1)}, u32[]{:S(2)}) copy-start(bf16[1024,256]{1,0:T(8,128)(2,1)S(1)} %get-tuple-element.24) | copy-start | bytes 1572868
  80.2 10.7 %copy-start.13 = (bf16[1024,256]{1,0:T(8,128)(2,1)}, bf16[1024,256]{1,0:T(8,128)(2,1)S(1)}, u32[]{:S(2)}) copy-start(bf16[1024,256]{1,0:T(8,128)(2,1)S(1)} %get-tuple-element.23) | copy-start | bytes 1572868
  81.4 23.0 %all-to-all-start.2 = ((bf16[32,64,128]{2,1,0:T(8,128)(2,1)}), bf16[32,64,128]{2,1,0:T(8,128)(2,1)S(1)}, u32[]{:S(2)}, u32[]{:S(2)}) async-start(bf16[32,64,128]{2,1,0:T(8,128)(2,1)} %bitcast.18), calls=%async_computation.2 | async-start | bytes 1048576 | tf_op jit(solution)/shard_map/all_to_all | solution.py:24
  88.4 2.5 %copy-start.3 = (bf16[1024,1024]{1,0:T(8,128)(2,1)S(1)}, bf16[1024,1024]{1,0:T(8,128)(2,1)}, u32[]{:S(2)}) copy-start(bf16[1024,1024]{1,0:T(8,128)(2,1)} %copy-done.2) | copy-start | bytes 6291460
  92.6 19.6 %copy-start.12 = (bf16[1,256,512]{2,1,0:T(8,128)(2,1)S(1)}, bf16[1,256,512]{2,1,0:T(8,128)(2,1)}, u32[]{:S(2)}) copy-start(bf16[1,256,512]{2,1,0:T(8,128)(2,1)} %copy.175) | copy-start | bytes 786436
  92.6 23.0 %collective-permute-start.8 = (bf16[1024,512]{1,0:T(8,128)(2,1)}, bf16[1024,512]{1,0:T(8,128)(2,1)}, u32[]{:S(2)}, u32[]{:S(2)}) collective-permute-start(bf16[1024,512]{1,0:T(8,128)(2,1)} %pad_maximum_fusion.2), channel_id=1, source_target_pairs={{0,1},{1,0},{2,3},{3,2},{4,5},{5,4},{6,7},{7,6},{8,9},{9,8},{10,11... | collective-permute-start | bytes 3145736 | tf_op jit(solution)/shard_map/ppermute | solution.py:20
  95.7 16.6 %copy-start.16 = (bf16[1024,256]{1,0:T(8,128)(2,1)S(1)}, bf16[1024,256]{1,0:T(8,128)(2,1)}, u32[]{:S(2)}) copy-start(bf16[1024,256]{1,0:T(8,128)(2,1)} %copy-done.15) | copy-start | bytes 1572868
  105.5 23.2 %all-to-all-start.3 = ((bf16[8,72,512]{2,1,0:T(8,128)(2,1)}), bf16[8,72,512]{2,1,0:T(8,128)(2,1)S(1)}, u32[]{:S(2)}, u32[]{:S(2)}) async-start(bf16[8,72,512]{2,1,0:T(8,128)(2,1)} %broadcast_in_dim.23), calls=%async_computation.3 | async-start | bytes 1179648 | tf_op jit(solution)/shard_map/all_to_all | solution.py:24
  112.4 2.5 %copy-start.9 = (bf16[1024,1024]{1,0:T(8,128)(2,1)S(1)}, bf16[1024,1024]{1,0:T(8,128)(2,1)}, u32[]{:S(2)}) copy-start(bf16[1024,1024]{1,0:T(8,128)(2,1)} %copy-done.8) | copy-start | bytes 6291460
  112.4 2.5 %copy-start.14 = (bf16[1024,256]{1,0:T(8,128)(2,1)S(1)}, bf16[1024,256]{1,0:T(8,128)(2,1)}, u32[]{:S(2)}) copy-start(bf16[1024,256]{1,0:T(8,128)(2,1)} %copy-done.13) | copy-start | bytes 1572868
  130.2 39.1 %all-to-all-start.4 = ((bf16[64,8,512]{2,1,0:T(8,128)(2,1)}), bf16[64,8,512]{2,1,0:T(8,128)(2,1)S(1)}, u32[]{:S(2)}, u32[]{:S(2)}) async-start(bf16[64,8,512]{2,1,0:T(8,128)(2,1)} %bitcast.29), calls=%async_computation.4 | async-start | bytes 1048576 | tf_op jit(solution)/shard_map/all_to_all | solution.py:24
  140.2 15.2 %collective-permute-start.4 = (bf16[512,128]{1,0:T(8,128)(2,1)S(1)}, bf16[512,128]{1,0:T(8,128)(2,1)S(1)}, u32[]{:S(2)}, u32[]{:S(2)}) collective-permute-start(bf16[512,128]{1,0:T(8,128)(2,1)S(1)} %get-tuple-element.79), channel_id=1, source_target_pairs={{0,16},{16,32},{32,48},{48,0},{1,17},{17,33},{33,49},{49,1},{2,18}... | collective-permute-start | bytes 393224 | tf_op jit(solution)/shard_map/ppermute | solution.py:20
  143.5 16.0 %collective-permute-start.6 = (bf16[512,128]{1,0:T(8,128)(2,1)S(1)}, bf16[512,128]{1,0:T(8,128)(2,1)S(1)}, u32[]{:S(2)}, u32[]{:S(2)}) collective-permute-start(bf16[512,128]{1,0:T(8,128)(2,1)S(1)} %get-tuple-element.80), channel_id=1, source_target_pairs={{0,32},{16,48},{32,0},{48,16},{1,33},{17,49},{33,1},{49,17},{2,34}... | collective-permute-start | bytes 393224 | tf_op jit(solution)/shard_map/ppermute | solution.py:20
  147.8 11.7 %collective-permute-start.5 = (bf16[512,128]{1,0:T(8,128)(2,1)S(1)}, bf16[512,128]{1,0:T(8,128)(2,1)S(1)}, u32[]{:S(2)}, u32[]{:S(2)}) collective-permute-start(bf16[512,128]{1,0:T(8,128)(2,1)S(1)} %get-tuple-element.81), channel_id=1, source_target_pairs={{0,48},{16,0},{32,16},{48,32},{1,49},{17,1},{33,17},{49,33},{2,50}... | collective-permute-start | bytes 393224 | tf_op jit(solution)/shard_map/ppermute | solution.py:20
  151.0 12.7 %collective-permute-start.9 = (bf16[256,512]{1,0:T(8,128)(2,1)S(1)}, bf16[256,512]{1,0:T(8,128)(2,1)S(1)}, u32[]{:S(2)}, u32[]{:S(2)}) collective-permute-start(bf16[256,512]{1,0:T(8,128)(2,1)S(1)} %get-tuple-element.76), channel_id=1, source_target_pairs={{0,32},{16,48},{32,0},{48,16},{1,33},{17,49},{33,1},{49,17},{2,34}... | collective-permute-start | bytes 786440 | tf_op jit(solution)/shard_map/ppermute | solution.py:20
  153.0 15.5 %collective-permute-start.10 = (bf16[256,512]{1,0:T(8,128)(2,1)S(1)}, bf16[256,512]{1,0:T(8,128)(2,1)S(1)}, u32[]{:S(2)}, u32[]{:S(2)}) collective-permute-start(bf16[256,512]{1,0:T(8,128)(2,1)S(1)} %get-tuple-element.77), channel_id=1, source_target_pairs={{0,16},{16,32},{32,48},{48,0},{1,17},{17,33},{33,49},{49,1},{2,18}... | collective-permute-start | bytes 786440 | tf_op jit(solution)/shard_map/ppermute | solution.py:20
  155.4 13.1 %collective-permute-start.11 = (bf16[256,512]{1,0:T(8,128)(2,1)S(1)}, bf16[256,512]{1,0:T(8,128)(2,1)S(1)}, u32[]{:S(2)}, u32[]{:S(2)}) collective-permute-start(bf16[256,512]{1,0:T(8,128)(2,1)S(1)} %get-tuple-element.78), channel_id=1, source_target_pairs={{0,48},{16,0},{32,16},{48,32},{1,49},{17,1},{33,17},{49,33},{2,50}... | collective-permute-start | bytes 786440 | tf_op jit(solution)/shard_map/ppermute | solution.py:20
  159.6 13.1 %collective-permute-start.7 = (bf16[256,128]{1,0:T(8,128)(2,1)S(1)}, bf16[256,128]{1,0:T(8,128)(2,1)S(1)}, u32[]{:S(2)}, u32[]{:S(2)}) collective-permute-start(bf16[256,128]{1,0:T(8,128)(2,1)S(1)} %select_convert_fusion), channel_id=1, source_target_pairs={{0,1},{1,0},{2,3},{3,2},{4,5},{5,4},{6,7},{7,6},{8,9},{9,8},{10,11... | collective-permute-start | bytes 196616 | tf_op jit(solution)/shard_map/ppermute | solution.py:20
  169.3 15.6 %all-to-all-start.5 = ((bf16[8,32,512]{2,1,0:T(8,128)(2,1)}), bf16[8,32,512]{2,1,0:T(8,128)(2,1)S(1)}, u32[]{:S(2)}, u32[]{:S(2)}) async-start(bf16[8,32,512]{2,1,0:T(8,128)(2,1)} %bitcast.34), calls=%async_computation.5 | async-start | bytes 524288 | tf_op jit(solution)/shard_map/all_to_all | solution.py:24

commit v2 on v1

--- a/solution.py
+++ b/solution.py
@@ -66,17 +66,12 @@
         v = lax.dynamic_slice(v, (0, core, 0, kv * HEAD_DIM), (ny, 1, bit, HEAD_DIM))
         return v.reshape(src // 2, HEAD_DIM)
 
-    halves = (target[: rows // 2], target[rows // 2 :])
-    pack = jnp.concatenate([half_of(keys), half_of(values)], axis=1)
-    pack = row_major(jnp.concatenate([pack, jnp.concatenate(halves, axis=1)], axis=0))
-    blocks = [pack] + [row_major(shifted(pack, "x", by)) for by in (1, -1, 2)]
+    pack = row_major(jnp.concatenate([half_of(keys), half_of(values), target], axis=0))
+    blocks = [pack] + [shifted(pack, "x", by) for by in (1, -1, 2)]
     half = nx * src // 2
-    mine = row_major(jnp.concatenate([b[: src // 2] for b in blocks], axis=0))
     target_all = jnp.zeros((nx * rows, cols), BF16)
     for block, off in zip(blocks, (0, 3, 1, 2)):
-        block = jnp.concatenate([block[src // 2 :, :cols], block[src // 2 :, cols:]], axis=0)
-        target_all = lax.dynamic_update_slice(target_all, block, (lax.rem(x_at + off, nx) * rows, 0))
-    target_t = row_major(row_major(target_all).T)
+        target_all = lax.dynamic_update_slice(target_all, block[src:], (lax.rem(x_at + off, nx) * rows, 0))
 
     w_parts = lax.dynamic_slice(
         w_query.reshape(cols, HEADS // 2, 2, nx, part), (0, 0, 0, x_at, 0), (cols, HEADS // 2, 2, 1, part)
@@ -85,10 +80,11 @@
     w_odd = w_parts[:, :, 1].reshape(cols, -1)
     w_mine = jnp.where(core == 0, w_even, w_odd)
     w_theirs = jnp.where(core == 0, w_odd, w_even)
-    swap = shifted(row_major(jnp.concatenate([mine, target_t, w_theirs], axis=0)), "c", 1)
-    theirs, target_other, w_other = swap[:half], swap[half : half + cols], swap[half + cols :]
-    key_one, value_one = mine[:, :HEAD_DIM], mine[:, HEAD_DIM:]
-    key_two, value_two = theirs[:, :HEAD_DIM], theirs[:, HEAD_DIM:]
+    mine = [b[: src // 2] for b in blocks] + [b[src // 2 : src] for b in blocks]
+    mine = row_major(jnp.concatenate(mine + [target_all, w_theirs[:, :cols], w_theirs[:, cols:]], axis=0))
+    theirs = shifted(mine, "c", 1)
+    key_one, value_one = mine[:half], mine[half : 2 * half]
+    key_two, value_two = theirs[:half], theirs[half : 2 * half]
 
     both = both.reshape(nz, rows + 8, 2 * cols)
     query_all = both[:, :rows, :cols].reshape(n_rows, cols)
@@ -120,18 +116,31 @@
     sent = (query_t * share[None]).astype(BF16).reshape(nx, part, nz, rows).transpose(2, 0, 1, 3)
     sent = sent.reshape(nz * nx, part, rows)
     got = exchanged(sent, ("z", "x")).reshape(nz, nx, part, rows)
+
+    query_share, grad_share, _ = lax.optimization_barrier(
+        ((query_all * share[:, None]).astype(BF16), (grad_all * share[:, None]).astype(BF16), sent)
+    )
+
+    def sums_of(grad, weight):
+        return jnp.concatenate([dot(grad, query_share, 1, 0), dot(weight, grad_share, 1, 0)], axis=1)
+
+    swap = shifted(row_major(sums_of(grad_two, weight_two).astype(BF16)), "c", 1)
+    mine = row_major((sums_of(grad_one, weight_one) + swap.astype(F32)).astype(BF16))
+
+    def by_core(mine, theirs):
+        return jnp.where(core == 0, jnp.stack([mine, theirs]), jnp.stack([theirs, mine]))
+
+    theirs, target_all, w_mine, _ = lax.optimization_barrier((theirs[2 * half :], target_all, w_mine, sent))
+    target_other, w_other = theirs[: nx * rows], theirs[nx * rows :]
+    w_other = jnp.concatenate([w_other[:cols], w_other[cols:]], axis=1)
+    target_both = row_major(by_core(row_major(target_all.T), row_major(target_other.T)))
+    w_both = by_core(w_mine, w_other).reshape(2 * cols, -1)
+    squares = jnp.sum(jnp.square(target_both.astype(F32)), axis=(0, 1))
+
+    got, mine, target_both = lax.optimization_barrier((got, mine, target_both))
+    target_both = target_both.astype(F32)
     part_t = got.astype(F32).sum(axis=0)
     part_t = part_t.transpose(1, 0, 2).reshape(part, nx * rows).astype(BF16)
-
-    query_share, grad_share, _ = lax.optimization_barrier(
-        ((query_all * share[:, None]).astype(BF16), (grad_all * share[:, None]).astype(BF16), sent)
-    )
-
-    def sums_of(grad, weight):
-        return jnp.concatenate([dot(grad, query_share, 1, 0), dot(weight, grad_share, 1, 0)], axis=1)
-
-    swap = shifted(row_major(sums_of(grad_two, weight_two).astype(BF16)), "c", 1)
-    mine = row_major((sums_of(grad_one, weight_one) + swap.astype(F32)).astype(BF16))
     own, left, right, far = (mine[src // 2 * k : src // 2 * (k + 1)] for k in range(nx))
     own = own.astype(F32)
     moved = [shifted(block, "x", by) for block, by in ((far, 2), (right, 1), (left, -1))]
@@ -139,13 +148,6 @@
         own = own + block.astype(F32)
     mine = own.astype(BF16)
 
-    def by_core(mine, theirs):
-        return jnp.where(core == 0, jnp.stack([mine, theirs]), jnp.stack([theirs, mine]))
-
-    target_t, target_other, _ = lax.optimization_barrier((target_t, target_other, sent))
-    target_both = by_core(target_t, target_other).astype(F32)
-    w_both = by_core(w_mine, w_other).reshape(2 * cols, -1)
-    squares = jnp.sum(target_both * target_both, axis=(0, 1))
     high = lax.reduce_precision(squares, 8, 7)
     extra = jnp.stack([high, squares - high]).astype(BF16)
     piece = jnp.concatenate([part_t, extra, jnp.zeros((6, nx * rows), BF16)], axis=0)

time: 189 us -> 197 us (1.042)
  the two profiles are of different devices: /device:TPU:1 before, /device:TPU:2 now
where the time goes in v2:
time: 197 us; the launch traced here: 195 us
  starting transfers between devices  81.2 us (41%)
  waiting for transfers between devices  42.9 us (22%)
  local copies, waits for them, and re-layouts  42.3 us (21%)
  other arithmetic  15 us (8%)
  matrix products  12.3 us (6%)
    all_to_all x6, starting transfers between devices, exchanged(): return lax.all_to_all(value, axis, split_axis=0, concat_axis=0, tiled=True)  42.9 us
    ppermute x12, starting transfers between devices, shifted(): return lax.ppermute(value, axis, [(i, (i + by) % n) for i in range(n)])  38.2 us
    all_to_all x6, waiting for transfers between devices, exchanged(): return lax.all_to_all(value, axis, split_axis=0, concat_axis=0, tiled=True)  32.1 us
    unnamed x53, local copies, waits for them, and re-layouts  24.9 us
    dot_general x12, matrix products, dot(): lax.dot_general(a, b, (((ca,), (cb,)), ((), ())), preferred_element_type=...  12.3 us
    ppermute x12, waiting for transfers between devices, shifted(): return lax.ppermute(value, axis, [(i, (i + by) % n) for i in range(n)])  10.8 us
  transfers between devices with their start and end apart: 18, of which 7 were waited for; matrix products, arithmetic and copies ran while one was open for 23% of the time, Pallas kernels for 0%

profile of v2, /device:TPU:2, one launch (start us, length us, event | category | flops | bytes accessed | tf_op | source)
XLA Modules:
  0.0 195.1 jit_solution(4921891032779505009)
XLA Ops:
  0.7 1.0 constant_dynamic-slice_fusion
  3.5 4.0 %collective-permute-start.2 = (bf16[640,256]{0,1:T(8,128)(2,1)}, bf16[640,256]{0,1:T(8,128)(2,1)}, u32[]{:S(2)}, u32[]{:S(2)}) collective-permute-start(bf16[640,256]{0,1:T(8,128)(2,1)} %copy.220), channel_id=1, source_target_pairs={{0,32},{16,48},{32,0},{48,16},{1,33},{17,49},{33,1},{49,17},{2,34}... | collective-permute-start | bytes 983048 | tf_op jit(solution)/shard_map/ppermute | solution.py:20
  7.5 5.7 %collective-permute-start.1 = (bf16[640,256]{0,1:T(8,128)(2,1)}, bf16[640,256]{0,1:T(8,128)(2,1)}, u32[]{:S(2)}, u32[]{:S(2)}) collective-permute-start(bf16[640,256]{0,1:T(8,128)(2,1)} %copy.220), channel_id=1, source_target_pairs={{0,48},{16,0},{32,16},{48,32},{1,49},{17,1},{33,17},{49,33},{2,50}... | collective-permute-start | bytes 983048 | tf_op jit(solution)/shard_map/ppermute | solution.py:20
  13.2 3.4 %collective-permute-start = (bf16[640,256]{0,1:T(8,128)(2,1)}, bf16[640,256]{0,1:T(8,128)(2,1)}, u32[]{:S(2)}, u32[]{:S(2)}) collective-permute-start(bf16[640,256]{0,1:T(8,128)(2,1)} %copy.220), channel_id=1, source_target_pairs={{0,16},{16,32},{32,48},{48,0},{1,17},{17,33},{33,49},{49,1},{2,18}... | collective-permute-start | bytes 983048 | tf_op jit(solution)/shard_map/ppermute | solution.py:20
  17.8 1.1 broadcast_in_dim.20
  18.9 7.1 %all-to-all-start = ((bf16[8,136,512]{2,1,0:T(8,128)(2,1)}), bf16[8,136,512]{2,1,0:T(8,128)(2,1)S(1)}, u32[]{:S(2)}, u32[]{:S(2)}) async-start(bf16[8,136,512]{2,1,0:T(8,128)(2,1)} %broadcast_in_dim.20), calls=%async_computation | async-start | bytes 2228224 | tf_op jit(solution)/shard_map/all_to_all | solution.py:24
  26.0 1.6 slice_dynamic-update-slice_fusion.9
  27.6 3.3 %copy.226 = bf16[256,4096]{0,1:T(8,128)(2,1)S(1)} copy(bf16[256,4096]{1,0:T(8,128)(2,1)} %param.10) | data formatting | bytes 4194304 | tf_op args[2]
  32.5 1.6 slice_dynamic-update-slice_fusion.8
  34.1 1.6 slice_dynamic-update-slice_fusion.7
  35.7 1.6 slice_dynamic-update-slice_fusion.6
  37.3 1.6 slice_dynamic-update-slice_fusion.5
  38.9 1.6 slice_dynamic-update-slice_fusion.4
  40.5 1.6 slice_dynamic-update-slice_fusion.3
  42.1 1.6 slice_dynamic-update-slice_fusion.2
  48.4 1.7 copy.227
  50.1 1.9 collective-permute-start.3
  52.1 3.3 %collective-permute-done.3 = bf16[3072,256]{1,0:T(8,128)(2,1)S(1)} collective-permute-done((bf16[3072,256]{1,0:T(8,128)(2,1)S(1)}, bf16[3072,256]{1,0:T(8,128)(2,1)S(1)}, u32[]{:S(2)}, u32[]{:S(2)}) %collective-permute-start.3) | collective-permute-done | bytes 1572896 | tf_op jit(solution)/shard_map/ppermute | solution.py:20
  55.4 1.2 copy-done.10
  59.2 1.8 multiply_reduce_fusion
  61.0 3.1 %fusion.2 = (f32[1024]{0:T(1024)S(1)}, f32[1024]{0:T(1024)S(1)}, bf16[1024,1024]{1,0:T(8,128)(2,1)}, bf16[1024,1024]{1,0:T(8,128)(2,1)}) fusion(f32[1024,1024]{1,0:T(8,128)S(1)} %get-tuple-element.104, f32[1024]{0:T(1024)S(1)} %max.18, f32[1024,1024]{1,0:T(8,128)S(1)} %get-tuple-element.102), kind=kLoop, calls=%fused_computation.8 | loop fusion | flops 8386560 | bytes 12595200 | tf_op jit(solution)/shard_map/reduce_sum | solution.py:98
  64.7 7.2 %all-to-all-start.1 = ((f32[8,16,128]{2,1,0:T(8,128)}), f32[8,16,128]{2,1,0:T(8,128)S(1)}, u32[]{:S(2)}, u32[]{:S(2)}) async-start(f32[8,16,128]{2,1,0:T(8,128)} %broadcast_in_dim.21), calls=%async_computation.1 | async-start | bytes 131072 | tf_op jit(solution)/shard_map/all_to_all | solution.py:24
  71.9 2.5 %multiply_convert_fusion.1 = bf16[1024,1024]{1,0:T(8,128)(2,1)S(1)} fusion(bf16[1024,1024]{1,0:T(8,128)(2,1)} %get-tuple-element.19, bf16[1024,256]{1,0:T(8,128)(2,1)S(1)} %bitcast.105, f32[1024]{0:T(1024)S(1)} %bitcast.126, bf16[3072,256]{1,0:T(8,128)(2,1)S(1)} %copy.227), kind=kOutput, calls=%fused_computation.1 | convolution fusion | flops 542113792 | bytes 5246976 | tf_op jit(solution)/shard_map/dot_general | solution.py:33
  75.2 1.6 copy-done.1
  77.7 1.4 copy-done.5
  80.5 2.3 %multiply_convert_fusion.3 = (bf16[1024,256]{1,0:T(8,128)(2,1)}, bf16[1024,256]{1,0:T(8,128)(2,1)}) fusion(f32[1024]{0:T(1024)S(1)} %subtract_exponential_fusion.2, bf16[8,128,256]{2,1,0:T(8,128)(2,1)} %get-tuple-element.82, bf16[8,128,256]{2,1,0:T(8,128)(2,1)S(1)} %get-tuple-element.83), kind=kLoop, calls=%fused_computation.20 | loop fusion | flops 1572864 | bytes 2101248 | tf_op jit(solution)/shard_map/convert_element_type | solution.py:121
  84.0 10.2 %all-to-all-start.2 = ((bf16[32,64,128]{2,1,0:T(8,128)(2,1)}), bf16[32,64,128]{2,1,0:T(8,128)(2,1)}, u32[]{:S(2)}, u32[]{:S(2)}) async-start(bf16[32,64,128]{2,1,0:T(8,128)(2,1)} %bitcast.15), calls=%async_computation.2 | async-start | bytes 1048576 | tf_op jit(solution)/shard_map/all_to_all | solution.py:24
  96.6 1.1 pad_maximum_fusion
  97.6 2.2 %collective-permute-start.4 = (bf16[1024,512]{1,0:T(8,128)(2,1)}, bf16[1024,512]{1,0:T(8,128)(2,1)}, u32[]{:S(2)}, u32[]{:S(2)}) collective-permute-start(bf16[1024,512]{1,0:T(8,128)(2,1)} %pad_maximum_fusion), channel_id=1, source_target_pairs={{0,1},{1,0},{2,3},{3,2},{4,5},{5,4},{6,7},{7,6},{8,9},{9,8},{10,11... | collective-permute-start | bytes 3145736 | tf_op jit(solution)/shard_map/ppermute | solution.py:20
  100.8 1.3 multiply_reduce_fusion.2
  102.1 1.9 fusion.25
  104.7 1.5 fusion.4
  106.2 4.5 %all-to-all-done.2 = bf16[32,64,128]{2,1,0:T(8,128)(2,1)} async-done(((bf16[32,64,128]{2,1,0:T(8,128)(2,1)}), bf16[32,64,128]{2,1,0:T(8,128)(2,1)}, u32[]{:S(2)}, u32[]{:S(2)}) %all-to-all-start.2) | async-done | bytes 524320 | tf_op jit(solution)/shard_map/all_to_all | solution.py:24
  110.8 1.1 reduce_sum.100
  112.9 7.1 %all-to-all-start.3 = ((bf16[8,72,512]{2,1,0:T(8,128)(2,1)}), bf16[8,72,512]{2,1,0:T(8,128)(2,1)S(1)}, u32[]{:S(2)}, u32[]{:S(2)}) async-start(bf16[8,72,512]{2,1,0:T(8,128)(2,1)} %broadcast_in_dim.23), calls=%async_computation.3 | async-start | bytes 1179648 | tf_op jit(solution)/shard_map/all_to_all | solution.py:24
  120.3 17.0 %all-to-all-done.3 = bf16[8,72,512]{2,1,0:T(8,128)(2,1)S(1)} async-done(((bf16[8,72,512]{2,1,0:T(8,128)(2,1)}), bf16[8,72,512]{2,1,0:T(8,128)(2,1)S(1)}, u32[]{:S(2)}, u32[]{:S(2)}) %all-to-all-start.3) | async-done | bytes 589856 | tf_op jit(solution)/shard_map/all_to_all | solution.py:24
  138.9 7.9 %all-to-all-start.4 = ((bf16[64,8,512]{2,1,0:T(8,128)(2,1)}), bf16[64,8,512]{2,1,0:T(8,128)(2,1)S(1)}, u32[]{:S(2)}, u32[]{:S(2)}) async-start(bf16[64,8,512]{2,1,0:T(8,128)(2,1)} %bitcast.32), calls=%async_computation.4 | async-start | bytes 1048576 | tf_op jit(solution)/shard_map/all_to_all | solution.py:24
  147.3 3.4 %collective-permute-start.5 = (bf16[512,128]{1,0:T(8,128)(2,1)S(1)}, bf16[512,128]{1,0:T(8,128)(2,1)S(1)}, u32[]{:S(2)}, u32[]{:S(2)}) collective-permute-start(bf16[512,128]{1,0:T(8,128)(2,1)S(1)} %get-tuple-element.87), channel_id=1, source_target_pairs={{0,16},{16,32},{32,48},{48,0},{1,17},{17,33},{33,49},{49,1},{2,18}... | collective-permute-start | bytes 393224 | tf_op jit(solution)/shard_map/ppermute | solution.py:20
  150.7 3.0 %collective-permute-start.7 = (bf16[512,128]{1,0:T(8,128)(2,1)S(1)}, bf16[512,128]{1,0:T(8,128)(2,1)S(1)}, u32[]{:S(2)}, u32[]{:S(2)}) collective-permute-start(bf16[512,128]{1,0:T(8,128)(2,1)S(1)} %get-tuple-element.88), channel_id=1, source_target_pairs={{0,32},{16,48},{32,0},{48,16},{1,33},{17,49},{33,1},{49,17},{2,34}... | collective-permute-start | bytes 393224 | tf_op jit(solution)/shard_map/ppermute | solution.py:20
  153.7 4.1 %collective-permute-start.6 = (bf16[512,128]{1,0:T(8,128)(2,1)S(1)}, bf16[512,128]{1,0:T(8,128)(2,1)S(1)}, u32[]{:S(2)}, u32[]{:S(2)}) collective-permute-start(bf16[512,128]{1,0:T(8,128)(2,1)S(1)} %get-tuple-element.89), channel_id=1, source_target_pairs={{0,48},{16,0},{32,16},{48,32},{1,49},{17,1},{33,17},{49,33},{2,50}... | collective-permute-start | bytes 393224 | tf_op jit(solution)/shard_map/ppermute | solution.py:20
  157.8 2.2 %collective-permute-start.9 = (bf16[256,512]{1,0:T(8,128)(2,1)S(1)}, bf16[256,512]{1,0:T(8,128)(2,1)S(1)}, u32[]{:S(2)}, u32[]{:S(2)}) collective-permute-start(bf16[256,512]{1,0:T(8,128)(2,1)S(1)} %get-tuple-element.84), channel_id=1, source_target_pairs={{0,32},{16,48},{32,0},{48,16},{1,33},{17,49},{33,1},{49,17},{2,34}... | collective-permute-start | bytes 786440 | tf_op jit(solution)/shard_map/ppermute | solution.py:20
  160.1 3.5 %collective-permute-start.11 = (bf16[256,512]{1,0:T(8,128)(2,1)S(1)}, bf16[256,512]{1,0:T(8,128)(2,1)S(1)}, u32[]{:S(2)}, u32[]{:S(2)}) collective-permute-start(bf16[256,512]{1,0:T(8,128)(2,1)S(1)} %get-tuple-element.85), channel_id=1, source_target_pairs={{0,48},{16,0},{32,16},{48,32},{1,49},{17,1},{33,17},{49,33},{2,50}... | collective-permute-start | bytes 786440 | tf_op jit(solution)/shard_map/ppermute | solution.py:20
  163.6 2.9 %collective-permute-start.10 = (bf16[256,512]{1,0:T(8,128)(2,1)S(1)}, bf16[256,512]{1,0:T(8,128)(2,1)S(1)}, u32[]{:S(2)}, u32[]{:S(2)}) collective-permute-start(bf16[256,512]{1,0:T(8,128)(2,1)S(1)} %get-tuple-element.86), channel_id=1, source_target_pairs={{0,16},{16,32},{32,48},{48,0},{1,17},{17,33},{33,49},{49,1},{2,18}... | collective-permute-start | bytes 786440 | tf_op jit(solution)/shard_map/ppermute | solution.py:20
  166.6 3.4 %collective-permute-done.6 = bf16[512,128]{1,0:T(8,128)(2,1)S(1)} collective-permute-done((bf16[512,128]{1,0:T(8,128)(2,1)S(1)}, bf16[512,128]{1,0:T(8,128)(2,1)S(1)}, u32[]{:S(2)}, u32[]{:S(2)}) %collective-permute-start.6) | collective-permute-done | bytes 131104 | tf_op jit(solution)/shard_map/ppermute | solution.py:20
  170.1 1.9 collective-permute-start.8
  172.0 4.1 %collective-permute-done.11 = bf16[256,512]{1,0:T(8,128)(2,1)S(1)} collective-permute-done((bf16[256,512]{1,0:T(8,128)(2,1)S(1)}, bf16[256,512]{1,0:T(8,128)(2,1)S(1)}, u32[]{:S(2)}, u32[]{:S(2)}) %collective-permute-start.11) | collective-permute-done | bytes 262176 | tf_op jit(solution)/shard_map/ppermute | solution.py:20
  177.0 3.4 %all-to-all-start.5 = ((bf16[8,32,512]{2,1,0:T(8,128)(2,1)}), bf16[8,32,512]{2,1,0:T(8,128)(2,1)S(1)}, u32[]{:S(2)}, u32[]{:S(2)}) async-start(bf16[8,32,512]{2,1,0:T(8,128)(2,1)} %bitcast.37), calls=%async_computation.5 | async-start | bytes 524288 | tf_op jit(solution)/shard_map/all_to_all | solution.py:24
  182.5 10.1 %all-to-all-done.5 = bf16[8,32,512]{2,1,0:T(8,128)(2,1)S(1)} async-done(((bf16[8,32,512]{2,1,0:T(8,128)(2,1)}), bf16[8,32,512]{2,1,0:T(8,128)(2,1)S(1)}, u32[]{:S(2)}, u32[]{:S(2)}) %all-to-all-start.5) | async-done | bytes 262176 | tf_op jit(solution)/shard_map/all_to_all | solution.py:24
  (130 shorter events, 29.6 us)
Async XLA Ops:
  0.6 17.1 %copy-start.16 = (bf16[128,256]{1,0:T(8,128)(2,1)S(1)}, bf16[128,256]{1,0:T(8,128)(2,1)}, u32[]{:S(2)}) copy-start(bf16[128,256]{1,0:T(8,128)(2,1)} %param.15) | copy-start | bytes 196612
  0.6 17.1 %copy-start.17 = (bf16[128,256]{1,0:T(8,128)(2,1)S(1)}, bf16[128,256]{1,0:T(8,128)(2,1)}, u32[]{:S(2)}) copy-start(bf16[128,256]{1,0:T(8,128)(2,1)} %param.11) | copy-start | bytes 196612
  3.5 32.2 %collective-permute-start.2 = (bf16[640,256]{0,1:T(8,128)(2,1)}, bf16[640,256]{0,1:T(8,128)(2,1)}, u32[]{:S(2)}, u32[]{:S(2)}) collective-permute-start(bf16[640,256]{0,1:T(8,128)(2,1)} %copy.220), channel_id=1, source_target_pairs={{0,32},{16,48},{32,0},{48,16},{1,33},{17,49},{33,1},{49,17},{2,34}... | collective-permute-start | bytes 983048 | tf_op jit(solution)/shard_map/ppermute | solution.py:20
  7.5 26.6 %collective-permute-start.1 = (bf16[640,256]{0,1:T(8,128)(2,1)}, bf16[640,256]{0,1:T(8,128)(2,1)}, u32[]{:S(2)}, u32[]{:S(2)}) collective-permute-start(bf16[640,256]{0,1:T(8,128)(2,1)} %copy.220), channel_id=1, source_target_pairs={{0,48},{16,0},{32,16},{48,32},{1,49},{17,1},{33,17},{49,33},{2,50}... | collective-permute-start | bytes 983048 | tf_op jit(solution)/shard_map/ppermute | solution.py:20
  13.2 19.3 %collective-permute-start = (bf16[640,256]{0,1:T(8,128)(2,1)}, bf16[640,256]{0,1:T(8,128)(2,1)}, u32[]{:S(2)}, u32[]{:S(2)}) collective-permute-start(bf16[640,256]{0,1:T(8,128)(2,1)} %copy.220), channel_id=1, source_target_pairs={{0,16},{16,32},{32,48},{48,0},{1,17},{17,33},{33,49},{49,1},{2,18}... | collective-permute-start | bytes 983048 | tf_op jit(solution)/shard_map/ppermute | solution.py:20
  18.9 38.6 %all-to-all-start = ((bf16[8,136,512]{2,1,0:T(8,128)(2,1)}), bf16[8,136,512]{2,1,0:T(8,128)(2,1)S(1)}, u32[]{:S(2)}, u32[]{:S(2)}) async-start(bf16[8,136,512]{2,1,0:T(8,128)(2,1)} %broadcast_in_dim.20), calls=%async_computation | async-start | bytes 2228224 | tf_op jit(solution)/shard_map/all_to_all | solution.py:24
  50.1 5.3 %collective-permute-start.3 = (bf16[3072,256]{1,0:T(8,128)(2,1)S(1)}, bf16[3072,256]{1,0:T(8,128)(2,1)S(1)}, u32[]{:S(2)}, u32[]{:S(2)}) collective-permute-start(bf16[3072,256]{1,0:T(8,128)(2,1)S(1)} %copy.227), channel_id=1, source_target_pairs={{0,1},{1,0},{2,3},{3,2},{4,5},{5,4},{6,7},{7,6},{8,9},{9,8},{10,11... | collective-permute-start | bytes 4718600 | tf_op jit(solution)/shard_map/ppermute | solution.py:20
  55.4 1.2 copy-start.10
  61.0 10.9 %copy-start.8 = (bf16[8,128,256]{2,1,0:T(8,128)(2,1)S(1)}, bf16[8,128,256]{2,1,0:T(8,128)(2,1)}, u32[]{:S(2)}) copy-start(bf16[8,128,256]{2,1,0:T(8,128)(2,1)} %get-tuple-element.82) | copy-start | bytes 1572868
  64.7 15.6 %all-to-all-start.1 = ((f32[8,16,128]{2,1,0:T(8,128)}), f32[8,16,128]{2,1,0:T(8,128)S(1)}, u32[]{:S(2)}, u32[]{:S(2)}) async-start(f32[8,16,128]{2,1,0:T(8,128)} %broadcast_in_dim.21), calls=%async_computation.1 | async-start | bytes 131072 | tf_op jit(solution)/shard_map/all_to_all | solution.py:24
  71.9 3.3 %copy-start.11 = (bf16[3072,256]{1,0:T(8,128)(2,1)S(1)}, bf16[3072,256]{1,0:T(8,128)(2,1)}, u32[]{:S(2)}) copy-start(bf16[3072,256]{1,0:T(8,128)(2,1)} %copy-done.10) | copy-start | bytes 4718596
  74.4 3.3 %copy-start.3 = (bf16[1024,1024]{1,0:T(8,128)(2,1)}, bf16[1024,1024]{1,0:T(8,128)(2,1)S(1)}, u32[]{:S(2)}) copy-start(bf16[1024,1024]{1,0:T(8,128)(2,1)S(1)} %multiply_convert_fusion.1) | copy-start | bytes 6291460
  74.5 2.3 %copy-start.1 = (bf16[1024,1024]{1,0:T(8,128)(2,1)S(1)}, bf16[1024,1024]{1,0:T(8,128)(2,1)}, u32[]{:S(2)}) copy-start(bf16[1024,1024]{1,0:T(8,128)(2,1)} %get-tuple-element.20) | copy-start | bytes 6291460
  74.5 2.4 %copy-start.9 = (bf16[8,128,256]{2,1,0:T(8,128)(2,1)S(1)}, bf16[8,128,256]{2,1,0:T(8,128)(2,1)}, u32[]{:S(2)}) copy-start(bf16[8,128,256]{2,1,0:T(8,128)(2,1)} %get-tuple-element.82) | copy-start | bytes 1572868
  77.7 1.4 copy-start.5
  82.8 11.4 %copy-start.2 = (bf16[1024,1024]{1,0:T(8,128)(2,1)S(1)}, bf16[1024,1024]{1,0:T(8,128)(2,1)}, u32[]{:S(2)}) copy-start(bf16[1024,1024]{1,0:T(8,128)(2,1)} %get-tuple-element.20) | copy-start | bytes 6291460
  82.9 11.3 %copy-start.15 = (bf16[1024,256]{1,0:T(8,128)(2,1)S(1)}, bf16[1024,256]{1,0:T(8,128)(2,1)}, u32[]{:S(2)}) copy-start(bf16[1024,256]{1,0:T(8,128)(2,1)} %get-tuple-element.27) | copy-start | bytes 1572868
  84.0 26.8 %all-to-all-start.2 = ((bf16[32,64,128]{2,1,0:T(8,128)(2,1)}), bf16[32,64,128]{2,1,0:T(8,128)(2,1)}, u32[]{:S(2)}, u32[]{:S(2)}) async-start(bf16[32,64,128]{2,1,0:T(8,128)(2,1)} %bitcast.15), calls=%async_computation.2 | async-start | bytes 1048576 | tf_op jit(solution)/shard_map/all_to_all | solution.py:24
  94.2 1.6 copy-start.6
  94.2 1.7 copy-start.13
  96.6 3.3 %copy-start.7 = (bf16[1024,256]{1,0:T(8,128)(2,1)S(1)}, bf16[1024,256]{1,0:T(8,128)(2,1)}, u32[]{:S(2)}) copy-start(bf16[1024,256]{1,0:T(8,128)(2,1)} %slice.176) | copy-start | bytes 1572868
  96.6 5.5 %copy-start = (bf16[1024,1024]{1,0:T(8,128)(2,1)S(1)}, bf16[1024,1024]{1,0:T(8,128)(2,1)}, u32[]{:S(2)}) copy-start(bf16[1024,1024]{1,0:T(8,128)(2,1)} %get-tuple-element.19) | copy-start | bytes 6291460
  97.6 7.1 %collective-permute-start.4 = (bf16[1024,512]{1,0:T(8,128)(2,1)}, bf16[1024,512]{1,0:T(8,128)(2,1)}, u32[]{:S(2)}, u32[]{:S(2)}) collective-permute-start(bf16[1024,512]{1,0:T(8,128)(2,1)} %pad_maximum_fusion), channel_id=1, source_target_pairs={{0,1},{1,0},{2,3},{3,2},{4,5},{5,4},{6,7},{7,6},{8,9},{9,8},{10,11... | collective-permute-start | bytes 3145736 | tf_op jit(solution)/shard_map/ppermute | solution.py:20
  102.0 1.9 copy-start.4
  102.1 1.9 copy-start.14
  106.2 13.8 %copy-start.18 = (f32[256]{0:T(256)S(1)}, f32[256]{0:T(256)}, u32[]{:S(2)}) copy-start(f32[256]{0:T(256)} %param.9) | copy-start | bytes 3076
  106.2 13.8 %copy-start.12 = (bf16[256,8,1,1,64]{0,4,3,2,1:T(8,128)(2,1)S(1)}, bf16[256,8,1,1,64]{0,4,3,2,1:T(8,128)(2,1)}, u32[]{:S(2)}) copy-start(bf16[256,8,1,1,64]{0,4,3,2,1:T(8,128)(2,1)} %get-tuple-element.80) | copy-start | bytes 786436
  112.9 24.4 %all-to-all-start.3 = ((bf16[8,72,512]{2,1,0:T(8,128)(2,1)}), bf16[8,72,512]{2,1,0:T(8,128)(2,1)S(1)}, u32[]{:S(2)}, u32[]{:S(2)}) async-start(bf16[8,72,512]{2,1,0:T(8,128)(2,1)} %broadcast_in_dim.23), calls=%async_computation.3 | async-start | bytes 1179648 | tf_op jit(solution)/shard_map/all_to_all | solution.py:24
  138.9 38.1 %all-to-all-start.4 = ((bf16[64,8,512]{2,1,0:T(8,128)(2,1)}), bf16[64,8,512]{2,1,0:T(8,128)(2,1)S(1)}, u32[]{:S(2)}, u32[]{:S(2)}) async-start(bf16[64,8,512]{2,1,0:T(8,128)(2,1)} %bitcast.32), calls=%async_computation.4 | async-start | bytes 1048576 | tf_op jit(solution)/shard_map/all_to_all | solution.py:24
  147.3 16.3 %collective-permute-start.5 = (bf16[512,128]{1,0:T(8,128)(2,1)S(1)}, bf16[512,128]{1,0:T(8,128)(2,1)S(1)}, u32[]{:S(2)}, u32[]{:S(2)}) collective-permute-start(bf16[512,128]{1,0:T(8,128)(2,1)S(1)} %get-tuple-element.87), channel_id=1, source_target_pairs={{0,16},{16,32},{32,48},{48,0},{1,17},{17,33},{33,49},{49,1},{2,18}... | collective-permute-start | bytes 393224 | tf_op jit(solution)/shard_map/ppermute | solution.py:20
  150.7 15.8 %collective-permute-start.7 = (bf16[512,128]{1,0:T(8,128)(2,1)S(1)}, bf16[512,128]{1,0:T(8,128)(2,1)S(1)}, u32[]{:S(2)}, u32[]{:S(2)}) collective-permute-start(bf16[512,128]{1,0:T(8,128)(2,1)S(1)} %get-tuple-element.88), channel_id=1, source_target_pairs={{0,32},{16,48},{32,0},{48,16},{1,33},{17,49},{33,1},{49,17},{2,34}... | collective-permute-start | bytes 393224 | tf_op jit(solution)/shard_map/ppermute | solution.py:20
  153.7 16.3 %collective-permute-start.6 = (bf16[512,128]{1,0:T(8,128)(2,1)S(1)}, bf16[512,128]{1,0:T(8,128)(2,1)S(1)}, u32[]{:S(2)}, u32[]{:S(2)}) collective-permute-start(bf16[512,128]{1,0:T(8,128)(2,1)S(1)} %get-tuple-element.89), channel_id=1, source_target_pairs={{0,48},{16,0},{32,16},{48,32},{1,49},{17,1},{33,17},{49,33},{2,50}... | collective-permute-start | bytes 393224 | tf_op jit(solution)/shard_map/ppermute | solution.py:20
  157.8 14.2 %collective-permute-start.9 = (bf16[256,512]{1,0:T(8,128)(2,1)S(1)}, bf16[256,512]{1,0:T(8,128)(2,1)S(1)}, u32[]{:S(2)}, u32[]{:S(2)}) collective-permute-start(bf16[256,512]{1,0:T(8,128)(2,1)S(1)} %get-tuple-element.84), channel_id=1, source_target_pairs={{0,32},{16,48},{32,0},{48,16},{1,33},{17,49},{33,1},{49,17},{2,34}... | collective-permute-start | bytes 786440 | tf_op jit(solution)/shard_map/ppermute | solution.py:20
  160.1 16.0 %collective-permute-start.11 = (bf16[256,512]{1,0:T(8,128)(2,1)S(1)}, bf16[256,512]{1,0:T(8,128)(2,1)S(1)}, u32[]{:S(2)}, u32[]{:S(2)}) collective-permute-start(bf16[256,512]{1,0:T(8,128)(2,1)S(1)} %get-tuple-element.85), channel_id=1, source_target_pairs={{0,48},{16,0},{32,16},{48,32},{1,49},{17,1},{33,17},{49,33},{2,50}... | collective-permute-start | bytes 786440 | tf_op jit(solution)/shard_map/ppermute | solution.py:20
  163.6 12.5 %collective-permute-start.10 = (bf16[256,512]{1,0:T(8,128)(2,1)S(1)}, bf16[256,512]{1,0:T(8,128)(2,1)S(1)}, u32[]{:S(2)}, u32[]{:S(2)}) collective-permute-start(bf16[256,512]{1,0:T(8,128)(2,1)S(1)} %get-tuple-element.86), channel_id=1, source_target_pairs={{0,16},{16,32},{32,48},{48,0},{1,17},{17,33},{33,49},{49,1},{2,18}... | collective-permute-start | bytes 786440 | tf_op jit(solution)/shard_map/ppermute | solution.py:20
  170.1 10.3 %collective-permute-start.8 = (bf16[256,128]{1,0:T(8,128)(2,1)S(1)}, bf16[256,128]{1,0:T(8,128)(2,1)S(1)}, u32[]{:S(2)}, u32[]{:S(2)}) collective-permute-start(bf16[256,128]{1,0:T(8,128)(2,1)S(1)} %select_convert_fusion), channel_id=1, source_target_pairs={{0,1},{1,0},{2,3},{3,2},{4,5},{5,4},{6,7},{7,6},{8,9},{9,8},{10,11... | collective-permute-start | bytes 196616 | tf_op jit(solution)/shard_map/ppermute | solution.py:20
  177.0 15.7 %all-to-all-start.5 = ((bf16[8,32,512]{2,1,0:T(8,128)(2,1)}), bf16[8,32,512]{2,1,0:T(8,128)(2,1)S(1)}, u32[]{:S(2)}, u32[]{:S(2)}) async-start(bf16[8,32,512]{2,1,0:T(8,128)(2,1)} %bitcast.37), calls=%async_computation.5 | async-start | bytes 524288 | tf_op jit(solution)/shard_map/all_to_all | solution.py:24

commit v3 on v0

--- a/solution.py
+++ b/solution.py
@@ -122,8 +122,9 @@
     mine = row_major((mine + shifted(row_major(theirs), "c", 1).astype(F32)).astype(BF16))
     own, left, right, far = (mine[src // 2 * k : src // 2 * (k + 1)] for k in range(nx))
     own = own.astype(F32)
-    for block, by in ((far, 2), (right, 1), (left, -1)):
-        own = own + shifted(block, "x", by).astype(F32)
+    moved = [shifted(block, "x", by) for block, by in ((far, 2), (right, 1), (left, -1))]
+    for block in moved:
+        own = own + block.astype(F32)
     mine = own.astype(BF16)
 
     def by_core(mine, theirs):
@@ -136,7 +137,6 @@
     extra = jnp.stack([high, squares - high]).astype(BF16)
     piece = jnp.concatenate([part_t, extra, jnp.zeros((6, nx * rows), BF16)], axis=0)
     every = told_all(piece, "y").reshape(HEADS // 2, part + 8, nx * rows)
-    every, mine = lax.optimization_barrier((every, mine))
     grad_t = every[:, :part].reshape(HEADS // 2 * part, nx * rows)
     squares_all = every[:, part : part + 2].astype(F32).sum(axis=(0, 1))
     inverse = lax.rsqrt(squares_all / WIDTH + EPS)

time: 202 us -> 205 us (1.015)
  the two profiles are of different devices: /device:TPU:3 before, /device:TPU:64 now
where the time goes in v3:
time: 205 us; the launch traced here: 204 us
  starting transfers between devices  79.8 us (39%)
  waiting for transfers between devices  55.4 us (27%)
  local copies, waits for them, and re-layouts  41.1 us (20%)
  matrix products  14.8 us (7%)
  other arithmetic  10.9 us (5%)
    all_to_all x6, starting transfers between devices, exchanged(): return lax.all_to_all(value, axis, split_axis=0, concat_axis=0, tiled=True)  42.9 us
    all_to_all x6, waiting for transfers between devices, exchanged(): return lax.all_to_all(value, axis, split_axis=0, concat_axis=0, tiled=True)  42.5 us
    ppermute x12, starting transfers between devices, shifted(): return lax.ppermute(value, axis, [(i, (i + by) % n) for i in range(n)])  36.9 us
    unnamed x64, local copies, waits for them, and re-layouts  24.3 us
    dot_general x7, matrix products, dot(): lax.dot_general(a, b, (((ca,), (cb,)), ((), ())), preferred_element_type=...  14.8 us
    ppermute x12, waiting for transfers between devices, shifted(): return lax.ppermute(value, axis, [(i, (i + by) % n) for i in range(n)])  12.9 us
  transfers between devices with their start and end apart: 18, of which 6 were waited for; matrix products, arithmetic and copies ran while one was open for 21% of the time, Pallas kernels for 0%

profile of v3, /device:TPU:64, one launch (start us, length us, event | category | flops | bytes accessed | tf_op | source)
XLA Modules:
  0.0 203.6 jit_solution(6290239913627623675)
XLA Ops:
  1.7 1.6 pad_maximum_fusion.1
  3.2 3.4 %collective-permute-start = (bf16[640,256]{1,0:T(8,128)(2,1)}, bf16[640,256]{1,0:T(8,128)(2,1)S(1)}, u32[]{:S(2)}, u32[]{:S(2)}) collective-permute-start(bf16[640,256]{1,0:T(8,128)(2,1)} %pad_maximum_fusion.1), channel_id=1, source_target_pairs={{0,16},{16,32},{32,48},{48,0},{1,17},{17,33},{33,49},{49,1},{2,18}... | collective-permute-start | bytes 983048 | tf_op jit(solution)/shard_map/ppermute | solution.py:20
  6.6 3.7 %collective-permute-start.1 = (bf16[640,256]{1,0:T(8,128)(2,1)}, bf16[640,256]{1,0:T(8,128)(2,1)S(1)}, u32[]{:S(2)}, u32[]{:S(2)}) collective-permute-start(bf16[640,256]{1,0:T(8,128)(2,1)} %pad_maximum_fusion.1), channel_id=1, source_target_pairs={{0,48},{16,0},{32,16},{48,32},{1,49},{17,1},{33,17},{49,33},{2,50}... | collective-permute-start | bytes 983048 | tf_op jit(solution)/shard_map/ppermute | solution.py:20
  10.3 3.7 %collective-permute-start.2 = (bf16[640,256]{1,0:T(8,128)(2,1)}, bf16[640,256]{1,0:T(8,128)(2,1)S(1)}, u32[]{:S(2)}, u32[]{:S(2)}) collective-permute-start(bf16[640,256]{1,0:T(8,128)(2,1)} %pad_maximum_fusion.1), channel_id=1, source_target_pairs={{0,32},{16,48},{32,0},{48,16},{1,33},{17,49},{33,1},{49,17},{2,34}... | collective-permute-start | bytes 983048 | tf_op jit(solution)/shard_map/ppermute | solution.py:20
  14.0 3.3 %copy.188 = bf16[256,4096]{0,1:T(8,128)(2,1)S(1)} copy(bf16[256,4096]{1,0:T(8,128)(2,1)} %param.10) | data formatting | bytes 4194304 | tf_op args[2]
  20.0 4.4 %collective-permute-done.1 = bf16[640,256]{1,0:T(8,128)(2,1)S(1)} collective-permute-done((bf16[640,256]{1,0:T(8,128)(2,1)}, bf16[640,256]{1,0:T(8,128)(2,1)S(1)}, u32[]{:S(2)}, u32[]{:S(2)}) %collective-permute-start.1) | collective-permute-done | bytes 327712 | tf_op jit(solution)/shard_map/ppermute | solution.py:20
  27.9 1.9 collective-permute-start.3
  30.2 1.1 broadcast_in_dim.20
  31.3 10.0 %all-to-all-start = ((bf16[8,136,512]{2,1,0:T(8,128)(2,1)}), bf16[8,136,512]{2,1,0:T(8,128)(2,1)S(1)}, u32[]{:S(2)}, u32[]{:S(2)}) async-start(bf16[8,136,512]{2,1,0:T(8,128)(2,1)} %broadcast_in_dim.20), calls=%async_computation | async-start | bytes 2228224 | tf_op jit(solution)/shard_map/all_to_all | solution.py:24
  42.5 1.6 slice_dynamic-update-slice_fusion.9
  44.2 1.6 slice_dynamic-update-slice_fusion.8
  47.7 1.7 slice_dynamic-update-slice_fusion.6
  49.4 1.6 slice_dynamic-update-slice_fusion.5
  51.0 1.6 slice_dynamic-update-slice_fusion.4
  52.6 1.8 slice_dynamic-update-slice_fusion.3
  54.5 16.2 %all-to-all-done = bf16[8,136,512]{2,1,0:T(8,128)(2,1)S(1)} async-done(((bf16[8,136,512]{2,1,0:T(8,128)(2,1)}), bf16[8,136,512]{2,1,0:T(8,128)(2,1)S(1)}, u32[]{:S(2)}, u32[]{:S(2)}) %all-to-all-start) | async-done | bytes 1114144 | tf_op jit(solution)/shard_map/all_to_all | solution.py:24
  70.8 1.3 multiply_reduce_fusion
  72.1 1.4 fusion.1
  73.5 1.8 copy-done
  76.0 4.8 %all-to-all-start.1 = ((f32[8,16,128]{2,1,0:T(8,128)}), f32[8,16,128]{2,1,0:T(8,128)S(1)}, u32[]{:S(2)}, u32[]{:S(2)}) async-start(f32[8,16,128]{2,1,0:T(8,128)} %broadcast_in_dim.21), calls=%async_computation.1 | async-start | bytes 131072 | tf_op jit(solution)/shard_map/all_to_all | solution.py:24
  80.7 5.0 %multiply_convert_fusion = bf16[2048,1024]{1,0:T(8,128)(2,1)S(1)} fusion(f32[2048,1024]{1,0:T(8,128)} %copy-done, bf16[2048,256]{1,0:T(8,128)(2,1)} %get-tuple-element.58, bf16[1024,256]{1,0:T(8,128)(2,1)S(1)} %bitcast.108, f32[1024]{0:T(1024)S(1)} %bitcast.122, f32[1024]{0:T(1024)S(1)} %get-tuple-element.93), kind=kOutput, calls=%fused_computation | convolution fusion | flops 1086324736 | bytes 14163968 | tf_op jit(solution)/shard_map/dot_general | solution.py:33
  85.7 2.0 copy-done.19
  87.7 1.3 fusion.20
  89.2 1.3 multiply_convert_fusion.1
  91.7 10.4 %all-to-all-start.2 = ((bf16[32,64,128]{2,1,0:T(8,128)(2,1)}), bf16[32,64,128]{2,1,0:T(8,128)(2,1)S(1)}, u32[]{:S(2)}, u32[]{:S(2)}) async-start(bf16[32,64,128]{2,1,0:T(8,128)(2,1)} %bitcast.17), calls=%async_computation.2 | async-start | bytes 1048576 | tf_op jit(solution)/shard_map/all_to_all | solution.py:24
  102.1 5.1 %fusion.2 = f32[2048,256]{1,0:T(8,128)S(1)} fusion(bf16[1024,256]{1,0:T(8,128)(2,1)S(1)} %copy-done.10, f32[2048,1024]{1,0:T(8,128)} %copy-done, f32[1024]{0:T(1024)S(1)} %get-tuple-element.93), kind=kOutput, calls=%fused_computation.5 | convolution fusion | flops 1080033280 | bytes 11014144 | tf_op jit(solution)/shard_map/dot_general | solution.py:33
  107.3 1.3 fusion.22
  108.6 1.3 copy-done.2
  110.0 1.1 pad_maximum_fusion
  111.1 2.0 %collective-permute-start.8 = (bf16[1024,512]{1,0:T(8,128)(2,1)}, bf16[1024,512]{1,0:T(8,128)(2,1)}, u32[]{:S(2)}, u32[]{:S(2)}) collective-permute-start(bf16[1024,512]{1,0:T(8,128)(2,1)} %pad_maximum_fusion), channel_id=1, source_target_pairs={{0,1},{1,0},{2,3},{3,2},{4,5},{5,4},{6,7},{7,6},{8,9},{9,8},{10,11... | collective-permute-start | bytes 3145736 | tf_op jit(solution)/shard_map/ppermute | solution.py:20
  113.1 6.1 %all-to-all-done.2 = bf16[32,64,128]{2,1,0:T(8,128)(2,1)S(1)} async-done(((bf16[32,64,128]{2,1,0:T(8,128)(2,1)}), bf16[32,64,128]{2,1,0:T(8,128)(2,1)S(1)}, u32[]{:S(2)}, u32[]{:S(2)}) %all-to-all-start.2) | async-done | bytes 524320 | tf_op jit(solution)/shard_map/all_to_all | solution.py:24
  120.3 7.1 %all-to-all-start.3 = ((bf16[8,72,512]{2,1,0:T(8,128)(2,1)}), bf16[8,72,512]{2,1,0:T(8,128)(2,1)}, u32[]{:S(2)}, u32[]{:S(2)}) async-start(bf16[8,72,512]{2,1,0:T(8,128)(2,1)} %broadcast_in_dim.46), calls=%async_computation.3 | async-start | bytes 1179648 | tf_op jit(solution)/shard_map/all_to_all | solution.py:24
  127.8 1.1 copy.195
  128.9 1.2 slice-done.1
  130.4 1.5 fusion.6
  131.9 11.9 %all-to-all-done.3 = bf16[8,72,512]{2,1,0:T(8,128)(2,1)} async-done(((bf16[8,72,512]{2,1,0:T(8,128)(2,1)}), bf16[8,72,512]{2,1,0:T(8,128)(2,1)}, u32[]{:S(2)}, u32[]{:S(2)}) %all-to-all-start.3) | async-done | bytes 589856 | tf_op jit(solution)/shard_map/all_to_all | solution.py:24
  145.1 1.1 slice.262
  147.6 7.3 %all-to-all-start.4 = ((bf16[64,8,512]{2,1,0:T(8,128)(2,1)}), bf16[64,8,512]{2,1,0:T(8,128)(2,1)S(1)}, u32[]{:S(2)}, u32[]{:S(2)}) async-start(bf16[64,8,512]{2,1,0:T(8,128)(2,1)} %bitcast.31), calls=%async_computation.4 | async-start | bytes 1048576 | tf_op jit(solution)/shard_map/all_to_all | solution.py:24
  155.5 4.9 %collective-permute-start.6 = (bf16[512,128]{1,0:T(8,128)(2,1)S(1)}, bf16[512,128]{1,0:T(8,128)(2,1)S(1)}, u32[]{:S(2)}, u32[]{:S(2)}) collective-permute-start(bf16[512,128]{1,0:T(8,128)(2,1)S(1)} %get-tuple-element.74), channel_id=1, source_target_pairs={{0,32},{16,48},{32,0},{48,16},{1,33},{17,49},{33,1},{49,17},{2,34}... | collective-permute-start | bytes 393224 | tf_op jit(solution)/shard_map/ppermute | solution.py:20
  160.3 3.1 %collective-permute-start.5 = (bf16[512,128]{1,0:T(8,128)(2,1)S(1)}, bf16[512,128]{1,0:T(8,128)(2,1)S(1)}, u32[]{:S(2)}, u32[]{:S(2)}) collective-permute-start(bf16[512,128]{1,0:T(8,128)(2,1)S(1)} %get-tuple-element.75), channel_id=1, source_target_pairs={{0,48},{16,0},{32,16},{48,32},{1,49},{17,1},{33,17},{49,33},{2,50}... | collective-permute-start | bytes 393224 | tf_op jit(solution)/shard_map/ppermute | solution.py:20
  163.4 2.8 %collective-permute-start.4 = (bf16[512,128]{1,0:T(8,128)(2,1)S(1)}, bf16[512,128]{1,0:T(8,128)(2,1)S(1)}, u32[]{:S(2)}, u32[]{:S(2)}) collective-permute-start(bf16[512,128]{1,0:T(8,128)(2,1)S(1)} %get-tuple-element.73), channel_id=1, source_target_pairs={{0,16},{16,32},{32,48},{48,0},{1,17},{17,33},{33,49},{49,1},{2,18}... | collective-permute-start | bytes 393224 | tf_op jit(solution)/shard_map/ppermute | solution.py:20
  166.3 4.3 %collective-permute-start.11 = (bf16[256,512]{1,0:T(8,128)(2,1)S(1)}, bf16[256,512]{1,0:T(8,128)(2,1)S(1)}, u32[]{:S(2)}, u32[]{:S(2)}) collective-permute-start(bf16[256,512]{1,0:T(8,128)(2,1)S(1)} %get-tuple-element.72), channel_id=1, source_target_pairs={{0,48},{16,0},{32,16},{48,32},{1,49},{17,1},{33,17},{49,33},{2,50}... | collective-permute-start | bytes 786440 | tf_op jit(solution)/shard_map/ppermute | solution.py:20
  170.6 1.9 collective-permute-start.10
  172.5 3.4 %collective-permute-start.9 = (bf16[256,512]{1,0:T(8,128)(2,1)S(1)}, bf16[256,512]{1,0:T(8,128)(2,1)S(1)}, u32[]{:S(2)}, u32[]{:S(2)}) collective-permute-start(bf16[256,512]{1,0:T(8,128)(2,1)S(1)} %get-tuple-element.70), channel_id=1, source_target_pairs={{0,32},{16,48},{32,0},{48,16},{1,33},{17,49},{33,1},{49,17},{2,34}... | collective-permute-start | bytes 786440 | tf_op jit(solution)/shard_map/ppermute | solution.py:20
  176.0 1.9 collective-permute-start.7
  177.9 8.6 %collective-permute-done.10 = bf16[256,512]{1,0:T(8,128)(2,1)S(1)} collective-permute-done((bf16[256,512]{1,0:T(8,128)(2,1)S(1)}, bf16[256,512]{1,0:T(8,128)(2,1)S(1)}, u32[]{:S(2)}, u32[]{:S(2)}) %collective-permute-start.10) | collective-permute-done | bytes 262176 | tf_op jit(solution)/shard_map/ppermute | solution.py:20
  187.3 3.4 %all-to-all-start.5 = ((bf16[8,32,512]{2,1,0:T(8,128)(2,1)}), bf16[8,32,512]{2,1,0:T(8,128)(2,1)S(1)}, u32[]{:S(2)}, u32[]{:S(2)}) async-start(bf16[8,32,512]{2,1,0:T(8,128)(2,1)} %bitcast.37), calls=%async_computation.5 | async-start | bytes 524288 | tf_op jit(solution)/shard_map/all_to_all | solution.py:24
  192.9 8.3 %all-to-all-done.5 = bf16[8,32,512]{2,1,0:T(8,128)(2,1)S(1)} async-done(((bf16[8,32,512]{2,1,0:T(8,128)(2,1)}), bf16[8,32,512]{2,1,0:T(8,128)(2,1)S(1)}, u32[]{:S(2)}, u32[]{:S(2)}) %all-to-all-start.5) | async-done | bytes 262176 | tf_op jit(solution)/shard_map/all_to_all | solution.py:24
  (139 shorter events, 23.2 us)
Async XLA Ops:
  3.2 16.0 %collective-permute-start = (bf16[640,256]{1,0:T(8,128)(2,1)}, bf16[640,256]{1,0:T(8,128)(2,1)S(1)}, u32[]{:S(2)}, u32[]{:S(2)}) collective-permute-start(bf16[640,256]{1,0:T(8,128)(2,1)} %pad_maximum_fusion.1), channel_id=1, source_target_pairs={{0,16},{16,32},{32,48},{48,0},{1,17},{17,33},{33,49},{49,1},{2,18}... | collective-permute-start | bytes 983048 | tf_op jit(solution)/shard_map/ppermute | solution.py:20
  6.6 17.7 %collective-permute-start.1 = (bf16[640,256]{1,0:T(8,128)(2,1)}, bf16[640,256]{1,0:T(8,128)(2,1)S(1)}, u32[]{:S(2)}, u32[]{:S(2)}) collective-permute-start(bf16[640,256]{1,0:T(8,128)(2,1)} %pad_maximum_fusion.1), channel_id=1, source_target_pairs={{0,48},{16,0},{32,16},{48,32},{1,49},{17,1},{33,17},{49,33},{2,50}... | collective-permute-start | bytes 983048 | tf_op jit(solution)/shard_map/ppermute | solution.py:20
  10.3 14.8 %collective-permute-start.2 = (bf16[640,256]{1,0:T(8,128)(2,1)}, bf16[640,256]{1,0:T(8,128)(2,1)S(1)}, u32[]{:S(2)}, u32[]{:S(2)}) collective-permute-start(bf16[640,256]{1,0:T(8,128)(2,1)} %pad_maximum_fusion.1), channel_id=1, source_target_pairs={{0,32},{16,48},{32,0},{48,16},{1,33},{17,49},{33,1},{49,17},{2,34}... | collective-permute-start | bytes 983048 | tf_op jit(solution)/shard_map/ppermute | solution.py:20
  17.3 1.8 copy-start.13
  18.2 11.6 %copy-start.14 = (bf16[128,256]{1,0:T(8,128)(2,1)S(1)}, bf16[128,256]{1,0:T(8,128)(2,1)}, u32[]{:S(2)}) copy-start(bf16[128,256]{1,0:T(8,128)(2,1)} %param.15) | copy-start | bytes 196612
  18.2 11.6 %copy-start.15 = (bf16[128,256]{1,0:T(8,128)(2,1)S(1)}, bf16[128,256]{1,0:T(8,128)(2,1)}, u32[]{:S(2)}) copy-start(bf16[128,256]{1,0:T(8,128)(2,1)} %param.14) | copy-start | bytes 196612
  18.4 11.8 %copy-start.16 = (bf16[128,256]{1,0:T(8,128)(2,1)S(1)}, bf16[128,256]{1,0:T(8,128)(2,1)}, u32[]{:S(2)}) copy-start(bf16[128,256]{1,0:T(8,128)(2,1)} %param.11) | copy-start | bytes 196612
  19.2 12.1 %copy-start.7 = (bf16[640,256]{1,0:T(8,128)(2,1)}, bf16[640,256]{1,0:T(8,128)(2,1)S(1)}, u32[]{:S(2)}) copy-start(bf16[640,256]{1,0:T(8,128)(2,1)S(1)} %collective-permute-done) | copy-start | bytes 983044
  24.3 7.0 %copy-start.6 = (bf16[640,256]{1,0:T(8,128)(2,1)}, bf16[640,256]{1,0:T(8,128)(2,1)S(1)}, u32[]{:S(2)}) copy-start(bf16[640,256]{1,0:T(8,128)(2,1)S(1)} %collective-permute-done.1) | copy-start | bytes 983044
  27.9 18.5 %collective-permute-start.3 = (bf16[3072,256]{1,0:T(8,128)(2,1)}, bf16[3072,256]{1,0:T(8,128)(2,1)}, u32[]{:S(2)}, u32[]{:S(2)}) collective-permute-start(bf16[3072,256]{1,0:T(8,128)(2,1)} %constant_dynamic-update-slice_fusion), channel_id=1, source_target_pairs={{0,1},{1,0},{2,3},{3,2},{4,5},{5,4},{6,7},{7,6},{8,9},{9,8},{10,11... | collective-permute-start | bytes 4718600 | tf_op jit(solution)/shard_map/ppermute | solution.py:20
  31.3 39.3 %all-to-all-start = ((bf16[8,136,512]{2,1,0:T(8,128)(2,1)}), bf16[8,136,512]{2,1,0:T(8,128)(2,1)S(1)}, u32[]{:S(2)}, u32[]{:S(2)}) async-start(bf16[8,136,512]{2,1,0:T(8,128)(2,1)} %broadcast_in_dim.20), calls=%async_computation | async-start | bytes 2228224 | tf_op jit(solution)/shard_map/all_to_all | solution.py:24
  47.5 23.2 %copy-start.3 = (bf16[1,256,512]{1,2,0:T(8,128)(2,1)}, bf16[1,256,512]{1,2,0:T(8,128)(2,1)S(1)}, u32[]{:S(2)}) copy-start(bf16[1,256,512]{1,2,0:T(8,128)(2,1)S(1)} %slice_bitcast_fusion) | copy-start | bytes 786436
  72.1 3.3 %copy-start = (f32[2048,1024]{1,0:T(8,128)}, f32[2048,1024]{1,0:T(8,128)S(1)}, u32[]{:S(2)}) copy-start(f32[2048,1024]{1,0:T(8,128)S(1)} %get-tuple-element.94) | copy-start | bytes 25165828
  76.0 13.0 %all-to-all-start.1 = ((f32[8,16,128]{2,1,0:T(8,128)}), f32[8,16,128]{2,1,0:T(8,128)S(1)}, u32[]{:S(2)}, u32[]{:S(2)}) async-start(f32[8,16,128]{2,1,0:T(8,128)} %broadcast_in_dim.21), calls=%async_computation.1 | async-start | bytes 131072 | tf_op jit(solution)/shard_map/all_to_all | solution.py:24
  85.7 2.0 copy-start.19
  90.6 11.5 %copy-start.10 = (bf16[1024,256]{1,0:T(8,128)(2,1)S(1)}, bf16[1024,256]{1,0:T(8,128)(2,1)}, u32[]{:S(2)}) copy-start(bf16[1024,256]{1,0:T(8,128)(2,1)} %get-tuple-element.14) | copy-start | bytes 1572868
  91.7 27.5 %all-to-all-start.2 = ((bf16[32,64,128]{2,1,0:T(8,128)(2,1)}), bf16[32,64,128]{2,1,0:T(8,128)(2,1)S(1)}, u32[]{:S(2)}, u32[]{:S(2)}) async-start(bf16[32,64,128]{2,1,0:T(8,128)(2,1)} %bitcast.17), calls=%async_computation.2 | async-start | bytes 1048576 | tf_op jit(solution)/shard_map/all_to_all | solution.py:24
  102.1 5.2 %copy-start.9 = (bf16[1024,256]{1,0:T(8,128)(2,1)S(1)}, bf16[1024,256]{1,0:T(8,128)(2,1)}, u32[]{:S(2)}) copy-start(bf16[1024,256]{1,0:T(8,128)(2,1)} %get-tuple-element.13) | copy-start | bytes 1572868
  102.1 5.2 %copy-start.20 = (bf16[2048,1024]{1,0:T(8,128)(2,1)S(1)}, bf16[2048,1024]{1,0:T(8,128)(2,1)}, u32[]{:S(2)}) copy-start(bf16[2048,1024]{1,0:T(8,128)(2,1)} %copy-done.19) | copy-start | bytes 12582916
  107.2 21.7 %copy-start.1 = (f32[2048,256]{1,0:T(8,128)}, f32[2048,256]{1,0:T(8,128)S(1)}, u32[]{:S(2)}) copy-start(f32[2048,256]{1,0:T(8,128)S(1)} %fusion.2) | copy-start | bytes 6291460
  108.6 1.3 copy-start.2
  109.9 9.4 %copy-start.17 = (bf16[72]{0:T(256)(128)(2,1)S(1)}, bf16[72]{0:T(256)(128)(2,1)}, u32[]{:S(2)}) copy-start(bf16[72]{0:T(256)(128)(2,1)} %pad.7.clone) | copy-start | bytes 436
  109.9 17.4 %copy-start.18 = (f32[256]{0:T(256)S(1)}, f32[256]{0:T(256)}, u32[]{:S(2)}) copy-start(f32[256]{0:T(256)} %param.9) | copy-start | bytes 3076
  110.0 17.6 %copy-start.11 = (bf16[256,256]{1,0:T(8,128)(2,1)S(1)}, bf16[256,256]{1,0:T(8,128)(2,1)}, u32[]{:S(2)}) copy-start(bf16[256,256]{1,0:T(8,128)(2,1)} %get-tuple-element.59) | copy-start | bytes 393220
  111.0 16.4 %copy-start.12 = (bf16[256,256]{1,0:T(8,128)(2,1)S(1)}, bf16[256,256]{1,0:T(8,128)(2,1)}, u32[]{:S(2)}) copy-start(bf16[256,256]{1,0:T(8,128)(2,1)} %get-tuple-element.61) | copy-start | bytes 393220
  111.0 16.6 %copy-start.8 = (bf16[256,8,1,1,64]{0,4,3,2,1:T(8,128)(2,1)S(1)}, bf16[256,8,1,1,64]{0,4,3,2,1:T(8,128)(2,1)}, u32[]{:S(2)}) copy-start(bf16[256,8,1,1,64]{0,4,3,2,1:T(8,128)(2,1)} %get-tuple-element.56) | copy-start | bytes 786436
  111.1 17.8 %collective-permute-start.8 = (bf16[1024,512]{1,0:T(8,128)(2,1)}, bf16[1024,512]{1,0:T(8,128)(2,1)}, u32[]{:S(2)}, u32[]{:S(2)}) collective-permute-start(bf16[1024,512]{1,0:T(8,128)(2,1)} %pad_maximum_fusion), channel_id=1, source_target_pairs={{0,1},{1,0},{2,3},{3,2},{4,5},{5,4},{6,7},{7,6},{8,9},{9,8},{10,11... | collective-permute-start | bytes 3145736 | tf_op jit(solution)/shard_map/ppermute | solution.py:20
  120.3 23.6 %all-to-all-start.3 = ((bf16[8,72,512]{2,1,0:T(8,128)(2,1)}), bf16[8,72,512]{2,1,0:T(8,128)(2,1)}, u32[]{:S(2)}, u32[]{:S(2)}) async-start(bf16[8,72,512]{2,1,0:T(8,128)(2,1)} %broadcast_in_dim.46), calls=%async_computation.3 | async-start | bytes 1179648 | tf_op jit(solution)/shard_map/all_to_all | solution.py:24
  128.8 1.2 slice-start.1
  128.9 1.5 slice-start
  128.9 15.9 %copy-start.4 = (bf16[1,256,512]{1,2,0:T(8,128)(2,1)S(1)}, bf16[1,256,512]{1,2,0:T(8,128)(2,1)}, u32[]{:S(2)}) copy-start(bf16[1,256,512]{1,2,0:T(8,128)(2,1)} %copy-done.3) | copy-start | bytes 786436
  146.2 8.7 %copy-start.5 = (bf16[2,256,512]{2,1,0:T(8,128)(2,1)S(1)}, bf16[2,256,512]{2,1,0:T(8,128)(2,1)}, u32[]{:S(2)}) copy-start(bf16[2,256,512]{2,1,0:T(8,128)(2,1)} %copy.195) | copy-start | bytes 1572868
  147.6 39.8 %all-to-all-start.4 = ((bf16[64,8,512]{2,1,0:T(8,128)(2,1)}), bf16[64,8,512]{2,1,0:T(8,128)(2,1)S(1)}, u32[]{:S(2)}, u32[]{:S(2)}) async-start(bf16[64,8,512]{2,1,0:T(8,128)(2,1)} %bitcast.31), calls=%async_computation.4 | async-start | bytes 1048576 | tf_op jit(solution)/shard_map/all_to_all | solution.py:24
  155.5 17.0 %collective-permute-start.6 = (bf16[512,128]{1,0:T(8,128)(2,1)S(1)}, bf16[512,128]{1,0:T(8,128)(2,1)S(1)}, u32[]{:S(2)}, u32[]{:S(2)}) collective-permute-start(bf16[512,128]{1,0:T(8,128)(2,1)S(1)} %get-tuple-element.74), channel_id=1, source_target_pairs={{0,32},{16,48},{32,0},{48,16},{1,33},{17,49},{33,1},{49,17},{2,34}... | collective-permute-start | bytes 393224 | tf_op jit(solution)/shard_map/ppermute | solution.py:20
  160.3 15.5 %collective-permute-start.5 = (bf16[512,128]{1,0:T(8,128)(2,1)S(1)}, bf16[512,128]{1,0:T(8,128)(2,1)S(1)}, u32[]{:S(2)}, u32[]{:S(2)}) collective-permute-start(bf16[512,128]{1,0:T(8,128)(2,1)S(1)} %get-tuple-element.75), channel_id=1, source_target_pairs={{0,48},{16,0},{32,16},{48,32},{1,49},{17,1},{33,17},{49,33},{2,50}... | collective-permute-start | bytes 393224 | tf_op jit(solution)/shard_map/ppermute | solution.py:20
  163.4 12.5 %collective-permute-start.4 = (bf16[512,128]{1,0:T(8,128)(2,1)S(1)}, bf16[512,128]{1,0:T(8,128)(2,1)S(1)}, u32[]{:S(2)}, u32[]{:S(2)}) collective-permute-start(bf16[512,128]{1,0:T(8,128)(2,1)S(1)} %get-tuple-element.73), channel_id=1, source_target_pairs={{0,16},{16,32},{32,48},{48,0},{1,17},{17,33},{33,49},{49,1},{2,18}... | collective-permute-start | bytes 393224 | tf_op jit(solution)/shard_map/ppermute | solution.py:20
  166.3 11.7 %collective-permute-start.11 = (bf16[256,512]{1,0:T(8,128)(2,1)S(1)}, bf16[256,512]{1,0:T(8,128)(2,1)S(1)}, u32[]{:S(2)}, u32[]{:S(2)}) collective-permute-start(bf16[256,512]{1,0:T(8,128)(2,1)S(1)} %get-tuple-element.72), channel_id=1, source_target_pairs={{0,48},{16,0},{32,16},{48,32},{1,49},{17,1},{33,17},{49,33},{2,50}... | collective-permute-start | bytes 786440 | tf_op jit(solution)/shard_map/ppermute | solution.py:20
  170.6 15.9 %collective-permute-start.10 = (bf16[256,512]{1,0:T(8,128)(2,1)S(1)}, bf16[256,512]{1,0:T(8,128)(2,1)S(1)}, u32[]{:S(2)}, u32[]{:S(2)}) collective-permute-start(bf16[256,512]{1,0:T(8,128)(2,1)S(1)} %get-tuple-element.71), channel_id=1, source_target_pairs={{0,16},{16,32},{32,48},{48,0},{1,17},{17,33},{33,49},{49,1},{2,18}... | collective-permute-start | bytes 786440 | tf_op jit(solution)/shard_map/ppermute | solution.py:20
  172.5 14.0 %collective-permute-start.9 = (bf16[256,512]{1,0:T(8,128)(2,1)S(1)}, bf16[256,512]{1,0:T(8,128)(2,1)S(1)}, u32[]{:S(2)}, u32[]{:S(2)}) collective-permute-start(bf16[256,512]{1,0:T(8,128)(2,1)S(1)} %get-tuple-element.70), channel_id=1, source_target_pairs={{0,32},{16,48},{32,0},{48,16},{1,33},{17,49},{33,1},{49,17},{2,34}... | collective-permute-start | bytes 786440 | tf_op jit(solution)/shard_map/ppermute | solution.py:20
  176.0 14.8 %collective-permute-start.7 = (bf16[256,128]{1,0:T(8,128)(2,1)S(1)}, bf16[256,128]{1,0:T(8,128)(2,1)S(1)}, u32[]{:S(2)}, u32[]{:S(2)}) collective-permute-start(bf16[256,128]{1,0:T(8,128)(2,1)S(1)} %select_convert_fusion), channel_id=1, source_target_pairs={{0,1},{1,0},{2,3},{3,2},{4,5},{5,4},{6,7},{7,6},{8,9},{9,8},{10,11... | collective-permute-start | bytes 196616 | tf_op jit(solution)/shard_map/ppermute | solution.py:20
  187.3 13.8 %all-to-all-start.5 = ((bf16[8,32,512]{2,1,0:T(8,128)(2,1)}), bf16[8,32,512]{2,1,0:T(8,128)(2,1)S(1)}, u32[]{:S(2)}, u32[]{:S(2)}) async-start(bf16[8,32,512]{2,1,0:T(8,128)(2,1)} %bitcast.37), calls=%async_computation.5 | async-start | bytes 524288 | tf_op jit(solution)/shard_map/all_to_all | solution.py:24

commit v4 on v3

--- a/solution.py
+++ b/solution.py
@@ -72,21 +72,12 @@
     for block, off in zip(blocks, (0, 3, 1, 2)):
         target_all = lax.dynamic_update_slice(target_all, block[src:], (lax.rem(x_at + off, nx) * rows, 0))
 
-    w_parts = lax.dynamic_slice(
-        w_query.reshape(cols, HEADS // 2, 2, nx, part), (0, 0, 0, x_at, 0), (cols, HEADS // 2, 2, 1, part)
-    )
-    w_even = w_parts[:, :, 0].reshape(cols, -1)
-    w_odd = w_parts[:, :, 1].reshape(cols, -1)
-    w_mine = jnp.where(core == 0, w_even, w_odd)
-    w_theirs = jnp.where(core == 0, w_odd, w_even)
-    swap = [b[:src] for b in blocks] + [target_all, w_theirs[:, :cols], w_theirs[:, cols:]]
+    swap = [b[:src] for b in blocks] + [target_all]
     swap = shifted(row_major(jnp.concatenate(swap, axis=0)), "c", 1)
     blocks = [b[:src] for b in blocks] + [swap[src * k : src * (k + 1)] for k in range(nx)]
     key_all = row_major(jnp.concatenate([b[: src // 2] for b in blocks], axis=0))
     value_all = row_major(jnp.concatenate([b[src // 2 :] for b in blocks], axis=0))
-    target_other = swap[nx * src : nx * src + nx * rows]
-    w_other = swap[nx * src + nx * rows :]
-    w_other = jnp.concatenate([w_other[:cols], w_other[cols:]], axis=1)
+    target_other = swap[nx * src :]
 
     both = both.reshape(nz, rows + 8, 2 * cols)
     query_all = both[:, :rows, :cols].reshape(n_rows, cols)
@@ -131,7 +122,6 @@
         return jnp.where(core == 0, jnp.stack([mine, theirs]), jnp.stack([theirs, mine]))
 
     target_both = by_core(target_all.T, target_other.T).astype(F32)
-    w_both = by_core(w_mine, w_other).reshape(2 * cols, -1)
     squares = jnp.sum(target_both * target_both, axis=(0, 1))
     high = lax.reduce_precision(squares, 8, 7)
     extra = jnp.stack([high, squares - high]).astype(BF16)
@@ -151,8 +141,17 @@
     weight_sum = lax.optimization_barrier(weight_sum).reshape(nx, 2, 8, HEADS // 2, part)
     grad_weight = weight_sum.transpose(2, 3, 1, 0, 4).reshape(8, WIDTH)
 
+    w_late, _ = lax.optimization_barrier((w_query, sent))
+    w_parts = lax.dynamic_slice(
+        w_late.reshape(cols, HEADS // 2, 2, nx, part), (0, 0, 0, x_at, 0), (cols, HEADS // 2, 2, 1, part)
+    )
+    w_even = w_parts[:, :, 0].reshape(cols, -1)
+    w_odd = w_parts[:, :, 1].reshape(cols, -1)
+    w_mine = jnp.where(core == 0, w_even, w_odd)
+    w_theirs = jnp.where(core == 0, w_odd, w_even)
     grad_t, _ = lax.optimization_barrier((grad_t, weight_sent))
-    rows_t = dot(w_both, grad_t, 1, 0)
+    grad_other = shifted(grad_t, "c", 1)
+    rows_t = dot(w_mine, grad_t, 1, 0) + dot(w_theirs, grad_other, 1, 0)
 
     def rows_at(off):
         return lax.dynamic_slice_in_dim(rows_t, lax.rem(x_at + off, nx) * rows, rows, 1)
@@ -160,9 +159,7 @@
     rows_sum = rows_at(0)
     for off, by in ((1, 1), (3, -1), (2, 2)):
         rows_sum = rows_sum + shifted(rows_at(off).astype(BF16), "x", by).astype(F32)
-    low, high = rows_sum[:cols], rows_sum[cols:]
-    rows_in = shifted(jnp.where(core == 0, high, low).astype(BF16), "c", 1)
-    grad_rows = (jnp.where(core == 0, low, high) + rows_in.astype(F32)).T.astype(BF16)
+    grad_rows = rows_sum.T.astype(BF16)
 
     mine, _ = lax.optimization_barrier((mine, weight_got))
     sums = exchanged(mine.reshape(ny, bit, 2 * HEAD_DIM), "y")

time: 205 us -> 201 us (0.980)
  the two profiles are of different devices: /device:TPU:64 before, /device:TPU:2 now
where the time goes in v4:
time: 201 us; the launch traced here: 200 us
  starting transfers between devices  83.8 us (42%)
  waiting for transfers between devices  51.7 us (26%)
  local copies, waits for them, and re-layouts  34.1 us (17%)
  matrix products  17.9 us (9%)
  other arithmetic  10.9 us (5%)
    all_to_all x6, waiting for transfers between devices, exchanged(): return lax.all_to_all(value, axis, split_axis=0, concat_axis=0, tiled=True)  43.7 us
    all_to_all x6, starting transfers between devices, exchanged(): return lax.all_to_all(value, axis, split_axis=0, concat_axis=0, tiled=True)  43.4 us
    ppermute x12, starting transfers between devices, shifted(): return lax.ppermute(value, axis, [(i, (i + by) % n) for i in range(n)])  40.4 us
    unnamed x39, local copies, waits for them, and re-layouts  19.2 us
    dot_general x8, matrix products, dot(): lax.dot_general(a, b, (((ca,), (cb,)), ((), ())), preferred_element_type=...  17.9 us
    ppermute x12, waiting for transfers between devices, shifted(): return lax.ppermute(value, axis, [(i, (i + by) % n) for i in range(n)])  7.96 us
  transfers between devices with their start and end apart: 18, of which 7 were waited for; matrix products, arithmetic and copies ran while one was open for 23% of the time, Pallas kernels for 0%

profile of v4, /device:TPU:2, one launch (start us, length us, event | category | flops | bytes accessed | tf_op | source)
XLA Modules:
  0.0 199.8 jit_solution(5405812083062219763)
XLA Ops:
  0.7 1.0 constant_dynamic-slice_fusion
  2.6 3.4 %collective-permute-start = (bf16[640,256]{1,0:T(8,128)(2,1)S(1)}, bf16[640,256]{1,0:T(8,128)(2,1)S(1)}, u32[]{:S(2)}, u32[]{:S(2)}) collective-permute-start(bf16[640,256]{1,0:T(8,128)(2,1)S(1)} %pad_maximum_fusion.1), channel_id=1, source_target_pairs={{0,16},{16,32},{32,48},{48,0},{1,17},{17,33},{33,49},{49,1},{2,18}... | collective-permute-start | bytes 983048 | tf_op jit(solution)/shard_map/ppermute | solution.py:20
  6.0 8.4 %collective-permute-start.2 = (bf16[640,256]{1,0:T(8,128)(2,1)S(1)}, bf16[640,256]{1,0:T(8,128)(2,1)S(1)}, u32[]{:S(2)}, u32[]{:S(2)}) collective-permute-start(bf16[640,256]{1,0:T(8,128)(2,1)S(1)} %pad_maximum_fusion.1), channel_id=1, source_target_pairs={{0,32},{16,48},{32,0},{48,16},{1,33},{17,49},{33,1},{49,17},{2,34}... | collective-permute-start | bytes 983048 | tf_op jit(solution)/shard_map/ppermute | solution.py:20
  14.4 1.9 collective-permute-start.1
  17.1 1.0 multiply_reduce_fusion.1
  19.1 6.5 %collective-permute-done.1 = bf16[640,256]{1,0:T(8,128)(2,1)S(1)} collective-permute-done((bf16[640,256]{1,0:T(8,128)(2,1)S(1)}, bf16[640,256]{1,0:T(8,128)(2,1)S(1)}, u32[]{:S(2)}, u32[]{:S(2)}) %collective-permute-start.1) | collective-permute-done | bytes 327712 | tf_op jit(solution)/shard_map/ppermute | solution.py:20
  27.8 1.9 collective-permute-start.3
  30.0 1.1 broadcast_in_dim.20
  31.1 10.3 %all-to-all-start = ((bf16[8,136,512]{2,1,0:T(8,128)(2,1)}), bf16[8,136,512]{2,1,0:T(8,128)(2,1)S(1)}, u32[]{:S(2)}, u32[]{:S(2)}) async-start(bf16[8,136,512]{2,1,0:T(8,128)(2,1)} %broadcast_in_dim.20), calls=%async_computation | async-start | bytes 2228224 | tf_op jit(solution)/shard_map/all_to_all | solution.py:24
  42.1 1.6 slice_dynamic-update-slice_fusion.9
  43.7 1.6 slice_dynamic-update-slice_fusion.8
  46.0 1.6 slice_dynamic-update-slice_fusion.6
  47.7 1.6 slice_dynamic-update-slice_fusion.5
  49.3 1.6 slice_dynamic-update-slice_fusion.4
  50.9 1.6 slice_dynamic-update-slice_fusion.3
  52.6 19.6 %all-to-all-done = bf16[8,136,512]{2,1,0:T(8,128)(2,1)S(1)} async-done(((bf16[8,136,512]{2,1,0:T(8,128)(2,1)}), bf16[8,136,512]{2,1,0:T(8,128)(2,1)S(1)}, u32[]{:S(2)}, u32[]{:S(2)}) %all-to-all-start) | async-done | bytes 1114144 | tf_op jit(solution)/shard_map/all_to_all | solution.py:24
  72.4 1.3 multiply_reduce_fusion
  73.7 1.4 fusion.1
  75.1 1.8 copy-done
  77.6 3.4 %all-to-all-start.1 = ((f32[8,16,128]{2,1,0:T(8,128)}), f32[8,16,128]{2,1,0:T(8,128)S(1)}, u32[]{:S(2)}, u32[]{:S(2)}) async-start(f32[8,16,128]{2,1,0:T(8,128)} %broadcast_in_dim.21), calls=%async_computation.1 | async-start | bytes 131072 | tf_op jit(solution)/shard_map/all_to_all | solution.py:24
  80.9 5.0 %multiply_convert_fusion = bf16[2048,1024]{1,0:T(8,128)(2,1)S(1)} fusion(f32[2048,1024]{1,0:T(8,128)} %copy-done, bf16[2048,256]{1,0:T(8,128)(2,1)} %get-tuple-element.60, bf16[1024,256]{1,0:T(8,128)(2,1)S(1)} %bitcast.107, f32[1024]{0:T(1024)S(1)} %bitcast.121, f32[1024]{0:T(1024)S(1)} %get-tuple-element.91), kind=kOutput, calls=%fused_computation | convolution fusion | flops 1086324736 | bytes 14163968 | tf_op jit(solution)/shard_map/dot_general | solution.py:33
  85.9 2.0 copy-done.11
  87.9 1.3 fusion.19
  89.7 0.9 copy.148
  90.6 9.3 %all-to-all-start.2 = ((bf16[32,64,128]{2,1,0:T(8,128)(2,1)}), bf16[32,64,128]{2,1,0:T(8,128)(2,1)S(1)}, u32[]{:S(2)}, u32[]{:S(2)}) async-start(bf16[32,64,128]{2,1,0:T(8,128)(2,1)} %bitcast.12), calls=%async_computation.2 | async-start | bytes 1048576 | tf_op jit(solution)/shard_map/all_to_all | solution.py:24
  100.0 1.0 slice_bitcast_fusion
  101.2 1.3 multiply_convert_fusion.1
  102.5 14.2 %all-to-all-done.2 = bf16[32,64,128]{2,1,0:T(8,128)(2,1)S(1)} async-done(((bf16[32,64,128]{2,1,0:T(8,128)(2,1)}), bf16[32,64,128]{2,1,0:T(8,128)(2,1)S(1)}, u32[]{:S(2)}, u32[]{:S(2)}) %all-to-all-start.2) | async-done | bytes 524320 | tf_op jit(solution)/shard_map/all_to_all | solution.py:24
  116.9 0.9 broadcast_in_dim.46
  117.8 7.1 %all-to-all-start.3 = ((bf16[8,72,512]{2,1,0:T(8,128)(2,1)}), bf16[8,72,512]{2,1,0:T(8,128)(2,1)S(1)}, u32[]{:S(2)}, u32[]{:S(2)}) async-start(bf16[8,72,512]{2,1,0:T(8,128)(2,1)} %broadcast_in_dim.46), calls=%async_computation.3 | async-start | bytes 1179648 | tf_op jit(solution)/shard_map/all_to_all | solution.py:24
  124.9 3.6 %fusion.21 = f32[2048,256]{1,0:T(8,128)S(1)} fusion(bf16[2048,1024]{1,0:T(8,128)(2,1)} %copy-done.11, bf16[1024,256]{1,0:T(8,128)(2,1)} %get-tuple-element.15), kind=kOutput, calls=%fused_computation.93 | convolution fusion | flops 1073741824 | bytes 6815744 | tf_op jit(solution)/shard_map/dot_general | solution.py:33
  128.6 5.6 %fusion.2 = f32[2048,256]{1,0:T(8,128)S(1)} fusion(bf16[1024,256]{1,0:T(8,128)(2,1)S(1)} %copy-done.6, f32[2048,1024]{1,0:T(8,128)} %copy-done, f32[1024]{0:T(1024)S(1)} %get-tuple-element.91), kind=kOutput, calls=%fused_computation.5 | convolution fusion | flops 1080033280 | bytes 11014144 | tf_op jit(solution)/shard_map/dot_general | solution.py:33
  134.3 1.3 copy-done.2
  135.7 1.1 pad_maximum_fusion
  136.7 2.1 %collective-permute-start.8 = (bf16[1024,512]{1,0:T(8,128)(2,1)}, bf16[1024,512]{1,0:T(8,128)(2,1)}, u32[]{:S(2)}, u32[]{:S(2)}) collective-permute-start(bf16[1024,512]{1,0:T(8,128)(2,1)} %pad_maximum_fusion), channel_id=1, source_target_pairs={{0,1},{1,0},{2,3},{3,2},{4,5},{5,4},{6,7},{7,6},{8,9},{9,8},{10,11... | collective-permute-start | bytes 3145736 | tf_op jit(solution)/shard_map/ppermute | solution.py:20
  138.9 3.3 %copy.149 = bf16[256,4096]{0,1:T(8,128)(2,1)S(1)} copy(bf16[256,4096]{1,0:T(8,128)(2,1)} %param.10) | data formatting | bytes 4194304 | tf_op jit(solution)/shard_map/optimization_barrier | solution.py:144
  144.8 2.4 %collective-permute-start.4 = (bf16[512,512]{1,0:T(8,128)(2,1)S(1)}, bf16[512,512]{1,0:T(8,128)(2,1)S(1)}, u32[]{:S(2)}, u32[]{:S(2)}) collective-permute-start(bf16[512,512]{1,0:T(8,128)(2,1)S(1)} %bitcast.90), channel_id=1, source_target_pairs={{0,1},{1,0},{2,3},{3,2},{4,5},{5,4},{6,7},{7,6},{8,9},{9,8},{10,11... | collective-permute-start | bytes 1572872 | tf_op jit(solution)/shard_map/ppermute | solution.py:20
  147.3 1.5 fusion.6
  148.8 6.1 %all-to-all-start.4 = ((bf16[64,8,512]{2,1,0:T(8,128)(2,1)}), bf16[64,8,512]{2,1,0:T(8,128)(2,1)S(1)}, u32[]{:S(2)}, u32[]{:S(2)}) async-start(bf16[64,8,512]{2,1,0:T(8,128)(2,1)} %bitcast.29), calls=%async_computation.4 | async-start | bytes 1048576 | tf_op jit(solution)/shard_map/all_to_all | solution.py:24
  154.9 4.0 %collective-permute-start.9 = (bf16[256,512]{1,0:T(8,128)(2,1)S(1)}, bf16[256,512]{1,0:T(8,128)(2,1)S(1)}, u32[]{:S(2)}, u32[]{:S(2)}) collective-permute-start(bf16[256,512]{1,0:T(8,128)(2,1)S(1)} %get-tuple-element.70), channel_id=1, source_target_pairs={{0,32},{16,48},{32,0},{48,16},{1,33},{17,49},{33,1},{49,17},{2,34}... | collective-permute-start | bytes 786440 | tf_op jit(solution)/shard_map/ppermute | solution.py:20
  158.9 1.9 collective-permute-start.10
  160.8 3.9 %collective-permute-start.11 = (bf16[256,512]{1,0:T(8,128)(2,1)S(1)}, bf16[256,512]{1,0:T(8,128)(2,1)S(1)}, u32[]{:S(2)}, u32[]{:S(2)}) collective-permute-start(bf16[256,512]{1,0:T(8,128)(2,1)S(1)} %get-tuple-element.72), channel_id=1, source_target_pairs={{0,48},{16,0},{32,16},{48,32},{1,49},{17,1},{33,17},{49,33},{2,50}... | collective-permute-start | bytes 786440 | tf_op jit(solution)/shard_map/ppermute | solution.py:20
  165.5 1.9 collective-permute-start.5
  167.4 6.6 %collective-permute-start.7 = (bf16[256,128]{1,0:T(8,128)(2,1)S(1)}, bf16[256,128]{1,0:T(8,128)(2,1)S(1)}, u32[]{:S(2)}, u32[]{:S(2)}) collective-permute-start(bf16[256,128]{1,0:T(8,128)(2,1)S(1)} %get-tuple-element.74), channel_id=1, source_target_pairs={{0,32},{16,48},{32,0},{48,16},{1,33},{17,49},{33,1},{49,17},{2,34}... | collective-permute-start | bytes 196616 | tf_op jit(solution)/shard_map/ppermute | solution.py:20
  174.1 1.9 collective-permute-start.6
  178.2 7.2 %all-to-all-start.5 = ((bf16[8,32,512]{2,1,0:T(8,128)(2,1)}), bf16[8,32,512]{2,1,0:T(8,128)(2,1)S(1)}, u32[]{:S(2)}, u32[]{:S(2)}) async-start(bf16[8,32,512]{2,1,0:T(8,128)(2,1)} %bitcast.35), calls=%async_computation.5 | async-start | bytes 524288 | tf_op jit(solution)/shard_map/all_to_all | solution.py:24
  186.6 0.9 reshape.172
  187.5 9.8 %all-to-all-done.5 = bf16[8,32,512]{2,1,0:T(8,128)(2,1)S(1)} async-done(((bf16[8,32,512]{2,1,0:T(8,128)(2,1)}), bf16[8,32,512]{2,1,0:T(8,128)(2,1)S(1)}, u32[]{:S(2)}, u32[]{:S(2)}) %all-to-all-start.5) | async-done | bytes 262176 | tf_op jit(solution)/shard_map/all_to_all | solution.py:24
  (110 shorter events, 17.5 us)
Async XLA Ops:
  0.6 17.4 %copy-start.7 = (bf16[128,256]{1,0:T(8,128)(2,1)S(1)}, bf16[128,256]{1,0:T(8,128)(2,1)}, u32[]{:S(2)}) copy-start(bf16[128,256]{1,0:T(8,128)(2,1)} %param.8) | copy-start | bytes 196612
  1.7 28.2 %copy-start.8 = (bf16[128,256]{1,0:T(8,128)(2,1)S(1)}, bf16[128,256]{1,0:T(8,128)(2,1)}, u32[]{:S(2)}) copy-start(bf16[128,256]{1,0:T(8,128)(2,1)} %param.15) | copy-start | bytes 196612
  1.7 28.2 %copy-start.9 = (bf16[128,256]{1,0:T(8,128)(2,1)S(1)}, bf16[128,256]{1,0:T(8,128)(2,1)}, u32[]{:S(2)}) copy-start(bf16[128,256]{1,0:T(8,128)(2,1)} %param.11) | copy-start | bytes 196612
  2.6 15.7 %collective-permute-start = (bf16[640,256]{1,0:T(8,128)(2,1)S(1)}, bf16[640,256]{1,0:T(8,128)(2,1)S(1)}, u32[]{:S(2)}, u32[]{:S(2)}) collective-permute-start(bf16[640,256]{1,0:T(8,128)(2,1)S(1)} %pad_maximum_fusion.1), channel_id=1, source_target_pairs={{0,16},{16,32},{32,48},{48,0},{1,17},{17,33},{33,49},{49,1},{2,18}... | collective-permute-start | bytes 983048 | tf_op jit(solution)/shard_map/ppermute | solution.py:20
  6.0 20.4 %collective-permute-start.2 = (bf16[640,256]{1,0:T(8,128)(2,1)S(1)}, bf16[640,256]{1,0:T(8,128)(2,1)S(1)}, u32[]{:S(2)}, u32[]{:S(2)}) collective-permute-start(bf16[640,256]{1,0:T(8,128)(2,1)S(1)} %pad_maximum_fusion.1), channel_id=1, source_target_pairs={{0,32},{16,48},{32,0},{48,16},{1,33},{17,49},{33,1},{49,17},{2,34}... | collective-permute-start | bytes 983048 | tf_op jit(solution)/shard_map/ppermute | solution.py:20
  14.4 11.2 %collective-permute-start.1 = (bf16[640,256]{1,0:T(8,128)(2,1)S(1)}, bf16[640,256]{1,0:T(8,128)(2,1)S(1)}, u32[]{:S(2)}, u32[]{:S(2)}) collective-permute-start(bf16[640,256]{1,0:T(8,128)(2,1)S(1)} %pad_maximum_fusion.1), channel_id=1, source_target_pairs={{0,48},{16,0},{32,16},{48,32},{1,49},{17,1},{33,17},{49,33},{2,50}... | collective-permute-start | bytes 983048 | tf_op jit(solution)/shard_map/ppermute | solution.py:20
  18.3 12.8 %copy-start.3 = (bf16[640,256]{1,0:T(8,128)(2,1)}, bf16[640,256]{1,0:T(8,128)(2,1)S(1)}, u32[]{:S(2)}) copy-start(bf16[640,256]{1,0:T(8,128)(2,1)S(1)} %collective-permute-done) | copy-start | bytes 983044
  25.6 5.5 %copy-start.4 = (bf16[640,256]{1,0:T(8,128)(2,1)}, bf16[640,256]{1,0:T(8,128)(2,1)S(1)}, u32[]{:S(2)}) copy-start(bf16[640,256]{1,0:T(8,128)(2,1)S(1)} %collective-permute-done.1) | copy-start | bytes 983044
  27.8 18.2 %collective-permute-start.3 = (bf16[2560,256]{1,0:T(8,128)(2,1)}, bf16[2560,256]{1,0:T(8,128)(2,1)}, u32[]{:S(2)}, u32[]{:S(2)}) collective-permute-start(bf16[2560,256]{1,0:T(8,128)(2,1)} %constant_dynamic-update-slice_fusion), channel_id=1, source_target_pairs={{0,1},{1,0},{2,3},{3,2},{4,5},{5,4},{6,7},{7,6},{8,9},{9,8},{10,11... | collective-permute-start | bytes 3932168 | tf_op jit(solution)/shard_map/ppermute | solution.py:20
  31.1 41.2 %all-to-all-start = ((bf16[8,136,512]{2,1,0:T(8,128)(2,1)}), bf16[8,136,512]{2,1,0:T(8,128)(2,1)S(1)}, u32[]{:S(2)}, u32[]{:S(2)}) async-start(bf16[8,136,512]{2,1,0:T(8,128)(2,1)} %broadcast_in_dim.20), calls=%async_computation | async-start | bytes 2228224 | tf_op jit(solution)/shard_map/all_to_all | solution.py:24
  73.7 3.2 %copy-start = (f32[2048,1024]{1,0:T(8,128)}, f32[2048,1024]{1,0:T(8,128)S(1)}, u32[]{:S(2)}) copy-start(f32[2048,1024]{1,0:T(8,128)S(1)} %get-tuple-element.92) | copy-start | bytes 25165828
  77.6 11.7 %all-to-all-start.1 = ((f32[8,16,128]{2,1,0:T(8,128)}), f32[8,16,128]{2,1,0:T(8,128)S(1)}, u32[]{:S(2)}, u32[]{:S(2)}) async-start(f32[8,16,128]{2,1,0:T(8,128)} %broadcast_in_dim.21), calls=%async_computation.1 | async-start | bytes 131072 | tf_op jit(solution)/shard_map/all_to_all | solution.py:24
  85.9 2.0 copy-start.11
  90.6 26.1 %all-to-all-start.2 = ((bf16[32,64,128]{2,1,0:T(8,128)(2,1)}), bf16[32,64,128]{2,1,0:T(8,128)(2,1)S(1)}, u32[]{:S(2)}, u32[]{:S(2)}) async-start(bf16[32,64,128]{2,1,0:T(8,128)(2,1)} %bitcast.12), calls=%async_computation.2 | async-start | bytes 1048576 | tf_op jit(solution)/shard_map/all_to_all | solution.py:24
  117.8 25.1 %all-to-all-start.3 = ((bf16[8,72,512]{2,1,0:T(8,128)(2,1)}), bf16[8,72,512]{2,1,0:T(8,128)(2,1)S(1)}, u32[]{:S(2)}, u32[]{:S(2)}) async-start(bf16[8,72,512]{2,1,0:T(8,128)(2,1)} %broadcast_in_dim.46), calls=%async_computation.3 | async-start | bytes 1179648 | tf_op jit(solution)/shard_map/all_to_all | solution.py:24
  124.9 3.7 %copy-start.6 = (bf16[1024,256]{1,0:T(8,128)(2,1)S(1)}, bf16[1024,256]{1,0:T(8,128)(2,1)}, u32[]{:S(2)}) copy-start(bf16[1024,256]{1,0:T(8,128)(2,1)} %get-tuple-element.16) | copy-start | bytes 1572868
  128.5 10.4 %copy-start.1 = (f32[2048,256]{1,0:T(8,128)}, f32[2048,256]{1,0:T(8,128)S(1)}, u32[]{:S(2)}) copy-start(f32[2048,256]{1,0:T(8,128)S(1)} %fusion.21) | copy-start | bytes 6291460
  134.3 1.3 copy-start.2
  135.6 3.2 %copy-start.10 = (f32[256]{0:T(256)S(1)}, f32[256]{0:T(256)}, u32[]{:S(2)}) copy-start(f32[256]{0:T(256)} %param.9) | copy-start | bytes 3076
  136.7 10.5 %collective-permute-start.8 = (bf16[1024,512]{1,0:T(8,128)(2,1)}, bf16[1024,512]{1,0:T(8,128)(2,1)}, u32[]{:S(2)}, u32[]{:S(2)}) collective-permute-start(bf16[1024,512]{1,0:T(8,128)(2,1)} %pad_maximum_fusion), channel_id=1, source_target_pairs={{0,1},{1,0},{2,3},{3,2},{4,5},{5,4},{6,7},{7,6},{8,9},{9,8},{10,11... | collective-permute-start | bytes 3145736 | tf_op jit(solution)/shard_map/ppermute | solution.py:20
  143.4 3.8 %slice-start = ((f32[2048,256]{1,0:T(8,128)}), f32[1024,256]{1,0:T(8,128)S(1)}, s32[]{:S(2)}) async-start(f32[2048,256]{1,0:T(8,128)} %copy-done.1), calls=%async_computation.6 | async-start | bytes 2097152 | tf_op jit(solution)/shard_map/slice | solution.py:112
  143.4 3.8 %slice-start.1 = ((f32[2048,256]{1,0:T(8,128)}), f32[1024,256]{1,0:T(8,128)S(1)}, s32[]{:S(2)}) async-start(f32[2048,256]{1,0:T(8,128)} %copy-done.2), calls=%async_computation.7 | async-start | bytes 2097152 | tf_op jit(solution)/shard_map/slice | solution.py:112
  144.8 20.3 %collective-permute-start.4 = (bf16[512,512]{1,0:T(8,128)(2,1)S(1)}, bf16[512,512]{1,0:T(8,128)(2,1)S(1)}, u32[]{:S(2)}, u32[]{:S(2)}) collective-permute-start(bf16[512,512]{1,0:T(8,128)(2,1)S(1)} %bitcast.90), channel_id=1, source_target_pairs={{0,1},{1,0},{2,3},{3,2},{4,5},{5,4},{6,7},{7,6},{8,9},{9,8},{10,11... | collective-permute-start | bytes 1572872 | tf_op jit(solution)/shard_map/ppermute | solution.py:20
  148.7 16.0 %copy-start.5 = (bf16[256,8,1,1,64]{0,4,3,2,1:T(8,128)(2,1)S(1)}, bf16[256,8,1,1,64]{0,4,3,2,1:T(8,128)(2,1)}, u32[]{:S(2)}) copy-start(bf16[256,8,1,1,64]{0,4,3,2,1:T(8,128)(2,1)} %get-tuple-element.59) | copy-start | bytes 786436
  148.8 29.4 %all-to-all-start.4 = ((bf16[64,8,512]{2,1,0:T(8,128)(2,1)}), bf16[64,8,512]{2,1,0:T(8,128)(2,1)S(1)}, u32[]{:S(2)}, u32[]{:S(2)}) async-start(bf16[64,8,512]{2,1,0:T(8,128)(2,1)} %bitcast.29), calls=%async_computation.4 | async-start | bytes 1048576 | tf_op jit(solution)/shard_map/all_to_all | solution.py:24
  154.9 19.2 %collective-permute-start.9 = (bf16[256,512]{1,0:T(8,128)(2,1)S(1)}, bf16[256,512]{1,0:T(8,128)(2,1)S(1)}, u32[]{:S(2)}, u32[]{:S(2)}) collective-permute-start(bf16[256,512]{1,0:T(8,128)(2,1)S(1)} %get-tuple-element.70), channel_id=1, source_target_pairs={{0,32},{16,48},{32,0},{48,16},{1,33},{17,49},{33,1},{49,17},{2,34}... | collective-permute-start | bytes 786440 | tf_op jit(solution)/shard_map/ppermute | solution.py:20
  158.9 17.5 %collective-permute-start.10 = (bf16[256,512]{1,0:T(8,128)(2,1)S(1)}, bf16[256,512]{1,0:T(8,128)(2,1)S(1)}, u32[]{:S(2)}, u32[]{:S(2)}) collective-permute-start(bf16[256,512]{1,0:T(8,128)(2,1)S(1)} %get-tuple-element.71), channel_id=1, source_target_pairs={{0,16},{16,32},{32,48},{48,0},{1,17},{17,33},{33,49},{49,1},{2,18}... | collective-permute-start | bytes 786440 | tf_op jit(solution)/shard_map/ppermute | solution.py:20
  160.8 16.5 %collective-permute-start.11 = (bf16[256,512]{1,0:T(8,128)(2,1)S(1)}, bf16[256,512]{1,0:T(8,128)(2,1)S(1)}, u32[]{:S(2)}, u32[]{:S(2)}) collective-permute-start(bf16[256,512]{1,0:T(8,128)(2,1)S(1)} %get-tuple-element.72), channel_id=1, source_target_pairs={{0,48},{16,0},{32,16},{48,32},{1,49},{17,1},{33,17},{49,33},{2,50}... | collective-permute-start | bytes 786440 | tf_op jit(solution)/shard_map/ppermute | solution.py:20
  165.5 19.8 %collective-permute-start.5 = (bf16[256,128]{1,0:T(8,128)(2,1)S(1)}, bf16[256,128]{1,0:T(8,128)(2,1)S(1)}, u32[]{:S(2)}, u32[]{:S(2)}) collective-permute-start(bf16[256,128]{1,0:T(8,128)(2,1)S(1)} %get-tuple-element.73), channel_id=1, source_target_pairs={{0,16},{16,32},{32,48},{48,0},{1,17},{17,33},{33,49},{49,1},{2,18}... | collective-permute-start | bytes 196616 | tf_op jit(solution)/shard_map/ppermute | solution.py:20
  167.4 17.9 %collective-permute-start.7 = (bf16[256,128]{1,0:T(8,128)(2,1)S(1)}, bf16[256,128]{1,0:T(8,128)(2,1)S(1)}, u32[]{:S(2)}, u32[]{:S(2)}) collective-permute-start(bf16[256,128]{1,0:T(8,128)(2,1)S(1)} %get-tuple-element.74), channel_id=1, source_target_pairs={{0,32},{16,48},{32,0},{48,16},{1,33},{17,49},{33,1},{49,17},{2,34}... | collective-permute-start | bytes 196616 | tf_op jit(solution)/shard_map/ppermute | solution.py:20
  174.1 11.3 %collective-permute-start.6 = (bf16[256,128]{1,0:T(8,128)(2,1)S(1)}, bf16[256,128]{1,0:T(8,128)(2,1)S(1)}, u32[]{:S(2)}, u32[]{:S(2)}) collective-permute-start(bf16[256,128]{1,0:T(8,128)(2,1)S(1)} %get-tuple-element.75), channel_id=1, source_target_pairs={{0,48},{16,0},{32,16},{48,32},{1,49},{17,1},{33,17},{49,33},{2,50}... | collective-permute-start | bytes 196616 | tf_op jit(solution)/shard_map/ppermute | solution.py:20
  178.2 19.2 %all-to-all-start.5 = ((bf16[8,32,512]{2,1,0:T(8,128)(2,1)}), bf16[8,32,512]{2,1,0:T(8,128)(2,1)S(1)}, u32[]{:S(2)}, u32[]{:S(2)}) async-start(bf16[8,32,512]{2,1,0:T(8,128)(2,1)} %bitcast.35), calls=%async_computation.5 | async-start | bytes 524288 | tf_op jit(solution)/shard_map/all_to_all | solution.py:24

commit v5 on v2

--- a/solution.py
+++ b/solution.py
@@ -68,7 +68,6 @@
 
     pack = row_major(jnp.concatenate([half_of(keys), half_of(values), target], axis=0))
     blocks = [pack] + [shifted(pack, "x", by) for by in (1, -1, 2)]
-    half = nx * src // 2
     target_all = jnp.zeros((nx * rows, cols), BF16)
     for block, off in zip(blocks, (0, 3, 1, 2)):
         target_all = lax.dynamic_update_slice(target_all, block[src:], (lax.rem(x_at + off, nx) * rows, 0))
@@ -80,9 +79,13 @@
     w_odd = w_parts[:, :, 1].reshape(cols, -1)
     w_mine = jnp.where(core == 0, w_even, w_odd)
     w_theirs = jnp.where(core == 0, w_odd, w_even)
-    mine = [b[: src // 2] for b in blocks] + [b[src // 2 : src] for b in blocks]
-    mine = row_major(jnp.concatenate(mine + [target_all, w_theirs[:, :cols], w_theirs[:, cols:]], axis=0))
+
+    half = nx * src // 2
+    mine = [b[: src // 2] for b in blocks] + [b[src // 2 : src] for b in blocks] + [target_all]
+    mine = row_major(jnp.concatenate(mine, axis=0))
+    mine, w_mine, w_theirs = lax.optimization_barrier((mine, w_mine, w_theirs))
     theirs = shifted(mine, "c", 1)
+    target_other = theirs[2 * half :]
     key_one, value_one = mine[:half], mine[half : 2 * half]
     key_two, value_two = theirs[:half], theirs[half : 2 * half]
 
@@ -116,6 +119,8 @@
     sent = (query_t * share[None]).astype(BF16).reshape(nx, part, nz, rows).transpose(2, 0, 1, 3)
     sent = sent.reshape(nz * nx, part, rows)
     got = exchanged(sent, ("z", "x")).reshape(nz, nx, part, rows)
+    part_t = got.astype(F32).sum(axis=0)
+    part_t = part_t.transpose(1, 0, 2).reshape(part, nx * rows).astype(BF16)
 
     query_share, grad_share, _ = lax.optimization_barrier(
         ((query_all * share[:, None]).astype(BF16), (grad_all * share[:, None]).astype(BF16), sent)
@@ -126,21 +131,6 @@
 
     swap = shifted(row_major(sums_of(grad_two, weight_two).astype(BF16)), "c", 1)
     mine = row_major((sums_of(grad_one, weight_one) + swap.astype(F32)).astype(BF16))
-
-    def by_core(mine, theirs):
-        return jnp.where(core == 0, jnp.stack([mine, theirs]), jnp.stack([theirs, mine]))
-
-    theirs, target_all, w_mine, _ = lax.optimization_barrier((theirs[2 * half :], target_all, w_mine, sent))
-    target_other, w_other = theirs[: nx * rows], theirs[nx * rows :]
-    w_other = jnp.concatenate([w_other[:cols], w_other[cols:]], axis=1)
-    target_both = row_major(by_core(row_major(target_all.T), row_major(target_other.T)))
-    w_both = by_core(w_mine, w_other).reshape(2 * cols, -1)
-    squares = jnp.sum(jnp.square(target_both.astype(F32)), axis=(0, 1))
-
-    got, mine, target_both = lax.optimization_barrier((got, mine, target_both))
-    target_both = target_both.astype(F32)
-    part_t = got.astype(F32).sum(axis=0)
-    part_t = part_t.transpose(1, 0, 2).reshape(part, nx * rows).astype(BF16)
     own, left, right, far = (mine[src // 2 * k : src // 2 * (k + 1)] for k in range(nx))
     own = own.astype(F32)
     moved = [shifted(block, "x", by) for block, by in ((far, 2), (right, 1), (left, -1))]
@@ -148,6 +138,11 @@
         own = own + block.astype(F32)
     mine = own.astype(BF16)
 
+    def by_core(mine, theirs):
+        return jnp.where(core == 0, jnp.stack([mine, theirs]), jnp.stack([theirs, mine]))
+
+    target_both = by_core(target_all.T, target_other.T).astype(F32)
+    squares = jnp.sum(target_both * target_both, axis=(0, 1))
     high = lax.reduce_precision(squares, 8, 7)
     extra = jnp.stack([high, squares - high]).astype(BF16)
     piece = jnp.concatenate([part_t, extra, jnp.zeros((6, nx * rows), BF16)], axis=0)
@@ -167,7 +162,8 @@
     grad_weight = weight_sum.transpose(2, 3, 1, 0, 4).reshape(8, WIDTH)
 
     grad_t, _ = lax.optimization_barrier((grad_t, weight_sent))
-    rows_t = dot(w_both, grad_t, 1, 0)
+    grad_other = shifted(grad_t, "c", 1)
+    rows_t = dot(w_mine, grad_t, 1, 0) + dot(w_theirs, grad_other, 1, 0)
 
     def rows_at(off):
         return lax.dynamic_slice_in_dim(rows_t, lax.rem(x_at + off, nx) * rows, rows, 1)
@@ -175,9 +171,7 @@
     rows_sum = rows_at(0)
     for off, by in ((1, 1), (3, -1), (2, 2)):
         rows_sum = rows_sum + shifted(rows_at(off).astype(BF16), "x", by).astype(F32)
-    low, high = rows_sum[:cols], rows_sum[cols:]
-    rows_in = shifted(jnp.where(core == 0, high, low).astype(BF16), "c", 1)
-    grad_rows = (jnp.where(core == 0, low, high) + rows_in.astype(F32)).T.astype(BF16)
+    grad_rows = rows_sum.T.astype(BF16)
 
     mine, _ = lax.optimization_barrier((mine, weight_got))
     sums = exchanged(mine.reshape(ny, bit, 2 * HEAD_DIM), "y")

time: 197 us -> 186 us (0.944)
  matrix products: 12.3 us -> 21 us
  local copies, waits for them, and re-layouts: 42.3 us -> 33.6 us
  starting transfers between devices: 81.2 us -> 76.6 us
  waiting for transfers between devices: 42.9 us -> 39.2 us
  other arithmetic: 15 us -> 12.4 us
    ppermute x12, waiting for transfers between devices: 10.8 us -> 0.24 us  [shifted(): return lax.ppermute(value, axis, [(i, (i + by) % n) for i in range(n)])]
    dot_general x12 -> x13, matrix products: 12.3 us -> 21 us  [dot(): lax.dot_general(a, b, (((ca,), (cb,)), ((), ())), preferred_element_type=...]
    all_to_all x6, waiting for transfers between devices: 32.1 us -> 38.9 us  [exchanged(): return lax.all_to_all(value, axis, split_axis=0, concat_axis=0, tiled=True)]
    all_to_all x6, starting transfers between devices: 42.9 us -> 36.4 us  [exchanged(): return lax.all_to_all(value, axis, split_axis=0, concat_axis=0, tiled=True)]
    unnamed x53 -> x51, local copies, waits for them, and re-layouts: 24.9 us -> 21.1 us
  transfers between devices with their start and end apart: 18 -> 18, of which waited for: 7 -> 5; matrix products, arithmetic and copies ran while one was open for 23% -> 28% of each run, Pallas kernels for 0% -> 0%
where the time goes in v5:
time: 186 us; the launch traced here: 184 us
  starting transfers between devices  76.6 us (41%)
  waiting for transfers between devices  39.2 us (21%)
  local copies, waits for them, and re-layouts  33.6 us (18%)
  matrix products  21 us (11%)
  other arithmetic  12.4 us (7%)
    ppermute x12, starting transfers between devices, shifted(): return lax.ppermute(value, axis, [(i, (i + by) % n) for i in range(n)])  40.2 us
    all_to_all x6, waiting for transfers between devices, exchanged(): return lax.all_to_all(value, axis, split_axis=0, concat_axis=0, tiled=True)  38.9 us
    all_to_all x6, starting transfers between devices, exchanged(): return lax.all_to_all(value, axis, split_axis=0, concat_axis=0, tiled=True)  36.4 us
    unnamed x51, local copies, waits for them, and re-layouts  21.1 us
    dot_general x13, matrix products, dot(): lax.dot_general(a, b, (((ca,), (cb,)), ((), ())), preferred_element_type=...  21 us
  transfers between devices with their start and end apart: 18, of which 5 were waited for; matrix products, arithmetic and copies ran while one was open for 28% of the time, Pallas kernels for 0%

profile of v5, /device:TPU:2, one launch (start us, length us, event | category | flops | bytes accessed | tf_op | source)
XLA Modules:
  0.0 184.3 jit_solution(7136937336845104625)
XLA Ops:
  2.3 1.6 pad_maximum_fusion.1
  3.9 3.4 %collective-permute-start = (bf16[640,256]{1,0:T(8,128)(2,1)}, bf16[640,256]{1,0:T(8,128)(2,1)}, u32[]{:S(2)}, u32[]{:S(2)}) collective-permute-start(bf16[640,256]{1,0:T(8,128)(2,1)} %pad_maximum_fusion.1), channel_id=1, source_target_pairs={{0,16},{16,32},{32,48},{48,0},{1,17},{17,33},{33,49},{49,1},{2,18}... | collective-permute-start | bytes 983048 | tf_op jit(solution)/shard_map/ppermute | solution.py:20
  7.3 8.4 %collective-permute-start.2 = (bf16[640,256]{1,0:T(8,128)(2,1)}, bf16[640,256]{1,0:T(8,128)(2,1)}, u32[]{:S(2)}, u32[]{:S(2)}) collective-permute-start(bf16[640,256]{1,0:T(8,128)(2,1)} %pad_maximum_fusion.1), channel_id=1, source_target_pairs={{0,32},{16,48},{32,0},{48,16},{1,33},{17,49},{33,1},{49,17},{2,34}... | collective-permute-start | bytes 983048 | tf_op jit(solution)/shard_map/ppermute | solution.py:20
  15.7 1.9 %collective-permute-start.1 = (bf16[640,256]{1,0:T(8,128)(2,1)}, bf16[640,256]{1,0:T(8,128)(2,1)}, u32[]{:S(2)}, u32[]{:S(2)}) collective-permute-start(bf16[640,256]{1,0:T(8,128)(2,1)} %pad_maximum_fusion.1), channel_id=1, source_target_pairs={{0,48},{16,0},{32,16},{48,32},{1,49},{17,1},{33,17},{49,33},{2,50}... | collective-permute-start | bytes 983048 | tf_op jit(solution)/shard_map/ppermute | solution.py:20
  20.8 7.1 %all-to-all-start = ((bf16[8,136,512]{2,1,0:T(8,128)(2,1)}), bf16[8,136,512]{2,1,0:T(8,128)(2,1)S(1)}, u32[]{:S(2)}, u32[]{:S(2)}) async-start(bf16[8,136,512]{2,1,0:T(8,128)(2,1)} %broadcast_in_dim.20), calls=%async_computation | async-start | bytes 2228224 | tf_op jit(solution)/shard_map/all_to_all | solution.py:24
  27.9 3.3 %copy.146 = bf16[256,4096]{0,1:T(8,128)(2,1)S(1)} copy(bf16[256,4096]{1,0:T(8,128)(2,1)} %param.10) | data formatting | bytes 4194304 | tf_op args[2]
  31.3 1.6 constant_dynamic-update-slice_fusion.2
  33.7 1.6 slice_dynamic-update-slice_fusion.5
  36.1 1.6 slice_dynamic-update-slice_fusion.4
  37.7 1.6 slice_dynamic-update-slice_fusion.3
  39.3 1.6 constant_dynamic-update-slice_fusion.1
  42.5 1.6 slice_dynamic-update-slice_fusion.2
  44.1 1.6 slice_dynamic-update-slice_fusion.1
  45.7 1.6 slice_dynamic-update-slice_fusion
  48.0 1.9 %collective-permute-start.3 = (bf16[2560,256]{1,0:T(8,128)(2,1)}, bf16[2560,256]{1,0:T(8,128)(2,1)}, u32[]{:S(2)}, u32[]{:S(2)}) collective-permute-start(bf16[2560,256]{1,0:T(8,128)(2,1)} %constant_dynamic-update-slice_fusion), channel_id=1, source_target_pairs={{0,1},{1,0},{2,3},{3,2},{4,5},{5,4},{6,7},{7,6},{8,9},{9,8},{10,11... | collective-permute-start | bytes 3932168 | tf_op jit(solution)/shard_map/ppermute | solution.py:20
  50.0 7.1 %all-to-all-done = bf16[8,136,512]{2,1,0:T(8,128)(2,1)S(1)} async-done(((bf16[8,136,512]{2,1,0:T(8,128)(2,1)}), bf16[8,136,512]{2,1,0:T(8,128)(2,1)S(1)}, u32[]{:S(2)}, u32[]{:S(2)}) %all-to-all-start) | async-done | bytes 1114144 | tf_op jit(solution)/shard_map/all_to_all | solution.py:24
  57.3 1.8 multiply_reduce_fusion.1
  59.1 1.8 multiply_reduce_fusion
  60.9 3.1 %fusion.2 = (f32[1024]{0:T(1024)S(1)}, f32[1024]{0:T(1024)S(1)}, bf16[1024,1024]{1,0:T(8,128)(2,1)}, bf16[1024,1024]{1,0:T(8,128)(2,1)}) fusion(f32[1024,1024]{1,0:T(8,128)S(1)} %get-tuple-element.94, f32[1024]{0:T(1024)S(1)} %max.18, f32[1024,1024]{1,0:T(8,128)S(1)} %get-tuple-element.92), kind=kLoop, calls=%fused_computation.8 | loop fusion | flops 8386560 | bytes 12595200 | tf_op jit(solution)/shard_map/reduce_sum | solution.py:101
  64.7 3.4 %all-to-all-start.1 = ((f32[8,16,128]{2,1,0:T(8,128)}), f32[8,16,128]{2,1,0:T(8,128)S(1)}, u32[]{:S(2)}, u32[]{:S(2)}) async-start(f32[8,16,128]{2,1,0:T(8,128)} %broadcast_in_dim.21), calls=%async_computation.1 | async-start | bytes 131072 | tf_op jit(solution)/shard_map/all_to_all | solution.py:24
  68.0 2.6 %multiply_convert_fusion.1 = bf16[1024,1024]{1,0:T(8,128)(2,1)S(1)} fusion(bf16[1024,1024]{1,0:T(8,128)(2,1)} %get-tuple-element.18, bf16[1024,256]{1,0:T(8,128)(2,1)S(1)} %bitcast.107, f32[1024]{0:T(1024)S(1)} %bitcast.126, bf16[2560,256]{1,0:T(8,128)(2,1)} %constant_dynamic-update-slice_fusion), kind=kOutput, calls=%fused_computation.1 | convolution fusion | flops 542113792 | bytes 5246976 | tf_op jit(solution)/shard_map/dot_general | solution.py:33
  70.6 2.3 %fusion.13 = f32[256,1024]{1,0:T(8,128)S(1)} fusion(bf16[1024,1024]{1,0:T(8,128)(2,1)S(1)} %multiply_convert_fusion.1, bf16[2560,256]{1,0:T(8,128)(2,1)} %constant_dynamic-update-slice_fusion), kind=kOutput, calls=%fused_computation.34 | convolution fusion | flops 536870912 | bytes 3670016 | tf_op jit(solution)/shard_map/dot_general | solution.py:33
  73.1 1.9 %multiply_convert_fusion = bf16[1024,1024]{1,0:T(8,128)(2,1)S(1)} fusion(bf16[1024,1024]{1,0:T(8,128)(2,1)S(1)} %copy-done.1, bf16[1024,256]{1,0:T(8,128)(2,1)S(1)} %bitcast.108, f32[1024]{0:T(1024)S(1)} %bitcast.127, bf16[2560,256]{1,0:T(8,128)(2,1)} %collective-permute-done.3), kind=kOutput, calls=%fused_computation | convolution fusion | flops 542113792 | bytes 5246976 | tf_op jit(solution)/shard_map/dot_general | solution.py:33
  75.0 1.3 copy-done.5
  76.4 1.8 convolution_add_fusion
  79.5 8.7 %all-to-all-start.2 = ((bf16[32,64,128]{2,1,0:T(8,128)(2,1)}), bf16[32,64,128]{2,1,0:T(8,128)(2,1)S(1)}, u32[]{:S(2)}, u32[]{:S(2)}) async-start(bf16[32,64,128]{2,1,0:T(8,128)(2,1)} %bitcast.15), calls=%async_computation.2 | async-start | bytes 1048576 | tf_op jit(solution)/shard_map/all_to_all | solution.py:24
  88.3 1.1 slice_bitcast_fusion
  89.6 1.1 multiply_convert_fusion.2
  91.6 1.5 convolution_convert_fusion.1
  93.1 11.9 %all-to-all-done.2 = bf16[32,64,128]{2,1,0:T(8,128)(2,1)S(1)} async-done(((bf16[32,64,128]{2,1,0:T(8,128)(2,1)}), bf16[32,64,128]{2,1,0:T(8,128)(2,1)S(1)}, u32[]{:S(2)}, u32[]{:S(2)}) %all-to-all-start.2) | async-done | bytes 524320 | tf_op jit(solution)/shard_map/all_to_all | solution.py:24
  106.1 7.1 %all-to-all-start.3 = ((bf16[8,72,512]{2,1,0:T(8,128)(2,1)}), bf16[8,72,512]{2,1,0:T(8,128)(2,1)S(1)}, u32[]{:S(2)}, u32[]{:S(2)}) async-start(bf16[8,72,512]{2,1,0:T(8,128)(2,1)} %broadcast_in_dim.23), calls=%async_computation.3 | async-start | bytes 1179648 | tf_op jit(solution)/shard_map/all_to_all | solution.py:24
  113.2 1.8 convolution_convert_fusion.2
  115.2 2.2 %collective-permute-start.8 = (bf16[1024,512]{1,0:T(8,128)(2,1)S(1)}, bf16[1024,512]{1,0:T(8,128)(2,1)}, u32[]{:S(2)}, u32[]{:S(2)}) collective-permute-start(bf16[1024,512]{1,0:T(8,128)(2,1)S(1)} %pad_maximum_fusion), channel_id=1, source_target_pairs={{0,1},{1,0},{2,3},{3,2},{4,5},{5,4},{6,7},{7,6},{8,9},{9,8},{10,11... | collective-permute-start | bytes 3145736 | tf_op jit(solution)/shard_map/ppermute | solution.py:20
  117.4 1.7 fusion.27
  119.1 1.7 fusion.26
  120.8 9.9 %all-to-all-done.3 = bf16[8,72,512]{2,1,0:T(8,128)(2,1)S(1)} async-done(((bf16[8,72,512]{2,1,0:T(8,128)(2,1)}), bf16[8,72,512]{2,1,0:T(8,128)(2,1)S(1)}, u32[]{:S(2)}, u32[]{:S(2)}) %all-to-all-start.3) | async-done | bytes 589856 | tf_op jit(solution)/shard_map/all_to_all | solution.py:24
  132.6 2.1 %collective-permute-start.4 = (bf16[512,512]{1,0:T(8,128)(2,1)S(1)}, bf16[512,512]{1,0:T(8,128)(2,1)}, u32[]{:S(2)}, u32[]{:S(2)}) collective-permute-start(bf16[512,512]{1,0:T(8,128)(2,1)S(1)} %bitcast.97), channel_id=1, source_target_pairs={{0,1},{1,0},{2,3},{3,2},{4,5},{5,4},{6,7},{7,6},{8,9},{9,8},{10,11... | collective-permute-start | bytes 1572872 | tf_op jit(solution)/shard_map/ppermute | solution.py:20
  134.7 1.5 fusion.4
  136.2 6.7 %all-to-all-start.4 = ((bf16[64,8,512]{2,1,0:T(8,128)(2,1)}), bf16[64,8,512]{2,1,0:T(8,128)(2,1)S(1)}, u32[]{:S(2)}, u32[]{:S(2)}) async-start(bf16[64,8,512]{2,1,0:T(8,128)(2,1)} %bitcast.29), calls=%async_computation.4 | async-start | bytes 1048576 | tf_op jit(solution)/shard_map/all_to_all | solution.py:24
  143.0 4.0 %collective-permute-start.9 = (bf16[256,512]{1,0:T(8,128)(2,1)S(1)}, bf16[256,512]{1,0:T(8,128)(2,1)S(1)}, u32[]{:S(2)}, u32[]{:S(2)}) collective-permute-start(bf16[256,512]{1,0:T(8,128)(2,1)S(1)} %get-tuple-element.76), channel_id=1, source_target_pairs={{0,32},{16,48},{32,0},{48,16},{1,33},{17,49},{33,1},{49,17},{2,34}... | collective-permute-start | bytes 786440 | tf_op jit(solution)/shard_map/ppermute | solution.py:20
  147.0 1.9 %collective-permute-start.10 = (bf16[256,512]{1,0:T(8,128)(2,1)S(1)}, bf16[256,512]{1,0:T(8,128)(2,1)S(1)}, u32[]{:S(2)}, u32[]{:S(2)}) collective-permute-start(bf16[256,512]{1,0:T(8,128)(2,1)S(1)} %get-tuple-element.77), channel_id=1, source_target_pairs={{0,16},{16,32},{32,48},{48,0},{1,17},{17,33},{33,49},{49,1},{2,18}... | collective-permute-start | bytes 786440 | tf_op jit(solution)/shard_map/ppermute | solution.py:20
  148.9 3.9 %collective-permute-start.11 = (bf16[256,512]{1,0:T(8,128)(2,1)S(1)}, bf16[256,512]{1,0:T(8,128)(2,1)S(1)}, u32[]{:S(2)}, u32[]{:S(2)}) collective-permute-start(bf16[256,512]{1,0:T(8,128)(2,1)S(1)} %get-tuple-element.78), channel_id=1, source_target_pairs={{0,48},{16,0},{32,16},{48,32},{1,49},{17,1},{33,17},{49,33},{2,50}... | collective-permute-start | bytes 786440 | tf_op jit(solution)/shard_map/ppermute | solution.py:20
  153.2 1.4 convolution_add_fusion.1
  154.7 1.9 %collective-permute-start.5 = (bf16[256,128]{1,0:T(8,128)(2,1)S(1)}, bf16[256,128]{1,0:T(8,128)(2,1)S(1)}, u32[]{:S(2)}, u32[]{:S(2)}) collective-permute-start(bf16[256,128]{1,0:T(8,128)(2,1)S(1)} %get-tuple-element.79), channel_id=1, source_target_pairs={{0,16},{16,32},{32,48},{48,0},{1,17},{17,33},{33,49},{49,1},{2,18}... | collective-permute-start | bytes 196616 | tf_op jit(solution)/shard_map/ppermute | solution.py:20
  156.6 6.6 %collective-permute-start.7 = (bf16[256,128]{1,0:T(8,128)(2,1)S(1)}, bf16[256,128]{1,0:T(8,128)(2,1)S(1)}, u32[]{:S(2)}, u32[]{:S(2)}) collective-permute-start(bf16[256,128]{1,0:T(8,128)(2,1)S(1)} %get-tuple-element.80), channel_id=1, source_target_pairs={{0,32},{16,48},{32,0},{48,16},{1,33},{17,49},{33,1},{49,17},{2,34}... | collective-permute-start | bytes 196616 | tf_op jit(solution)/shard_map/ppermute | solution.py:20
  163.2 1.9 %collective-permute-start.6 = (bf16[256,128]{1,0:T(8,128)(2,1)S(1)}, bf16[256,128]{1,0:T(8,128)(2,1)S(1)}, u32[]{:S(2)}, u32[]{:S(2)}) collective-permute-start(bf16[256,128]{1,0:T(8,128)(2,1)S(1)} %get-tuple-element.81), channel_id=1, source_target_pairs={{0,48},{16,0},{32,16},{48,32},{1,49},{17,1},{33,17},{49,33},{2,50}... | collective-permute-start | bytes 196616 | tf_op jit(solution)/shard_map/ppermute | solution.py:20
  166.2 3.4 %all-to-all-start.5 = ((bf16[8,32,512]{2,1,0:T(8,128)(2,1)}), bf16[8,32,512]{2,1,0:T(8,128)(2,1)S(1)}, u32[]{:S(2)}, u32[]{:S(2)}) async-start(bf16[8,32,512]{2,1,0:T(8,128)(2,1)} %bitcast.35), calls=%async_computation.5 | async-start | bytes 524288 | tf_op jit(solution)/shard_map/all_to_all | solution.py:24
  171.8 10.0 %all-to-all-done.5 = bf16[8,32,512]{2,1,0:T(8,128)(2,1)S(1)} async-done(((bf16[8,32,512]{2,1,0:T(8,128)(2,1)}), bf16[8,32,512]{2,1,0:T(8,128)(2,1)S(1)}, u32[]{:S(2)}, u32[]{:S(2)}) %all-to-all-start.5) | async-done | bytes 262176 | tf_op jit(solution)/shard_map/all_to_all | solution.py:24
  (120 shorter events, 21.5 us)
Async XLA Ops:
  1.7 0.7 copy-start.7
  1.7 2.2 %copy-start.8 = (bf16[8,1,32,256]{3,2,1,0:T(8,128)(2,1)}, bf16[8,1,32,256]{3,2,1,0:T(8,128)(2,1)S(1)}, u32[]{:S(2)}) copy-start(bf16[8,1,32,256]{3,2,1,0:T(8,128)(2,1)S(1)} %get-tuple-element.96) | copy-start | bytes 393220
  3.9 29.8 %collective-permute-start = (bf16[640,256]{1,0:T(8,128)(2,1)}, bf16[640,256]{1,0:T(8,128)(2,1)}, u32[]{:S(2)}, u32[]{:S(2)}) collective-permute-start(bf16[640,256]{1,0:T(8,128)(2,1)} %pad_maximum_fusion.1), channel_id=1, source_target_pairs={{0,16},{16,32},{32,48},{48,0},{1,17},{17,33},{33,49},{49,1},{2,18}... | collective-permute-start | bytes 983048 | tf_op jit(solution)/shard_map/ppermute | solution.py:20
  7.3 30.4 %collective-permute-start.2 = (bf16[640,256]{1,0:T(8,128)(2,1)}, bf16[640,256]{1,0:T(8,128)(2,1)}, u32[]{:S(2)}, u32[]{:S(2)}) collective-permute-start(bf16[640,256]{1,0:T(8,128)(2,1)} %pad_maximum_fusion.1), channel_id=1, source_target_pairs={{0,32},{16,48},{32,0},{48,16},{1,33},{17,49},{33,1},{49,17},{2,34}... | collective-permute-start | bytes 983048 | tf_op jit(solution)/shard_map/ppermute | solution.py:20
  15.7 20.5 %collective-permute-start.1 = (bf16[640,256]{1,0:T(8,128)(2,1)}, bf16[640,256]{1,0:T(8,128)(2,1)}, u32[]{:S(2)}, u32[]{:S(2)}) collective-permute-start(bf16[640,256]{1,0:T(8,128)(2,1)} %pad_maximum_fusion.1), channel_id=1, source_target_pairs={{0,48},{16,0},{32,16},{48,32},{1,49},{17,1},{33,17},{49,33},{2,50}... | collective-permute-start | bytes 983048 | tf_op jit(solution)/shard_map/ppermute | solution.py:20
  20.8 36.4 %all-to-all-start = ((bf16[8,136,512]{2,1,0:T(8,128)(2,1)}), bf16[8,136,512]{2,1,0:T(8,128)(2,1)S(1)}, u32[]{:S(2)}, u32[]{:S(2)}) async-start(bf16[8,136,512]{2,1,0:T(8,128)(2,1)} %broadcast_in_dim.20), calls=%async_computation | async-start | bytes 2228224 | tf_op jit(solution)/shard_map/all_to_all | solution.py:24
  27.9 3.4 %copy-start.17 = (bf16[128,256]{1,0:T(8,128)(2,1)S(1)}, bf16[128,256]{1,0:T(8,128)(2,1)}, u32[]{:S(2)}) copy-start(bf16[128,256]{1,0:T(8,128)(2,1)} %param.8) | copy-start | bytes 196612
  31.3 18.7 %copy-start.18 = (f32[256]{0:T(256)S(1)}, f32[256]{0:T(256)}, u32[]{:S(2)}) copy-start(f32[256]{0:T(256)} %param.9) | copy-start | bytes 3076
  48.0 11.2 %collective-permute-start.3 = (bf16[2560,256]{1,0:T(8,128)(2,1)}, bf16[2560,256]{1,0:T(8,128)(2,1)}, u32[]{:S(2)}, u32[]{:S(2)}) collective-permute-start(bf16[2560,256]{1,0:T(8,128)(2,1)} %constant_dynamic-update-slice_fusion), channel_id=1, source_target_pairs={{0,1},{1,0},{2,3},{3,2},{4,5},{5,4},{6,7},{7,6},{8,9},{9,8},{10,11... | collective-permute-start | bytes 3932168 | tf_op jit(solution)/shard_map/ppermute | solution.py:20
  64.7 13.5 %all-to-all-start.1 = ((f32[8,16,128]{2,1,0:T(8,128)}), f32[8,16,128]{2,1,0:T(8,128)S(1)}, u32[]{:S(2)}, u32[]{:S(2)}) async-start(f32[8,16,128]{2,1,0:T(8,128)} %broadcast_in_dim.21), calls=%async_computation.1 | async-start | bytes 131072 | tf_op jit(solution)/shard_map/all_to_all | solution.py:24
  70.6 4.4 %copy-start.3 = (bf16[1024,1024]{1,0:T(8,128)(2,1)}, bf16[1024,1024]{1,0:T(8,128)(2,1)S(1)}, u32[]{:S(2)}) copy-start(bf16[1024,1024]{1,0:T(8,128)(2,1)S(1)} %multiply_convert_fusion.1) | copy-start | bytes 6291460
  70.6 2.5 %copy-start.1 = (bf16[1024,1024]{1,0:T(8,128)(2,1)S(1)}, bf16[1024,1024]{1,0:T(8,128)(2,1)}, u32[]{:S(2)}) copy-start(bf16[1024,1024]{1,0:T(8,128)(2,1)} %get-tuple-element.19) | copy-start | bytes 6291460
  75.0 1.4 copy-start.5
  79.5 25.5 %all-to-all-start.2 = ((bf16[32,64,128]{2,1,0:T(8,128)(2,1)}), bf16[32,64,128]{2,1,0:T(8,128)(2,1)S(1)}, u32[]{:S(2)}, u32[]{:S(2)}) async-start(bf16[32,64,128]{2,1,0:T(8,128)(2,1)} %bitcast.15), calls=%async_computation.2 | async-start | bytes 1048576 | tf_op jit(solution)/shard_map/all_to_all | solution.py:24
  88.3 3.3 %copy-start.2 = (bf16[1024,1024]{1,0:T(8,128)(2,1)S(1)}, bf16[1024,1024]{1,0:T(8,128)(2,1)}, u32[]{:S(2)}) copy-start(bf16[1024,1024]{1,0:T(8,128)(2,1)} %get-tuple-element.19) | copy-start | bytes 6291460
  90.8 0.8 copy-start.14
  93.1 20.1 %copy-start.6 = (bf16[1024,1024]{1,0:T(8,128)(2,1)S(1)}, bf16[1024,1024]{1,0:T(8,128)(2,1)}, u32[]{:S(2)}) copy-start(bf16[1024,1024]{1,0:T(8,128)(2,1)} %copy-done.5) | copy-start | bytes 6291460
  106.1 24.6 %all-to-all-start.3 = ((bf16[8,72,512]{2,1,0:T(8,128)(2,1)}), bf16[8,72,512]{2,1,0:T(8,128)(2,1)S(1)}, u32[]{:S(2)}, u32[]{:S(2)}) async-start(bf16[8,72,512]{2,1,0:T(8,128)(2,1)} %broadcast_in_dim.23), calls=%async_computation.3 | async-start | bytes 1179648 | tf_op jit(solution)/shard_map/all_to_all | solution.py:24
  113.2 1.9 %copy-start.16 = (bf16[1024,256]{1,0:T(8,128)(2,1)S(1)}, bf16[1024,256]{1,0:T(8,128)(2,1)}, u32[]{:S(2)}) copy-start(bf16[1024,256]{1,0:T(8,128)(2,1)} %convolution_convert_fusion.1) | copy-start | bytes 1572868
  113.2 4.2 %copy-start.15 = (bf16[1024,256]{1,0:T(8,128)(2,1)S(1)}, bf16[1024,256]{1,0:T(8,128)(2,1)}, u32[]{:S(2)}) copy-start(bf16[1024,256]{1,0:T(8,128)(2,1)} %copy-done.14) | copy-start | bytes 1572868
  115.1 2.3 %copy-start = (bf16[1024,1024]{1,0:T(8,128)(2,1)S(1)}, bf16[1024,1024]{1,0:T(8,128)(2,1)}, u32[]{:S(2)}) copy-start(bf16[1024,1024]{1,0:T(8,128)(2,1)} %get-tuple-element.18) | copy-start | bytes 6291460
  115.2 3.9 %copy-start.4 = (bf16[1024,1024]{1,0:T(8,128)(2,1)S(1)}, bf16[1024,1024]{1,0:T(8,128)(2,1)}, u32[]{:S(2)}) copy-start(bf16[1024,1024]{1,0:T(8,128)(2,1)} %copy-done.3) | copy-start | bytes 6291460
  115.2 3.9 %copy-start.13 = (bf16[1024,256]{1,0:T(8,128)(2,1)S(1)}, bf16[1024,256]{1,0:T(8,128)(2,1)}, u32[]{:S(2)}) copy-start(bf16[1024,256]{1,0:T(8,128)(2,1)} %get-tuple-element.25) | copy-start | bytes 1572868
  115.2 19.5 %collective-permute-start.8 = (bf16[1024,512]{1,0:T(8,128)(2,1)S(1)}, bf16[1024,512]{1,0:T(8,128)(2,1)}, u32[]{:S(2)}, u32[]{:S(2)}) collective-permute-start(bf16[1024,512]{1,0:T(8,128)(2,1)S(1)} %pad_maximum_fusion), channel_id=1, source_target_pairs={{0,1},{1,0},{2,3},{3,2},{4,5},{5,4},{6,7},{7,6},{8,9},{9,8},{10,11... | collective-permute-start | bytes 3145736 | tf_op jit(solution)/shard_map/ppermute | solution.py:20
  131.2 3.5 %copy-start.11 = (f32[1024,256]{1,0:T(8,128)S(1)}, f32[1024,256]{1,0:T(8,128)}, u32[]{:S(2)}) copy-start(f32[1024,256]{1,0:T(8,128)} %fusion.27) | copy-start | bytes 3145732
  131.2 3.5 %copy-start.12 = (f32[1024,256]{1,0:T(8,128)S(1)}, f32[1024,256]{1,0:T(8,128)}, u32[]{:S(2)}) copy-start(f32[1024,256]{1,0:T(8,128)} %fusion.26) | copy-start | bytes 3145732
  132.6 20.6 %collective-permute-start.4 = (bf16[512,512]{1,0:T(8,128)(2,1)S(1)}, bf16[512,512]{1,0:T(8,128)(2,1)}, u32[]{:S(2)}, u32[]{:S(2)}) collective-permute-start(bf16[512,512]{1,0:T(8,128)(2,1)S(1)} %bitcast.97), channel_id=1, source_target_pairs={{0,1},{1,0},{2,3},{3,2},{4,5},{5,4},{6,7},{7,6},{8,9},{9,8},{10,11... | collective-permute-start | bytes 1572872 | tf_op jit(solution)/shard_map/ppermute | solution.py:20
  136.2 16.7 %copy-start.10 = (bf16[256,8,1,1,64]{0,4,3,2,1:T(8,128)(2,1)S(1)}, bf16[256,8,1,1,64]{0,4,3,2,1:T(8,128)(2,1)}, u32[]{:S(2)}) copy-start(bf16[256,8,1,1,64]{0,4,3,2,1:T(8,128)(2,1)} %get-tuple-element.73) | copy-start | bytes 786436
  136.2 17.0 %copy-start.9 = (bf16[256,8,1,1,64]{0,4,3,2,1:T(8,128)(2,1)S(1)}, bf16[256,8,1,1,64]{0,4,3,2,1:T(8,128)(2,1)}, u32[]{:S(2)}) copy-start(bf16[256,8,1,1,64]{0,4,3,2,1:T(8,128)(2,1)} %get-tuple-element.72) | copy-start | bytes 786436
  136.2 30.0 %all-to-all-start.4 = ((bf16[64,8,512]{2,1,0:T(8,128)(2,1)}), bf16[64,8,512]{2,1,0:T(8,128)(2,1)S(1)}, u32[]{:S(2)}, u32[]{:S(2)}) async-start(bf16[64,8,512]{2,1,0:T(8,128)(2,1)} %bitcast.29), calls=%async_computation.4 | async-start | bytes 1048576 | tf_op jit(solution)/shard_map/all_to_all | solution.py:24
  143.0 20.2 %collective-permute-start.9 = (bf16[256,512]{1,0:T(8,128)(2,1)S(1)}, bf16[256,512]{1,0:T(8,128)(2,1)S(1)}, u32[]{:S(2)}, u32[]{:S(2)}) collective-permute-start(bf16[256,512]{1,0:T(8,128)(2,1)S(1)} %get-tuple-element.76), channel_id=1, source_target_pairs={{0,32},{16,48},{32,0},{48,16},{1,33},{17,49},{33,1},{49,17},{2,34}... | collective-permute-start | bytes 786440 | tf_op jit(solution)/shard_map/ppermute | solution.py:20
  147.0 18.2 %collective-permute-start.10 = (bf16[256,512]{1,0:T(8,128)(2,1)S(1)}, bf16[256,512]{1,0:T(8,128)(2,1)S(1)}, u32[]{:S(2)}, u32[]{:S(2)}) collective-permute-start(bf16[256,512]{1,0:T(8,128)(2,1)S(1)} %get-tuple-element.77), channel_id=1, source_target_pairs={{0,16},{16,32},{32,48},{48,0},{1,17},{17,33},{33,49},{49,1},{2,18}... | collective-permute-start | bytes 786440 | tf_op jit(solution)/shard_map/ppermute | solution.py:20
  148.9 16.5 %collective-permute-start.11 = (bf16[256,512]{1,0:T(8,128)(2,1)S(1)}, bf16[256,512]{1,0:T(8,128)(2,1)S(1)}, u32[]{:S(2)}, u32[]{:S(2)}) collective-permute-start(bf16[256,512]{1,0:T(8,128)(2,1)S(1)} %get-tuple-element.78), channel_id=1, source_target_pairs={{0,48},{16,0},{32,16},{48,32},{1,49},{17,1},{33,17},{49,33},{2,50}... | collective-permute-start | bytes 786440 | tf_op jit(solution)/shard_map/ppermute | solution.py:20
  154.7 15.0 %collective-permute-start.5 = (bf16[256,128]{1,0:T(8,128)(2,1)S(1)}, bf16[256,128]{1,0:T(8,128)(2,1)S(1)}, u32[]{:S(2)}, u32[]{:S(2)}) collective-permute-start(bf16[256,128]{1,0:T(8,128)(2,1)S(1)} %get-tuple-element.79), channel_id=1, source_target_pairs={{0,16},{16,32},{32,48},{48,0},{1,17},{17,33},{33,49},{49,1},{2,18}... | collective-permute-start | bytes 196616 | tf_op jit(solution)/shard_map/ppermute | solution.py:20
  156.6 13.1 %collective-permute-start.7 = (bf16[256,128]{1,0:T(8,128)(2,1)S(1)}, bf16[256,128]{1,0:T(8,128)(2,1)S(1)}, u32[]{:S(2)}, u32[]{:S(2)}) collective-permute-start(bf16[256,128]{1,0:T(8,128)(2,1)S(1)} %get-tuple-element.80), channel_id=1, source_target_pairs={{0,32},{16,48},{32,0},{48,16},{1,33},{17,49},{33,1},{49,17},{2,34}... | collective-permute-start | bytes 196616 | tf_op jit(solution)/shard_map/ppermute | solution.py:20
  163.2 6.4 %collective-permute-start.6 = (bf16[256,128]{1,0:T(8,128)(2,1)S(1)}, bf16[256,128]{1,0:T(8,128)(2,1)S(1)}, u32[]{:S(2)}, u32[]{:S(2)}) collective-permute-start(bf16[256,128]{1,0:T(8,128)(2,1)S(1)} %get-tuple-element.81), channel_id=1, source_target_pairs={{0,48},{16,0},{32,16},{48,32},{1,49},{17,1},{33,17},{49,33},{2,50}... | collective-permute-start | bytes 196616 | tf_op jit(solution)/shard_map/ppermute | solution.py:20
  166.2 15.6 %all-to-all-start.5 = ((bf16[8,32,512]{2,1,0:T(8,128)(2,1)}), bf16[8,32,512]{2,1,0:T(8,128)(2,1)S(1)}, u32[]{:S(2)}, u32[]{:S(2)}) async-start(bf16[8,32,512]{2,1,0:T(8,128)(2,1)} %bitcast.35), calls=%async_computation.5 | async-start | bytes 524288 | tf_op jit(solution)/shard_map/all_to_all | solution.py:24

commit v6 on v5

--- a/solution.py
+++ b/solution.py
@@ -81,11 +81,10 @@
     w_theirs = jnp.where(core == 0, w_odd, w_even)
 
     half = nx * src // 2
-    mine = [b[: src // 2] for b in blocks] + [b[src // 2 : src] for b in blocks] + [target_all]
+    mine = [b[: src // 2] for b in blocks] + [b[src // 2 : src] for b in blocks]
     mine = row_major(jnp.concatenate(mine, axis=0))
     mine, w_mine, w_theirs = lax.optimization_barrier((mine, w_mine, w_theirs))
     theirs = shifted(mine, "c", 1)
-    target_other = theirs[2 * half :]
     key_one, value_one = mine[:half], mine[half : 2 * half]
     key_two, value_two = theirs[:half], theirs[half : 2 * half]
 
@@ -119,18 +118,20 @@
     sent = (query_t * share[None]).astype(BF16).reshape(nx, part, nz, rows).transpose(2, 0, 1, 3)
     sent = sent.reshape(nz * nx, part, rows)
     got = exchanged(sent, ("z", "x")).reshape(nz, nx, part, rows)
+
+    query_share, grad_share, _ = lax.optimization_barrier(
+        ((query_all * share[:, None]).astype(BF16), (grad_all * share[:, None]).astype(BF16), sent)
+    )
+
+    def sums_of(grad, weight):
+        return jnp.concatenate([dot(grad, query_share, 1, 0), dot(weight, grad_share, 1, 0)], axis=1)
+
+    swap = row_major(sums_of(grad_two, weight_two).astype(BF16))
+    swap = shifted(swap, "c", 1)
+    mine = row_major((sums_of(grad_one, weight_one) + swap.astype(F32)).astype(BF16))
+    got, mine = lax.optimization_barrier((got, mine))
     part_t = got.astype(F32).sum(axis=0)
     part_t = part_t.transpose(1, 0, 2).reshape(part, nx * rows).astype(BF16)
-
-    query_share, grad_share, _ = lax.optimization_barrier(
-        ((query_all * share[:, None]).astype(BF16), (grad_all * share[:, None]).astype(BF16), sent)
-    )
-
-    def sums_of(grad, weight):
-        return jnp.concatenate([dot(grad, query_share, 1, 0), dot(weight, grad_share, 1, 0)], axis=1)
-
-    swap = shifted(row_major(sums_of(grad_two, weight_two).astype(BF16)), "c", 1)
-    mine = row_major((sums_of(grad_one, weight_one) + swap.astype(F32)).astype(BF16))
     own, left, right, far = (mine[src // 2 * k : src // 2 * (k + 1)] for k in range(nx))
     own = own.astype(F32)
     moved = [shifted(block, "x", by) for block, by in ((far, 2), (right, 1), (left, -1))]
@@ -141,6 +142,8 @@
     def by_core(mine, theirs):
         return jnp.where(core == 0, jnp.stack([mine, theirs]), jnp.stack([theirs, mine]))
 
+    target_all, _ = lax.optimization_barrier((target_all, sent))
+    target_other = shifted(target_all, "c", 1)
     target_both = by_core(target_all.T, target_other.T).astype(F32)
     squares = jnp.sum(target_both * target_both, axis=(0, 1))
     high = lax.reduce_precision(squares, 8, 7)

time: 186 us -> 192 us (1.032)
  the two profiles are of different devices: /device:TPU:2 before, /device:TPU:1 now
where the time goes in v6:
time: 192 us; the launch traced here: 190 us
  starting transfers between devices  75.3 us (39%)
  waiting for transfers between devices  37.6 us (20%)
  local copies, waits for them, and re-layouts  26.6 us (14%)
  blocking collectives  22.3 us (12%)
  matrix products  14.4 us (8%)
  other arithmetic  12.5 us (7%)
    ppermute x13, starting transfers between devices, shifted(): return lax.ppermute(value, axis, [(i, (i + by) % n) for i in range(n)])  45.1 us
    all_to_all x5, waiting for transfers between devices, exchanged(): return lax.all_to_all(value, axis, split_axis=0, concat_axis=0, tiled=True)  34.7 us
    all_to_all x5, starting transfers between devices, exchanged(): return lax.all_to_all(value, axis, split_axis=0, concat_axis=0, tiled=True)  30.3 us
    all_to_all x1, blocking collectives, exchanged(): return lax.all_to_all(value, axis, split_axis=0, concat_axis=0, tiled=True)  22.3 us
    unnamed x36, local copies, waits for them, and re-layouts  14.7 us
    dot_general x13, matrix products, dot(): lax.dot_general(a, b, (((ca,), (cb,)), ((), ())), preferred_element_type=...  14.4 us
  transfers between devices with their start and end apart: 18, of which 6 were waited for; matrix products, arithmetic and copies ran while one was open for 17% of the time, Pallas kernels for 0%

profile of v6, /device:TPU:1, one launch (start us, length us, event | category | flops | bytes accessed | tf_op | source)
XLA Modules:
  0.0 190.3 jit_solution(10927837190339432075)
XLA Ops:
  0.6 1.0 constant_dynamic-slice_fusion
  1.7 1.6 pad_maximum_fusion.1
  3.2 3.9 %collective-permute-start = (bf16[640,256]{1,0:T(8,128)(2,1)}, bf16[640,256]{1,0:T(8,128)(2,1)}, u32[]{:S(2)}, u32[]{:S(2)}) collective-permute-start(bf16[640,256]{1,0:T(8,128)(2,1)} %pad_maximum_fusion.1), channel_id=1, source_target_pairs={{0,16},{16,32},{32,48},{48,0},{1,17},{17,33},{33,49},{49,1},{2,18}... | collective-permute-start | bytes 983048 | tf_op jit(solution)/shard_map/ppermute | solution.py:20
  7.2 4.4 %collective-permute-start.2 = (bf16[640,256]{1,0:T(8,128)(2,1)}, bf16[640,256]{1,0:T(8,128)(2,1)}, u32[]{:S(2)}, u32[]{:S(2)}) collective-permute-start(bf16[640,256]{1,0:T(8,128)(2,1)} %pad_maximum_fusion.1), channel_id=1, source_target_pairs={{0,32},{16,48},{32,0},{48,16},{1,33},{17,49},{33,1},{49,17},{2,34}... | collective-permute-start | bytes 983048 | tf_op jit(solution)/shard_map/ppermute | solution.py:20
  11.5 3.1 %collective-permute-start.1 = (bf16[640,256]{1,0:T(8,128)(2,1)}, bf16[640,256]{1,0:T(8,128)(2,1)}, u32[]{:S(2)}, u32[]{:S(2)}) collective-permute-start(bf16[640,256]{1,0:T(8,128)(2,1)} %pad_maximum_fusion.1), channel_id=1, source_target_pairs={{0,48},{16,0},{32,16},{48,32},{1,49},{17,1},{33,17},{49,33},{2,50}... | collective-permute-start | bytes 983048 | tf_op jit(solution)/shard_map/ppermute | solution.py:20
  14.6 1.0 multiply_reduce_fusion.2
  15.7 1.0 maximum_maximum_fusion
  16.7 1.1 broadcast_in_dim.19
  17.8 10.0 %all-to-all-start = ((bf16[8,136,512]{2,1,0:T(8,128)(2,1)}), bf16[8,136,512]{2,1,0:T(8,128)(2,1)S(1)}, u32[]{:S(2)}, u32[]{:S(2)}) async-start(bf16[8,136,512]{2,1,0:T(8,128)(2,1)} %broadcast_in_dim.19), calls=%async_computation | async-start | bytes 2228224 | tf_op jit(solution)/shard_map/all_to_all | solution.py:24
  27.8 3.3 %copy.170 = bf16[256,4096]{0,1:T(8,128)(2,1)S(1)} copy(bf16[256,4096]{1,0:T(8,128)(2,1)} %param.10) | data formatting | bytes 4194304 | tf_op args[2]
  32.0 0.9 slice_dynamic-update-slice_fusion.5
  32.9 0.9 slice_dynamic-update-slice_fusion.4
  33.8 0.9 slice_dynamic-update-slice_fusion.3
  34.8 0.9 slice_dynamic-update-slice_fusion.2
  35.7 0.9 slice_dynamic-update-slice_fusion.1
  36.6 0.9 slice_dynamic-update-slice_fusion
  37.5 3.7 %collective-permute-start.3 = (bf16[2048,256]{1,0:T(8,128)(2,1)S(1)}, bf16[2048,256]{1,0:T(8,128)(2,1)}, u32[]{:S(2)}, u32[]{:S(2)}) collective-permute-start(bf16[2048,256]{1,0:T(8,128)(2,1)S(1)} %slice_dynamic-update-slice_fusion), channel_id=1, source_target_pairs={{0,1},{1,0},{2,3},{3,2},{4,5},{5,4},{6,7},{7,6},{8,9},{9,8},{10,11... | collective-permute-start | bytes 3145736 | tf_op jit(solution)/shard_map/ppermute | solution.py:20
  43.5 14.9 %all-to-all-done = bf16[8,136,512]{2,1,0:T(8,128)(2,1)S(1)} async-done(((bf16[8,136,512]{2,1,0:T(8,128)(2,1)}), bf16[8,136,512]{2,1,0:T(8,128)(2,1)S(1)}, u32[]{:S(2)}, u32[]{:S(2)}) %all-to-all-start) | async-done | bytes 1114144 | tf_op jit(solution)/shard_map/all_to_all | solution.py:24
  59.3 1.8 multiply_reduce_fusion
  61.1 3.1 %fusion.2 = (f32[1024]{0:T(1024)S(1)}, f32[1024]{0:T(1024)S(1)}, bf16[1024,1024]{1,0:T(8,128)(2,1)}, bf16[1024,1024]{1,0:T(8,128)(2,1)}) fusion(f32[1024,1024]{1,0:T(8,128)S(1)} %get-tuple-element.100, f32[1024]{0:T(1024)S(1)} %max.18, f32[1024,1024]{1,0:T(8,128)S(1)} %get-tuple-element.98), kind=kLoop, calls=%fused_computation.8 | loop fusion | flops 8386560 | bytes 12595200 | tf_op jit(solution)/shard_map/reduce_sum | solution.py:100
  64.9 4.0 %all-to-all-start.1 = ((f32[8,16,128]{2,1,0:T(8,128)}), f32[8,16,128]{2,1,0:T(8,128)}, u32[]{:S(2)}, u32[]{:S(2)}) async-start(f32[8,16,128]{2,1,0:T(8,128)} %broadcast_in_dim.20), calls=%async_computation.1 | async-start | bytes 131072 | tf_op jit(solution)/shard_map/all_to_all | solution.py:24
  68.9 2.4 %multiply_convert_fusion.1 = bf16[1024,1024]{1,0:T(8,128)(2,1)S(1)} fusion(bf16[1024,1024]{1,0:T(8,128)(2,1)} %get-tuple-element.21, bf16[1024,256]{1,0:T(8,128)(2,1)S(1)} %bitcast.106, f32[1024]{0:T(1024)S(1)} %bitcast.127, bf16[2048,256]{1,0:T(8,128)(2,1)S(1)} %slice_dynamic-update-slice_fusion), kind=kOutput, calls=%fused_computation.1 | convolution fusion | flops 542113792 | bytes 5246976 | tf_op jit(solution)/shard_map/dot_general | solution.py:33
  72.0 1.6 copy-done.1
  73.7 1.9 multiply_convert_fusion
  75.6 1.3 copy-done.5
  76.9 1.8 convolution_add_fusion
  80.3 1.0 copy.173
  84.3 1.0 pad_maximum_fusion
  85.4 2.4 %collective-permute-start.4 = (bf16[1024,512]{1,0:T(8,128)(2,1)}, bf16[1024,512]{1,0:T(8,128)(2,1)}, u32[]{:S(2)}, u32[]{:S(2)}) collective-permute-start(bf16[1024,512]{1,0:T(8,128)(2,1)} %pad_maximum_fusion), channel_id=1, source_target_pairs={{0,1},{1,0},{2,3},{3,2},{4,5},{5,4},{6,7},{7,6},{8,9},{9,8},{10,11... | collective-permute-start | bytes 3145736 | tf_op jit(solution)/shard_map/ppermute | solution.py:20
  88.8 7.2 %all-to-all-start.2 = ((bf16[32,64,128]{2,1,0:T(8,128)(2,1)}), bf16[32,64,128]{2,1,0:T(8,128)(2,1)S(1)}, u32[]{:S(2)}, u32[]{:S(2)}) async-start(bf16[32,64,128]{2,1,0:T(8,128)(2,1)} %bitcast.15), calls=%async_computation.2 | async-start | bytes 1048576 | tf_op jit(solution)/shard_map/all_to_all | solution.py:24
  96.1 1.9 %fusion.26 = f32[1024,256]{1,0:T(8,128)S(1)} fusion(bf16[1024,1024]{1,0:T(8,128)(2,1)S(1)} %copy-done, bf16[1024,256]{1,0:T(8,128)(2,1)} %copy-done.9), kind=kOutput, calls=%fused_computation.89 | convolution fusion | flops 536870912 | bytes 3670016 | tf_op jit(solution)/shard_map/dot_general | solution.py:33
  98.0 2.2 %collective-permute-start.5 = (bf16[512,256]{0,1:T(8,128)(2,1)S(1)}, bf16[512,256]{0,1:T(8,128)(2,1)S(1)}, u32[]{:S(2)}, u32[]{:S(2)}) collective-permute-start(bf16[512,256]{0,1:T(8,128)(2,1)S(1)} %constant_dynamic-update-slice_fusion.2), channel_id=1, source_target_pairs={{0,1},{1,0},{2,3},{3,2},{4,5},{5,4},{6,7},{7,6},{8,9},{9,8},{10,11... | collective-permute-start | bytes 786440 | tf_op jit(solution)/shard_map/ppermute | solution.py:20
  101.6 1.5 fusion.4
  103.1 9.7 %all-to-all-done.2 = bf16[32,64,128]{2,1,0:T(8,128)(2,1)S(1)} async-done(((bf16[32,64,128]{2,1,0:T(8,128)(2,1)}), bf16[32,64,128]{2,1,0:T(8,128)(2,1)S(1)}, u32[]{:S(2)}, u32[]{:S(2)}) %all-to-all-start.2) | async-done | bytes 524320 | tf_op jit(solution)/shard_map/all_to_all | solution.py:24
  113.0 22.3 %all_to_all.30 = bf16[8,72,512]{2,1,0:T(8,128)(2,1)S(1)} all-to-all(bf16[8,72,512]{2,1,0:T(8,128)(2,1)S(1)} %broadcast_in_dim.23), channel_id=1, replica_groups=mesh['z'=8,'x'=4,'y'=8,'c'=2] {'y'}, dimensions={0} | all-to-all | bytes 1179648 | tf_op jit(solution)/shard_map/all_to_all | solution.py:24
  136.9 6.2 %collective-permute-start.6 = (bf16[512,512]{1,0:T(8,128)(2,1)S(1)}, bf16[512,512]{1,0:T(8,128)(2,1)S(1)}, u32[]{:S(2)}, u32[]{:S(2)}) collective-permute-start(bf16[512,512]{1,0:T(8,128)(2,1)S(1)} %bitcast.96), channel_id=1, source_target_pairs={{0,1},{1,0},{2,3},{3,2},{4,5},{5,4},{6,7},{7,6},{8,9},{9,8},{10,11... | collective-permute-start | bytes 1572872 | tf_op jit(solution)/shard_map/ppermute | solution.py:20
  143.2 5.6 %all-to-all-start.4 = ((bf16[64,8,512]{2,1,0:T(8,128)(2,1)}), bf16[64,8,512]{2,1,0:T(8,128)(2,1)S(1)}, u32[]{:S(2)}, u32[]{:S(2)}) async-start(bf16[64,8,512]{2,1,0:T(8,128)(2,1)} %bitcast.30), calls=%async_computation.4 | async-start | bytes 1048576 | tf_op jit(solution)/shard_map/all_to_all | solution.py:24
  148.9 4.8 %collective-permute-start.10 = (bf16[256,512]{1,0:T(8,128)(2,1)S(1)}, bf16[256,512]{1,0:T(8,128)(2,1)S(1)}, u32[]{:S(2)}, u32[]{:S(2)}) collective-permute-start(bf16[256,512]{1,0:T(8,128)(2,1)S(1)} %get-tuple-element.82), channel_id=1, source_target_pairs={{0,32},{16,48},{32,0},{48,16},{1,33},{17,49},{33,1},{49,17},{2,34}... | collective-permute-start | bytes 786440 | tf_op jit(solution)/shard_map/ppermute | solution.py:20
  153.7 2.8 %collective-permute-start.12 = (bf16[256,512]{1,0:T(8,128)(2,1)S(1)}, bf16[256,512]{1,0:T(8,128)(2,1)S(1)}, u32[]{:S(2)}, u32[]{:S(2)}) collective-permute-start(bf16[256,512]{1,0:T(8,128)(2,1)S(1)} %get-tuple-element.83), channel_id=1, source_target_pairs={{0,48},{16,0},{32,16},{48,32},{1,49},{17,1},{33,17},{49,33},{2,50}... | collective-permute-start | bytes 786440 | tf_op jit(solution)/shard_map/ppermute | solution.py:20
  156.5 2.5 %collective-permute-start.11 = (bf16[256,512]{1,0:T(8,128)(2,1)S(1)}, bf16[256,512]{1,0:T(8,128)(2,1)S(1)}, u32[]{:S(2)}, u32[]{:S(2)}) collective-permute-start(bf16[256,512]{1,0:T(8,128)(2,1)S(1)} %get-tuple-element.84), channel_id=1, source_target_pairs={{0,16},{16,32},{32,48},{48,0},{1,17},{17,33},{33,49},{49,1},{2,18}... | collective-permute-start | bytes 786440 | tf_op jit(solution)/shard_map/ppermute | solution.py:20
  159.7 2.2 %collective-permute-start.7 = (bf16[256,128]{1,0:T(8,128)(2,1)S(1)}, bf16[256,128]{1,0:T(8,128)(2,1)S(1)}, u32[]{:S(2)}, u32[]{:S(2)}) collective-permute-start(bf16[256,128]{1,0:T(8,128)(2,1)S(1)} %get-tuple-element.85), channel_id=1, source_target_pairs={{0,16},{16,32},{32,48},{48,0},{1,17},{17,33},{33,49},{49,1},{2,18}... | collective-permute-start | bytes 196616 | tf_op jit(solution)/shard_map/ppermute | solution.py:20
  161.9 4.9 %collective-permute-start.9 = (bf16[256,128]{1,0:T(8,128)(2,1)S(1)}, bf16[256,128]{1,0:T(8,128)(2,1)S(1)}, u32[]{:S(2)}, u32[]{:S(2)}) collective-permute-start(bf16[256,128]{1,0:T(8,128)(2,1)S(1)} %get-tuple-element.86), channel_id=1, source_target_pairs={{0,32},{16,48},{32,0},{48,16},{1,33},{17,49},{33,1},{49,17},{2,34}... | collective-permute-start | bytes 196616 | tf_op jit(solution)/shard_map/ppermute | solution.py:20
  166.8 2.1 %collective-permute-start.8 = (bf16[256,128]{1,0:T(8,128)(2,1)S(1)}, bf16[256,128]{1,0:T(8,128)(2,1)S(1)}, u32[]{:S(2)}, u32[]{:S(2)}) collective-permute-start(bf16[256,128]{1,0:T(8,128)(2,1)S(1)} %get-tuple-element.87), channel_id=1, source_target_pairs={{0,48},{16,0},{32,16},{48,32},{1,49},{17,1},{33,17},{49,33},{2,50}... | collective-permute-start | bytes 196616 | tf_op jit(solution)/shard_map/ppermute | solution.py:20
  168.9 1.5 collective-permute-done.12
  170.4 0.9 collective-permute-done.11
  172.2 3.4 %all-to-all-start.5 = ((bf16[8,32,512]{2,1,0:T(8,128)(2,1)}), bf16[8,32,512]{2,1,0:T(8,128)(2,1)S(1)}, u32[]{:S(2)}, u32[]{:S(2)}) async-start(bf16[8,32,512]{2,1,0:T(8,128)(2,1)} %bitcast.35), calls=%async_computation.5 | async-start | bytes 524288 | tf_op jit(solution)/shard_map/all_to_all | solution.py:24
  176.9 0.9 reshape.185
  177.8 10.1 %all-to-all-done.5 = bf16[8,32,512]{2,1,0:T(8,128)(2,1)S(1)} async-done(((bf16[8,32,512]{2,1,0:T(8,128)(2,1)}), bf16[8,32,512]{2,1,0:T(8,128)(2,1)S(1)}, u32[]{:S(2)}, u32[]{:S(2)}) %all-to-all-start.5) | async-done | bytes 262176 | tf_op jit(solution)/shard_map/all_to_all | solution.py:24
  (111 shorter events, 19.5 us)
Async XLA Ops:
  3.2 28.7 %collective-permute-start = (bf16[640,256]{1,0:T(8,128)(2,1)}, bf16[640,256]{1,0:T(8,128)(2,1)}, u32[]{:S(2)}, u32[]{:S(2)}) collective-permute-start(bf16[640,256]{1,0:T(8,128)(2,1)} %pad_maximum_fusion.1), channel_id=1, source_target_pairs={{0,16},{16,32},{32,48},{48,0},{1,17},{17,33},{33,49},{49,1},{2,18}... | collective-permute-start | bytes 983048 | tf_op jit(solution)/shard_map/ppermute | solution.py:20
  7.2 26.6 %collective-permute-start.2 = (bf16[640,256]{1,0:T(8,128)(2,1)}, bf16[640,256]{1,0:T(8,128)(2,1)}, u32[]{:S(2)}, u32[]{:S(2)}) collective-permute-start(bf16[640,256]{1,0:T(8,128)(2,1)} %pad_maximum_fusion.1), channel_id=1, source_target_pairs={{0,32},{16,48},{32,0},{48,16},{1,33},{17,49},{33,1},{49,17},{2,34}... | collective-permute-start | bytes 983048 | tf_op jit(solution)/shard_map/ppermute | solution.py:20
  11.5 21.3 %collective-permute-start.1 = (bf16[640,256]{1,0:T(8,128)(2,1)}, bf16[640,256]{1,0:T(8,128)(2,1)}, u32[]{:S(2)}, u32[]{:S(2)}) collective-permute-start(bf16[640,256]{1,0:T(8,128)(2,1)} %pad_maximum_fusion.1), channel_id=1, source_target_pairs={{0,48},{16,0},{32,16},{48,32},{1,49},{17,1},{33,17},{49,33},{2,50}... | collective-permute-start | bytes 983048 | tf_op jit(solution)/shard_map/ppermute | solution.py:20
  17.8 40.6 %all-to-all-start = ((bf16[8,136,512]{2,1,0:T(8,128)(2,1)}), bf16[8,136,512]{2,1,0:T(8,128)(2,1)S(1)}, u32[]{:S(2)}, u32[]{:S(2)}) async-start(bf16[8,136,512]{2,1,0:T(8,128)(2,1)} %broadcast_in_dim.19), calls=%async_computation | async-start | bytes 2228224 | tf_op jit(solution)/shard_map/all_to_all | solution.py:24
  31.1 10.2 %copy-start.10 = (bf16[128,256]{1,0:T(8,128)(2,1)S(1)}, bf16[128,256]{1,0:T(8,128)(2,1)}, u32[]{:S(2)}) copy-start(bf16[128,256]{1,0:T(8,128)(2,1)} %param.8) | copy-start | bytes 196612
  37.5 21.8 %collective-permute-start.3 = (bf16[2048,256]{1,0:T(8,128)(2,1)S(1)}, bf16[2048,256]{1,0:T(8,128)(2,1)}, u32[]{:S(2)}, u32[]{:S(2)}) collective-permute-start(bf16[2048,256]{1,0:T(8,128)(2,1)S(1)} %slice_dynamic-update-slice_fusion), channel_id=1, source_target_pairs={{0,1},{1,0},{2,3},{3,2},{4,5},{5,4},{6,7},{7,6},{8,9},{9,8},{10,11... | collective-permute-start | bytes 3145736 | tf_op jit(solution)/shard_map/ppermute | solution.py:20
  64.9 13.8 %all-to-all-start.1 = ((f32[8,16,128]{2,1,0:T(8,128)}), f32[8,16,128]{2,1,0:T(8,128)}, u32[]{:S(2)}, u32[]{:S(2)}) async-start(f32[8,16,128]{2,1,0:T(8,128)} %broadcast_in_dim.20), calls=%async_computation.1 | async-start | bytes 131072 | tf_op jit(solution)/shard_map/all_to_all | solution.py:24
  71.3 4.2 %copy-start.3 = (bf16[1024,1024]{1,0:T(8,128)(2,1)}, bf16[1024,1024]{1,0:T(8,128)(2,1)S(1)}, u32[]{:S(2)}) copy-start(bf16[1024,1024]{1,0:T(8,128)(2,1)S(1)} %multiply_convert_fusion.1) | copy-start | bytes 6291460
  71.3 2.3 %copy-start.1 = (bf16[1024,1024]{1,0:T(8,128)(2,1)S(1)}, bf16[1024,1024]{1,0:T(8,128)(2,1)}, u32[]{:S(2)}) copy-start(bf16[1024,1024]{1,0:T(8,128)(2,1)} %get-tuple-element.22) | copy-start | bytes 6291460
  75.5 1.4 copy-start.5
  80.0 4.3 %copy-start.9 = (bf16[1024,256]{1,0:T(8,128)(2,1)}, bf16[1024,256]{1,0:T(8,128)(2,1)S(1)}, u32[]{:S(2)}) copy-start(bf16[1024,256]{1,0:T(8,128)(2,1)S(1)} %get-tuple-element.27) | copy-start | bytes 1572868
  80.0 2.0 %copy-start.2 = (bf16[1024,1024]{1,0:T(8,128)(2,1)S(1)}, bf16[1024,1024]{1,0:T(8,128)(2,1)}, u32[]{:S(2)}) copy-start(bf16[1024,1024]{1,0:T(8,128)(2,1)} %get-tuple-element.22) | copy-start | bytes 6291460
  82.0 1.6 copy-start.6
  84.3 11.7 %copy-start = (bf16[1024,1024]{1,0:T(8,128)(2,1)S(1)}, bf16[1024,1024]{1,0:T(8,128)(2,1)}, u32[]{:S(2)}) copy-start(bf16[1024,1024]{1,0:T(8,128)(2,1)} %get-tuple-element.21) | copy-start | bytes 6291460
  85.4 16.2 %collective-permute-start.4 = (bf16[1024,512]{1,0:T(8,128)(2,1)}, bf16[1024,512]{1,0:T(8,128)(2,1)}, u32[]{:S(2)}, u32[]{:S(2)}) collective-permute-start(bf16[1024,512]{1,0:T(8,128)(2,1)} %pad_maximum_fusion), channel_id=1, source_target_pairs={{0,1},{1,0},{2,3},{3,2},{4,5},{5,4},{6,7},{7,6},{8,9},{9,8},{10,11... | collective-permute-start | bytes 3145736 | tf_op jit(solution)/shard_map/ppermute | solution.py:20
  88.8 24.0 %all-to-all-start.2 = ((bf16[32,64,128]{2,1,0:T(8,128)(2,1)}), bf16[32,64,128]{2,1,0:T(8,128)(2,1)S(1)}, u32[]{:S(2)}, u32[]{:S(2)}) async-start(bf16[32,64,128]{2,1,0:T(8,128)(2,1)} %bitcast.15), calls=%async_computation.2 | async-start | bytes 1048576 | tf_op jit(solution)/shard_map/all_to_all | solution.py:24
  96.0 4.1 %copy-start.4 = (bf16[1024,1024]{1,0:T(8,128)(2,1)S(1)}, bf16[1024,1024]{1,0:T(8,128)(2,1)}, u32[]{:S(2)}) copy-start(bf16[1024,1024]{1,0:T(8,128)(2,1)} %copy-done.3) | copy-start | bytes 6291460
  98.0 3.4 %collective-permute-start.5 = (bf16[512,256]{0,1:T(8,128)(2,1)S(1)}, bf16[512,256]{0,1:T(8,128)(2,1)S(1)}, u32[]{:S(2)}, u32[]{:S(2)}) collective-permute-start(bf16[512,256]{0,1:T(8,128)(2,1)S(1)} %constant_dynamic-update-slice_fusion.2), channel_id=1, source_target_pairs={{0,1},{1,0},{2,3},{3,2},{4,5},{5,4},{6,7},{7,6},{8,9},{9,8},{10,11... | collective-permute-start | bytes 786440 | tf_op jit(solution)/shard_map/ppermute | solution.py:20
  135.5 7.6 %copy-start.11 = (f32[256]{0:T(256)S(1)}, f32[256]{0:T(256)}, u32[]{:S(2)}) copy-start(f32[256]{0:T(256)} %param.9) | copy-start | bytes 3076
  136.1 22.9 %copy-start.8 = (bf16[256,8,1,1,64]{0,4,3,2,1:T(8,128)(2,1)S(1)}, bf16[256,8,1,1,64]{0,4,3,2,1:T(8,128)(2,1)}, u32[]{:S(2)}) copy-start(bf16[256,8,1,1,64]{0,4,3,2,1:T(8,128)(2,1)} %get-tuple-element.79) | copy-start | bytes 786436
  136.9 22.4 %copy-start.7 = (bf16[256,8,1,1,64]{0,4,3,2,1:T(8,128)(2,1)S(1)}, bf16[256,8,1,1,64]{0,4,3,2,1:T(8,128)(2,1)}, u32[]{:S(2)}) copy-start(bf16[256,8,1,1,64]{0,4,3,2,1:T(8,128)(2,1)} %get-tuple-element.78) | copy-start | bytes 786436
  136.9 22.4 %collective-permute-start.6 = (bf16[512,512]{1,0:T(8,128)(2,1)S(1)}, bf16[512,512]{1,0:T(8,128)(2,1)S(1)}, u32[]{:S(2)}, u32[]{:S(2)}) collective-permute-start(bf16[512,512]{1,0:T(8,128)(2,1)S(1)} %bitcast.96), channel_id=1, source_target_pairs={{0,1},{1,0},{2,3},{3,2},{4,5},{5,4},{6,7},{7,6},{8,9},{9,8},{10,11... | collective-permute-start | bytes 1572872 | tf_op jit(solution)/shard_map/ppermute | solution.py:20
  143.2 29.0 %all-to-all-start.4 = ((bf16[64,8,512]{2,1,0:T(8,128)(2,1)}), bf16[64,8,512]{2,1,0:T(8,128)(2,1)S(1)}, u32[]{:S(2)}, u32[]{:S(2)}) async-start(bf16[64,8,512]{2,1,0:T(8,128)(2,1)} %bitcast.30), calls=%async_computation.4 | async-start | bytes 1048576 | tf_op jit(solution)/shard_map/all_to_all | solution.py:24
  148.9 17.9 %collective-permute-start.10 = (bf16[256,512]{1,0:T(8,128)(2,1)S(1)}, bf16[256,512]{1,0:T(8,128)(2,1)S(1)}, u32[]{:S(2)}, u32[]{:S(2)}) collective-permute-start(bf16[256,512]{1,0:T(8,128)(2,1)S(1)} %get-tuple-element.82), channel_id=1, source_target_pairs={{0,32},{16,48},{32,0},{48,16},{1,33},{17,49},{33,1},{49,17},{2,34}... | collective-permute-start | bytes 786440 | tf_op jit(solution)/shard_map/ppermute | solution.py:20
  153.7 16.8 %collective-permute-start.12 = (bf16[256,512]{1,0:T(8,128)(2,1)S(1)}, bf16[256,512]{1,0:T(8,128)(2,1)S(1)}, u32[]{:S(2)}, u32[]{:S(2)}) collective-permute-start(bf16[256,512]{1,0:T(8,128)(2,1)S(1)} %get-tuple-element.83), channel_id=1, source_target_pairs={{0,48},{16,0},{32,16},{48,32},{1,49},{17,1},{33,17},{49,33},{2,50}... | collective-permute-start | bytes 786440 | tf_op jit(solution)/shard_map/ppermute | solution.py:20
  156.5 14.9 %collective-permute-start.11 = (bf16[256,512]{1,0:T(8,128)(2,1)S(1)}, bf16[256,512]{1,0:T(8,128)(2,1)S(1)}, u32[]{:S(2)}, u32[]{:S(2)}) collective-permute-start(bf16[256,512]{1,0:T(8,128)(2,1)S(1)} %get-tuple-element.84), channel_id=1, source_target_pairs={{0,16},{16,32},{32,48},{48,0},{1,17},{17,33},{33,49},{49,1},{2,18}... | collective-permute-start | bytes 786440 | tf_op jit(solution)/shard_map/ppermute | solution.py:20
  159.7 15.9 %collective-permute-start.7 = (bf16[256,128]{1,0:T(8,128)(2,1)S(1)}, bf16[256,128]{1,0:T(8,128)(2,1)S(1)}, u32[]{:S(2)}, u32[]{:S(2)}) collective-permute-start(bf16[256,128]{1,0:T(8,128)(2,1)S(1)} %get-tuple-element.85), channel_id=1, source_target_pairs={{0,16},{16,32},{32,48},{48,0},{1,17},{17,33},{33,49},{49,1},{2,18}... | collective-permute-start | bytes 196616 | tf_op jit(solution)/shard_map/ppermute | solution.py:20
  161.9 13.7 %collective-permute-start.9 = (bf16[256,128]{1,0:T(8,128)(2,1)S(1)}, bf16[256,128]{1,0:T(8,128)(2,1)S(1)}, u32[]{:S(2)}, u32[]{:S(2)}) collective-permute-start(bf16[256,128]{1,0:T(8,128)(2,1)S(1)} %get-tuple-element.86), channel_id=1, source_target_pairs={{0,32},{16,48},{32,0},{48,16},{1,33},{17,49},{33,1},{49,17},{2,34}... | collective-permute-start | bytes 196616 | tf_op jit(solution)/shard_map/ppermute | solution.py:20
  166.8 8.8 %collective-permute-start.8 = (bf16[256,128]{1,0:T(8,128)(2,1)S(1)}, bf16[256,128]{1,0:T(8,128)(2,1)S(1)}, u32[]{:S(2)}, u32[]{:S(2)}) collective-permute-start(bf16[256,128]{1,0:T(8,128)(2,1)S(1)} %get-tuple-element.87), channel_id=1, source_target_pairs={{0,48},{16,0},{32,16},{48,32},{1,49},{17,1},{33,17},{49,33},{2,50}... | collective-permute-start | bytes 196616 | tf_op jit(solution)/shard_map/ppermute | solution.py:20
  172.2 15.6 %all-to-all-start.5 = ((bf16[8,32,512]{2,1,0:T(8,128)(2,1)}), bf16[8,32,512]{2,1,0:T(8,128)(2,1)S(1)}, u32[]{:S(2)}, u32[]{:S(2)}) async-start(bf16[8,32,512]{2,1,0:T(8,128)(2,1)} %bitcast.35), calls=%async_computation.5 | async-start | bytes 524288 | tf_op jit(solution)/shard_map/all_to_all | solution.py:24

commit v7 on v6

--- a/solution.py
+++ b/solution.py
@@ -101,7 +101,7 @@
     weight_one, weight_two, total = lax.optimization_barrier(
         (weight_one.astype(BF16), weight_two.astype(BF16), total)
     )
-    stats = told_all(jnp.concatenate([peak, total]).reshape(2 * nz, rows), "z").reshape(nz, 2, n_rows)
+    stats = told_all(jnp.concatenate([peak, total]).reshape(2 * nz, rows), "z").reshape(nz, 2 * nz, rows)
 
     def grads_of(weight, value):
         product = dot(value, grad_all, 1, 1)
@@ -111,17 +111,18 @@
     grad_two = grads_of(weight_two, value_two)
     query_t = dot(key_one, grad_one, 0, 0) + dot(key_two, grad_two, 0, 0)
     query_t, stats = lax.optimization_barrier((query_t, stats))
-    top = jnp.max(stats[:, 0], axis=0)
-    log_totals = top + jnp.log(jnp.sum(stats[:, 1] * jnp.exp(stats[:, 0] - top[None]), axis=0))
+    peaks, totals = stats[:, :nz], stats[:, nz:]
+    top = jnp.max(peaks, axis=0)
+    log_totals = (top + jnp.log(jnp.sum(totals * jnp.exp(peaks - top[None]), axis=0))).reshape(n_rows)
     share = jnp.exp(peak - log_totals)
 
     sent = (query_t * share[None]).astype(BF16).reshape(nx, part, nz, rows).transpose(2, 0, 1, 3)
     sent = sent.reshape(nz * nx, part, rows)
     got = exchanged(sent, ("z", "x")).reshape(nz, nx, part, rows)
 
-    query_share, grad_share, _ = lax.optimization_barrier(
-        ((query_all * share[:, None]).astype(BF16), (grad_all * share[:, None]).astype(BF16), sent)
-    )
+    share, _ = lax.optimization_barrier((share, sent))
+    query_share = (query_all * share[:, None]).astype(BF16)
+    grad_share = (grad_all * share[:, None]).astype(BF16)
 
     def sums_of(grad, weight):
         return jnp.concatenate([dot(grad, query_share, 1, 0), dot(weight, grad_share, 1, 0)], axis=1)

time: 192 us -> 189 us (0.984)
    unnamed x36 -> x32, local copies, waits for them, and re-layouts: 14.7 us -> 14.3 us
where the time goes in v7:
time: 189 us; the launch traced here: 187 us
  starting transfers between devices  74.7 us (40%)
  waiting for transfers between devices  36.8 us (19%)
  local copies, waits for them, and re-layouts  25.3 us (13%)
  blocking collectives  22.3 us (12%)
  matrix products  15.4 us (8%)
  other arithmetic  11.2 us (6%)
    ppermute x13, starting transfers between devices, shifted(): return lax.ppermute(value, axis, [(i, (i + by) % n) for i in range(n)])  45.1 us
    all_to_all x5, waiting for transfers between devices, exchanged(): return lax.all_to_all(value, axis, split_axis=0, concat_axis=0, tiled=True)  34 us
    all_to_all x5, starting transfers between devices, exchanged(): return lax.all_to_all(value, axis, split_axis=0, concat_axis=0, tiled=True)  29.7 us
    all_to_all x1, blocking collectives, exchanged(): return lax.all_to_all(value, axis, split_axis=0, concat_axis=0, tiled=True)  22.3 us
    dot_general x13, matrix products, dot(): lax.dot_general(a, b, (((ca,), (cb,)), ((), ())), preferred_element_type=...  15.4 us
    unnamed x32, local copies, waits for them, and re-layouts  14.3 us
  transfers between devices with their start and end apart: 18, of which 6 were waited for; matrix products, arithmetic and copies ran while one was open for 17% of the time, Pallas kernels for 0%

profile of v7, /device:TPU:1, one launch (start us, length us, event | category | flops | bytes accessed | tf_op | source)
XLA Modules:
  0.0 187.3 jit_solution(4418587392913599522)
XLA Ops:
  0.6 1.0 constant_dynamic-slice_fusion
  1.7 1.6 pad_maximum_fusion.1
  3.2 3.9 %collective-permute-start = (bf16[640,256]{1,0:T(8,128)(2,1)}, bf16[640,256]{1,0:T(8,128)(2,1)}, u32[]{:S(2)}, u32[]{:S(2)}) collective-permute-start(bf16[640,256]{1,0:T(8,128)(2,1)} %pad_maximum_fusion.1), channel_id=1, source_target_pairs={{0,16},{16,32},{32,48},{48,0},{1,17},{17,33},{33,49},{49,1},{2,18}... | collective-permute-start | bytes 983048 | tf_op jit(solution)/shard_map/ppermute | solution.py:20
  7.2 4.4 %collective-permute-start.2 = (bf16[640,256]{1,0:T(8,128)(2,1)}, bf16[640,256]{1,0:T(8,128)(2,1)}, u32[]{:S(2)}, u32[]{:S(2)}) collective-permute-start(bf16[640,256]{1,0:T(8,128)(2,1)} %pad_maximum_fusion.1), channel_id=1, source_target_pairs={{0,32},{16,48},{32,0},{48,16},{1,33},{17,49},{33,1},{49,17},{2,34}... | collective-permute-start | bytes 983048 | tf_op jit(solution)/shard_map/ppermute | solution.py:20
  11.5 3.1 %collective-permute-start.1 = (bf16[640,256]{1,0:T(8,128)(2,1)}, bf16[640,256]{1,0:T(8,128)(2,1)}, u32[]{:S(2)}, u32[]{:S(2)}) collective-permute-start(bf16[640,256]{1,0:T(8,128)(2,1)} %pad_maximum_fusion.1), channel_id=1, source_target_pairs={{0,48},{16,0},{32,16},{48,32},{1,49},{17,1},{33,17},{49,33},{2,50}... | collective-permute-start | bytes 983048 | tf_op jit(solution)/shard_map/ppermute | solution.py:20
  14.6 1.0 multiply_reduce_fusion.2
  15.7 1.0 maximum_maximum_fusion
  16.7 1.1 broadcast_in_dim.19
  17.8 10.0 %all-to-all-start = ((bf16[8,136,512]{2,1,0:T(8,128)(2,1)}), bf16[8,136,512]{2,1,0:T(8,128)(2,1)S(1)}, u32[]{:S(2)}, u32[]{:S(2)}) async-start(bf16[8,136,512]{2,1,0:T(8,128)(2,1)} %broadcast_in_dim.19), calls=%async_computation | async-start | bytes 2228224 | tf_op jit(solution)/shard_map/all_to_all | solution.py:24
  27.8 3.3 %copy.162 = bf16[256,4096]{0,1:T(8,128)(2,1)S(1)} copy(bf16[256,4096]{1,0:T(8,128)(2,1)} %param.10) | data formatting | bytes 4194304 | tf_op args[2]
  31.9 0.9 slice_dynamic-update-slice_fusion.5
  32.9 0.9 slice_dynamic-update-slice_fusion.4
  33.8 0.9 slice_dynamic-update-slice_fusion.3
  34.7 0.9 slice_dynamic-update-slice_fusion.2
  35.7 0.9 slice_dynamic-update-slice_fusion.1
  36.6 0.9 slice_dynamic-update-slice_fusion
  37.5 3.7 %collective-permute-start.3 = (bf16[2048,256]{1,0:T(8,128)(2,1)S(1)}, bf16[2048,256]{1,0:T(8,128)(2,1)}, u32[]{:S(2)}, u32[]{:S(2)}) collective-permute-start(bf16[2048,256]{1,0:T(8,128)(2,1)S(1)} %slice_dynamic-update-slice_fusion), channel_id=1, source_target_pairs={{0,1},{1,0},{2,3},{3,2},{4,5},{5,4},{6,7},{7,6},{8,9},{9,8},{10,11... | collective-permute-start | bytes 3145736 | tf_op jit(solution)/shard_map/ppermute | solution.py:20
  43.5 14.9 %all-to-all-done = bf16[8,136,512]{2,1,0:T(8,128)(2,1)S(1)} async-done(((bf16[8,136,512]{2,1,0:T(8,128)(2,1)}), bf16[8,136,512]{2,1,0:T(8,128)(2,1)S(1)}, u32[]{:S(2)}, u32[]{:S(2)}) %all-to-all-start) | async-done | bytes 1114144 | tf_op jit(solution)/shard_map/all_to_all | solution.py:24
  59.3 1.8 multiply_reduce_fusion
  61.1 3.1 %fusion.2 = (f32[1024]{0:T(1024)S(1)}, f32[1024]{0:T(1024)S(1)}, bf16[1024,1024]{1,0:T(8,128)(2,1)}, bf16[1024,1024]{1,0:T(8,128)(2,1)}) fusion(f32[1024,1024]{1,0:T(8,128)S(1)} %get-tuple-element.96, f32[1024]{0:T(1024)S(1)} %max.14, f32[1024,1024]{1,0:T(8,128)S(1)} %get-tuple-element.94), kind=kLoop, calls=%fused_computation.8 | loop fusion | flops 8386560 | bytes 12595200 | tf_op jit(solution)/shard_map/reduce_sum | solution.py:100
  64.9 3.4 %all-to-all-start.1 = ((f32[8,16,128]{2,1,0:T(8,128)}), f32[8,16,128]{2,1,0:T(8,128)S(1)}, u32[]{:S(2)}, u32[]{:S(2)}) async-start(f32[8,16,128]{2,1,0:T(8,128)} %broadcast_in_dim.20), calls=%async_computation.1 | async-start | bytes 131072 | tf_op jit(solution)/shard_map/all_to_all | solution.py:24
  68.2 2.4 %multiply_convert_fusion.1 = bf16[1024,1024]{1,0:T(8,128)(2,1)S(1)} fusion(bf16[1024,1024]{1,0:T(8,128)(2,1)} %get-tuple-element.20, bf16[1024,256]{1,0:T(8,128)(2,1)S(1)} %bitcast.108, f32[1024]{0:T(1024)S(1)} %bitcast.119, bf16[2048,256]{1,0:T(8,128)(2,1)S(1)} %slice_dynamic-update-slice_fusion), kind=kOutput, calls=%fused_computation.1 | convolution fusion | flops 542113792 | bytes 5246976 | tf_op jit(solution)/shard_map/dot_general | solution.py:33
  71.4 1.6 copy-done
  73.0 1.9 %multiply_convert_fusion = bf16[1024,1024]{1,0:T(8,128)(2,1)S(1)} fusion(bf16[1024,1024]{1,0:T(8,128)(2,1)S(1)} %copy-done, bf16[1024,256]{1,0:T(8,128)(2,1)S(1)} %bitcast.109, f32[1024]{0:T(1024)S(1)} %bitcast.120, bf16[2048,256]{1,0:T(8,128)(2,1)} %collective-permute-done.3), kind=kOutput, calls=%fused_computation | convolution fusion | flops 542113792 | bytes 5246976 | tf_op jit(solution)/shard_map/dot_general | solution.py:33
  74.9 1.3 copy-done.4
  76.3 1.8 convolution_add_fusion
  78.4 1.0 copy.164
  82.3 2.4 %collective-permute-start.4 = (bf16[1024,512]{1,0:T(8,128)(2,1)S(1)}, bf16[1024,512]{1,0:T(8,128)(2,1)}, u32[]{:S(2)}, u32[]{:S(2)}) collective-permute-start(bf16[1024,512]{1,0:T(8,128)(2,1)S(1)} %pad_maximum_fusion), channel_id=1, source_target_pairs={{0,1},{1,0},{2,3},{3,2},{4,5},{5,4},{6,7},{7,6},{8,9},{9,8},{10,11... | collective-permute-start | bytes 3145736 | tf_op jit(solution)/shard_map/ppermute | solution.py:20
  85.8 7.3 %all-to-all-start.2 = ((bf16[32,64,128]{2,1,0:T(8,128)(2,1)}), bf16[32,64,128]{2,1,0:T(8,128)(2,1)S(1)}, u32[]{:S(2)}, u32[]{:S(2)}) async-start(bf16[32,64,128]{2,1,0:T(8,128)(2,1)} %bitcast.15), calls=%async_computation.2 | async-start | bytes 1048576 | tf_op jit(solution)/shard_map/all_to_all | solution.py:24
  93.0 2.6 %fusion.18 = f32[1024,256]{1,0:T(8,128)S(1)} fusion(bf16[1024,1024]{1,0:T(8,128)(2,1)} %get-tuple-element.20, bf16[1024,256]{1,0:T(8,128)(2,1)S(1)} %bitcast.111, f32[1024]{0:T(1024)S(1)} %fusion.20), kind=kOutput, calls=%fused_computation.42 | convolution fusion | flops 537657344 | bytes 3674112 | tf_op jit(solution)/shard_map/dot_general | solution.py:33
  95.6 2.2 %collective-permute-start.5 = (bf16[512,256]{0,1:T(8,128)(2,1)S(1)}, bf16[512,256]{0,1:T(8,128)(2,1)S(1)}, u32[]{:S(2)}, u32[]{:S(2)}) collective-permute-start(bf16[512,256]{0,1:T(8,128)(2,1)S(1)} %constant_dynamic-update-slice_fusion.2), channel_id=1, source_target_pairs={{0,1},{1,0},{2,3},{3,2},{4,5},{5,4},{6,7},{7,6},{8,9},{9,8},{10,11... | collective-permute-start | bytes 786440 | tf_op jit(solution)/shard_map/ppermute | solution.py:20
  99.2 1.5 fusion.4
  100.7 9.0 %all-to-all-done.2 = bf16[32,64,128]{2,1,0:T(8,128)(2,1)S(1)} async-done(((bf16[32,64,128]{2,1,0:T(8,128)(2,1)}), bf16[32,64,128]{2,1,0:T(8,128)(2,1)S(1)}, u32[]{:S(2)}, u32[]{:S(2)}) %all-to-all-start.2) | async-done | bytes 524320 | tf_op jit(solution)/shard_map/all_to_all | solution.py:24
  110.0 22.3 %all_to_all.30 = bf16[8,72,512]{2,1,0:T(8,128)(2,1)S(1)} all-to-all(bf16[8,72,512]{2,1,0:T(8,128)(2,1)S(1)} %broadcast_in_dim.23), channel_id=1, replica_groups=mesh['z'=8,'x'=4,'y'=8,'c'=2] {'y'}, dimensions={0} | all-to-all | bytes 1179648 | tf_op jit(solution)/shard_map/all_to_all | solution.py:24
  133.1 0.9 copy.175
  133.9 6.2 %collective-permute-start.6 = (bf16[512,512]{1,0:T(8,128)(2,1)S(1)}, bf16[512,512]{1,0:T(8,128)(2,1)S(1)}, u32[]{:S(2)}, u32[]{:S(2)}) collective-permute-start(bf16[512,512]{1,0:T(8,128)(2,1)S(1)} %bitcast.86), channel_id=1, source_target_pairs={{0,1},{1,0},{2,3},{3,2},{4,5},{5,4},{6,7},{7,6},{8,9},{9,8},{10,11... | collective-permute-start | bytes 1572872 | tf_op jit(solution)/shard_map/ppermute | solution.py:20
  140.2 5.6 %all-to-all-start.4 = ((bf16[64,8,512]{2,1,0:T(8,128)(2,1)}), bf16[64,8,512]{2,1,0:T(8,128)(2,1)S(1)}, u32[]{:S(2)}, u32[]{:S(2)}) async-start(bf16[64,8,512]{2,1,0:T(8,128)(2,1)} %bitcast.30), calls=%async_computation.4 | async-start | bytes 1048576 | tf_op jit(solution)/shard_map/all_to_all | solution.py:24
  145.9 4.8 %collective-permute-start.10 = (bf16[256,512]{1,0:T(8,128)(2,1)S(1)}, bf16[256,512]{1,0:T(8,128)(2,1)S(1)}, u32[]{:S(2)}, u32[]{:S(2)}) collective-permute-start(bf16[256,512]{1,0:T(8,128)(2,1)S(1)} %get-tuple-element.80), channel_id=1, source_target_pairs={{0,32},{16,48},{32,0},{48,16},{1,33},{17,49},{33,1},{49,17},{2,34}... | collective-permute-start | bytes 786440 | tf_op jit(solution)/shard_map/ppermute | solution.py:20
  150.7 2.8 %collective-permute-start.12 = (bf16[256,512]{1,0:T(8,128)(2,1)S(1)}, bf16[256,512]{1,0:T(8,128)(2,1)S(1)}, u32[]{:S(2)}, u32[]{:S(2)}) collective-permute-start(bf16[256,512]{1,0:T(8,128)(2,1)S(1)} %get-tuple-element.81), channel_id=1, source_target_pairs={{0,48},{16,0},{32,16},{48,32},{1,49},{17,1},{33,17},{49,33},{2,50}... | collective-permute-start | bytes 786440 | tf_op jit(solution)/shard_map/ppermute | solution.py:20
  153.5 2.5 %collective-permute-start.11 = (bf16[256,512]{1,0:T(8,128)(2,1)S(1)}, bf16[256,512]{1,0:T(8,128)(2,1)S(1)}, u32[]{:S(2)}, u32[]{:S(2)}) collective-permute-start(bf16[256,512]{1,0:T(8,128)(2,1)S(1)} %get-tuple-element.82), channel_id=1, source_target_pairs={{0,16},{16,32},{32,48},{48,0},{1,17},{17,33},{33,49},{49,1},{2,18}... | collective-permute-start | bytes 786440 | tf_op jit(solution)/shard_map/ppermute | solution.py:20
  156.7 2.2 %collective-permute-start.7 = (bf16[256,128]{1,0:T(8,128)(2,1)S(1)}, bf16[256,128]{1,0:T(8,128)(2,1)S(1)}, u32[]{:S(2)}, u32[]{:S(2)}) collective-permute-start(bf16[256,128]{1,0:T(8,128)(2,1)S(1)} %get-tuple-element.83), channel_id=1, source_target_pairs={{0,16},{16,32},{32,48},{48,0},{1,17},{17,33},{33,49},{49,1},{2,18}... | collective-permute-start | bytes 196616 | tf_op jit(solution)/shard_map/ppermute | solution.py:20
  158.9 4.9 %collective-permute-start.9 = (bf16[256,128]{1,0:T(8,128)(2,1)S(1)}, bf16[256,128]{1,0:T(8,128)(2,1)S(1)}, u32[]{:S(2)}, u32[]{:S(2)}) collective-permute-start(bf16[256,128]{1,0:T(8,128)(2,1)S(1)} %get-tuple-element.84), channel_id=1, source_target_pairs={{0,32},{16,48},{32,0},{48,16},{1,33},{17,49},{33,1},{49,17},{2,34}... | collective-permute-start | bytes 196616 | tf_op jit(solution)/shard_map/ppermute | solution.py:20
  163.8 2.1 %collective-permute-start.8 = (bf16[256,128]{1,0:T(8,128)(2,1)S(1)}, bf16[256,128]{1,0:T(8,128)(2,1)S(1)}, u32[]{:S(2)}, u32[]{:S(2)}) collective-permute-start(bf16[256,128]{1,0:T(8,128)(2,1)S(1)} %get-tuple-element.85), channel_id=1, source_target_pairs={{0,48},{16,0},{32,16},{48,32},{1,49},{17,1},{33,17},{49,33},{2,50}... | collective-permute-start | bytes 196616 | tf_op jit(solution)/shard_map/ppermute | solution.py:20
  165.9 1.5 collective-permute-done.12
  167.4 0.9 collective-permute-done.11
  169.1 3.4 %all-to-all-start.5 = ((bf16[8,32,512]{2,1,0:T(8,128)(2,1)}), bf16[8,32,512]{2,1,0:T(8,128)(2,1)S(1)}, u32[]{:S(2)}, u32[]{:S(2)}) async-start(bf16[8,32,512]{2,1,0:T(8,128)(2,1)} %bitcast.35), calls=%async_computation.5 | async-start | bytes 524288 | tf_op jit(solution)/shard_map/all_to_all | solution.py:24
  173.8 0.9 reshape.178
  174.7 10.1 %all-to-all-done.5 = bf16[8,32,512]{2,1,0:T(8,128)(2,1)S(1)} async-done(((bf16[8,32,512]{2,1,0:T(8,128)(2,1)}), bf16[8,32,512]{2,1,0:T(8,128)(2,1)S(1)}, u32[]{:S(2)}, u32[]{:S(2)}) %all-to-all-start.5) | async-done | bytes 262176 | tf_op jit(solution)/shard_map/all_to_all | solution.py:24
  (103 shorter events, 17.3 us)
Async XLA Ops:
  3.2 28.7 %collective-permute-start = (bf16[640,256]{1,0:T(8,128)(2,1)}, bf16[640,256]{1,0:T(8,128)(2,1)}, u32[]{:S(2)}, u32[]{:S(2)}) collective-permute-start(bf16[640,256]{1,0:T(8,128)(2,1)} %pad_maximum_fusion.1), channel_id=1, source_target_pairs={{0,16},{16,32},{32,48},{48,0},{1,17},{17,33},{33,49},{49,1},{2,18}... | collective-permute-start | bytes 983048 | tf_op jit(solution)/shard_map/ppermute | solution.py:20
  7.2 26.6 %collective-permute-start.2 = (bf16[640,256]{1,0:T(8,128)(2,1)}, bf16[640,256]{1,0:T(8,128)(2,1)}, u32[]{:S(2)}, u32[]{:S(2)}) collective-permute-start(bf16[640,256]{1,0:T(8,128)(2,1)} %pad_maximum_fusion.1), channel_id=1, source_target_pairs={{0,32},{16,48},{32,0},{48,16},{1,33},{17,49},{33,1},{49,17},{2,34}... | collective-permute-start | bytes 983048 | tf_op jit(solution)/shard_map/ppermute | solution.py:20
  11.5 21.3 %collective-permute-start.1 = (bf16[640,256]{1,0:T(8,128)(2,1)}, bf16[640,256]{1,0:T(8,128)(2,1)}, u32[]{:S(2)}, u32[]{:S(2)}) collective-permute-start(bf16[640,256]{1,0:T(8,128)(2,1)} %pad_maximum_fusion.1), channel_id=1, source_target_pairs={{0,48},{16,0},{32,16},{48,32},{1,49},{17,1},{33,17},{49,33},{2,50}... | collective-permute-start | bytes 983048 | tf_op jit(solution)/shard_map/ppermute | solution.py:20
  17.8 40.6 %all-to-all-start = ((bf16[8,136,512]{2,1,0:T(8,128)(2,1)}), bf16[8,136,512]{2,1,0:T(8,128)(2,1)S(1)}, u32[]{:S(2)}, u32[]{:S(2)}) async-start(bf16[8,136,512]{2,1,0:T(8,128)(2,1)} %broadcast_in_dim.19), calls=%async_computation | async-start | bytes 2228224 | tf_op jit(solution)/shard_map/all_to_all | solution.py:24
  31.1 10.2 %copy-start.8 = (bf16[128,256]{1,0:T(8,128)(2,1)S(1)}, bf16[128,256]{1,0:T(8,128)(2,1)}, u32[]{:S(2)}) copy-start(bf16[128,256]{1,0:T(8,128)(2,1)} %param.8) | copy-start | bytes 196612
  37.5 21.8 %collective-permute-start.3 = (bf16[2048,256]{1,0:T(8,128)(2,1)S(1)}, bf16[2048,256]{1,0:T(8,128)(2,1)}, u32[]{:S(2)}, u32[]{:S(2)}) collective-permute-start(bf16[2048,256]{1,0:T(8,128)(2,1)S(1)} %slice_dynamic-update-slice_fusion), channel_id=1, source_target_pairs={{0,1},{1,0},{2,3},{3,2},{4,5},{5,4},{6,7},{7,6},{8,9},{9,8},{10,11... | collective-permute-start | bytes 3145736 | tf_op jit(solution)/shard_map/ppermute | solution.py:20
  64.9 13.2 %all-to-all-start.1 = ((f32[8,16,128]{2,1,0:T(8,128)}), f32[8,16,128]{2,1,0:T(8,128)S(1)}, u32[]{:S(2)}, u32[]{:S(2)}) async-start(f32[8,16,128]{2,1,0:T(8,128)} %broadcast_in_dim.20), calls=%async_computation.1 | async-start | bytes 131072 | tf_op jit(solution)/shard_map/all_to_all | solution.py:24
  70.7 4.2 %copy-start.2 = (bf16[1024,1024]{1,0:T(8,128)(2,1)}, bf16[1024,1024]{1,0:T(8,128)(2,1)S(1)}, u32[]{:S(2)}) copy-start(bf16[1024,1024]{1,0:T(8,128)(2,1)S(1)} %multiply_convert_fusion.1) | copy-start | bytes 6291460
  70.7 2.3 %copy-start = (bf16[1024,1024]{1,0:T(8,128)(2,1)S(1)}, bf16[1024,1024]{1,0:T(8,128)(2,1)}, u32[]{:S(2)}) copy-start(bf16[1024,1024]{1,0:T(8,128)(2,1)} %get-tuple-element.21) | copy-start | bytes 6291460
  74.9 1.4 copy-start.4
  78.0 1.8 copy-start.1
  79.8 1.6 copy-start.5
  82.3 16.9 %collective-permute-start.4 = (bf16[1024,512]{1,0:T(8,128)(2,1)S(1)}, bf16[1024,512]{1,0:T(8,128)(2,1)}, u32[]{:S(2)}, u32[]{:S(2)}) collective-permute-start(bf16[1024,512]{1,0:T(8,128)(2,1)S(1)} %pad_maximum_fusion), channel_id=1, source_target_pairs={{0,1},{1,0},{2,3},{3,2},{4,5},{5,4},{6,7},{7,6},{8,9},{9,8},{10,11... | collective-permute-start | bytes 3145736 | tf_op jit(solution)/shard_map/ppermute | solution.py:20
  85.8 24.0 %all-to-all-start.2 = ((bf16[32,64,128]{2,1,0:T(8,128)(2,1)}), bf16[32,64,128]{2,1,0:T(8,128)(2,1)S(1)}, u32[]{:S(2)}, u32[]{:S(2)}) async-start(bf16[32,64,128]{2,1,0:T(8,128)(2,1)} %bitcast.15), calls=%async_computation.2 | async-start | bytes 1048576 | tf_op jit(solution)/shard_map/all_to_all | solution.py:24
  93.0 4.8 %copy-start.3 = (bf16[1024,1024]{1,0:T(8,128)(2,1)S(1)}, bf16[1024,1024]{1,0:T(8,128)(2,1)}, u32[]{:S(2)}) copy-start(bf16[1024,1024]{1,0:T(8,128)(2,1)} %copy-done.2) | copy-start | bytes 6291460
  95.6 3.4 %collective-permute-start.5 = (bf16[512,256]{0,1:T(8,128)(2,1)S(1)}, bf16[512,256]{0,1:T(8,128)(2,1)S(1)}, u32[]{:S(2)}, u32[]{:S(2)}) collective-permute-start(bf16[512,256]{0,1:T(8,128)(2,1)S(1)} %constant_dynamic-update-slice_fusion.2), channel_id=1, source_target_pairs={{0,1},{1,0},{2,3},{3,2},{4,5},{5,4},{6,7},{7,6},{8,9},{9,8},{10,11... | collective-permute-start | bytes 786440 | tf_op jit(solution)/shard_map/ppermute | solution.py:20
  132.5 7.6 %copy-start.9 = (f32[256]{0:T(256)S(1)}, f32[256]{0:T(256)}, u32[]{:S(2)}) copy-start(f32[256]{0:T(256)} %param.9) | copy-start | bytes 3076
  133.1 22.9 %copy-start.7 = (bf16[256,8,1,1,64]{0,4,3,2,1:T(8,128)(2,1)S(1)}, bf16[256,8,1,1,64]{0,4,3,2,1:T(8,128)(2,1)}, u32[]{:S(2)}) copy-start(bf16[256,8,1,1,64]{0,4,3,2,1:T(8,128)(2,1)} %get-tuple-element.77) | copy-start | bytes 786436
  133.9 22.4 %copy-start.6 = (bf16[256,8,1,1,64]{0,4,3,2,1:T(8,128)(2,1)S(1)}, bf16[256,8,1,1,64]{0,4,3,2,1:T(8,128)(2,1)}, u32[]{:S(2)}) copy-start(bf16[256,8,1,1,64]{0,4,3,2,1:T(8,128)(2,1)} %get-tuple-element.76) | copy-start | bytes 786436
  133.9 22.4 %collective-permute-start.6 = (bf16[512,512]{1,0:T(8,128)(2,1)S(1)}, bf16[512,512]{1,0:T(8,128)(2,1)S(1)}, u32[]{:S(2)}, u32[]{:S(2)}) collective-permute-start(bf16[512,512]{1,0:T(8,128)(2,1)S(1)} %bitcast.86), channel_id=1, source_target_pairs={{0,1},{1,0},{2,3},{3,2},{4,5},{5,4},{6,7},{7,6},{8,9},{9,8},{10,11... | collective-permute-start | bytes 1572872 | tf_op jit(solution)/shard_map/ppermute | solution.py:20
  140.2 28.9 %all-to-all-start.4 = ((bf16[64,8,512]{2,1,0:T(8,128)(2,1)}), bf16[64,8,512]{2,1,0:T(8,128)(2,1)S(1)}, u32[]{:S(2)}, u32[]{:S(2)}) async-start(bf16[64,8,512]{2,1,0:T(8,128)(2,1)} %bitcast.30), calls=%async_computation.4 | async-start | bytes 1048576 | tf_op jit(solution)/shard_map/all_to_all | solution.py:24
  145.9 17.9 %collective-permute-start.10 = (bf16[256,512]{1,0:T(8,128)(2,1)S(1)}, bf16[256,512]{1,0:T(8,128)(2,1)S(1)}, u32[]{:S(2)}, u32[]{:S(2)}) collective-permute-start(bf16[256,512]{1,0:T(8,128)(2,1)S(1)} %get-tuple-element.80), channel_id=1, source_target_pairs={{0,32},{16,48},{32,0},{48,16},{1,33},{17,49},{33,1},{49,17},{2,34}... | collective-permute-start | bytes 786440 | tf_op jit(solution)/shard_map/ppermute | solution.py:20
  150.7 16.8 %collective-permute-start.12 = (bf16[256,512]{1,0:T(8,128)(2,1)S(1)}, bf16[256,512]{1,0:T(8,128)(2,1)S(1)}, u32[]{:S(2)}, u32[]{:S(2)}) collective-permute-start(bf16[256,512]{1,0:T(8,128)(2,1)S(1)} %get-tuple-element.81), channel_id=1, source_target_pairs={{0,48},{16,0},{32,16},{48,32},{1,49},{17,1},{33,17},{49,33},{2,50}... | collective-permute-start | bytes 786440 | tf_op jit(solution)/shard_map/ppermute | solution.py:20
  153.5 14.9 %collective-permute-start.11 = (bf16[256,512]{1,0:T(8,128)(2,1)S(1)}, bf16[256,512]{1,0:T(8,128)(2,1)S(1)}, u32[]{:S(2)}, u32[]{:S(2)}) collective-permute-start(bf16[256,512]{1,0:T(8,128)(2,1)S(1)} %get-tuple-element.82), channel_id=1, source_target_pairs={{0,16},{16,32},{32,48},{48,0},{1,17},{17,33},{33,49},{49,1},{2,18}... | collective-permute-start | bytes 786440 | tf_op jit(solution)/shard_map/ppermute | solution.py:20
  156.7 15.9 %collective-permute-start.7 = (bf16[256,128]{1,0:T(8,128)(2,1)S(1)}, bf16[256,128]{1,0:T(8,128)(2,1)S(1)}, u32[]{:S(2)}, u32[]{:S(2)}) collective-permute-start(bf16[256,128]{1,0:T(8,128)(2,1)S(1)} %get-tuple-element.83), channel_id=1, source_target_pairs={{0,16},{16,32},{32,48},{48,0},{1,17},{17,33},{33,49},{49,1},{2,18}... | collective-permute-start | bytes 196616 | tf_op jit(solution)/shard_map/ppermute | solution.py:20
  158.9 13.7 %collective-permute-start.9 = (bf16[256,128]{1,0:T(8,128)(2,1)S(1)}, bf16[256,128]{1,0:T(8,128)(2,1)S(1)}, u32[]{:S(2)}, u32[]{:S(2)}) collective-permute-start(bf16[256,128]{1,0:T(8,128)(2,1)S(1)} %get-tuple-element.84), channel_id=1, source_target_pairs={{0,32},{16,48},{32,0},{48,16},{1,33},{17,49},{33,1},{49,17},{2,34}... | collective-permute-start | bytes 196616 | tf_op jit(solution)/shard_map/ppermute | solution.py:20
  163.8 8.8 %collective-permute-start.8 = (bf16[256,128]{1,0:T(8,128)(2,1)S(1)}, bf16[256,128]{1,0:T(8,128)(2,1)S(1)}, u32[]{:S(2)}, u32[]{:S(2)}) collective-permute-start(bf16[256,128]{1,0:T(8,128)(2,1)S(1)} %get-tuple-element.85), channel_id=1, source_target_pairs={{0,48},{16,0},{32,16},{48,32},{1,49},{17,1},{33,17},{49,33},{2,50}... | collective-permute-start | bytes 196616 | tf_op jit(solution)/shard_map/ppermute | solution.py:20
  169.1 15.6 %all-to-all-start.5 = ((bf16[8,32,512]{2,1,0:T(8,128)(2,1)}), bf16[8,32,512]{2,1,0:T(8,128)(2,1)S(1)}, u32[]{:S(2)}, u32[]{:S(2)}) async-start(bf16[8,32,512]{2,1,0:T(8,128)(2,1)} %bitcast.35), calls=%async_computation.5 | async-start | bytes 524288 | tf_op jit(solution)/shard_map/all_to_all | solution.py:24

commit v8 on v7

--- a/solution.py
+++ b/solution.py
@@ -81,8 +81,11 @@
     w_theirs = jnp.where(core == 0, w_odd, w_even)
 
     half = nx * src // 2
-    mine = [b[: src // 2] for b in blocks] + [b[src // 2 : src] for b in blocks]
-    mine = row_major(jnp.concatenate(mine, axis=0))
+    mine = jnp.zeros((2 * half, HEAD_DIM), BF16)
+    for k, block in enumerate(blocks):
+        mine = lax.dynamic_update_slice(mine, block[: src // 2], (k * src // 2, 0))
+        mine = lax.dynamic_update_slice(mine, block[src // 2 : src], (half + k * src // 2, 0))
+    mine = row_major(mine)
     mine, w_mine, w_theirs = lax.optimization_barrier((mine, w_mine, w_theirs))
     theirs = shifted(mine, "c", 1)
     key_one, value_one = mine[:half], mine[half : 2 * half]

time: 189 us -> 184 us (0.974)
  local copies, waits for them, and re-layouts: 25.3 us -> 18.2 us
  starting transfers between devices: 74.7 us -> 78.4 us
  waiting for transfers between devices: 36.8 us -> 33.5 us
  other arithmetic: 11.2 us -> 13.2 us
    all_to_all x5, waiting for transfers between devices: 34 us -> 29 us  [exchanged(): return lax.all_to_all(value, axis, split_axis=0, concat_axis=0, tiled=True)]
    unnamed x32 -> x31, local copies, waits for them, and re-layouts: 14.3 us -> 10.5 us
    slice x7 -> x8, local copies, waits for them, and re-layouts: 2.98 us -> 0.46 us  [local(): block[src:]]
    all_to_all x5, starting transfers between devices: 29.7 us -> 31.8 us  [exchanged(): return lax.all_to_all(value, axis, split_axis=0, concat_axis=0, tiled=True)]
  transfers between devices with their start and end apart: 18 -> 18, of which waited for: 6 -> 7; matrix products, arithmetic and copies ran while one was open for 17% -> 14% of each run, Pallas kernels for 0% -> 0%
where the time goes in v8:
time: 184 us; the launch traced here: 182 us
  starting transfers between devices  78.4 us (43%)
  waiting for transfers between devices  33.5 us (18%)
  blocking collectives  22.3 us (12%)
  local copies, waits for them, and re-layouts  18.2 us (10%)
  matrix products  14.9 us (8%)
  other arithmetic  13.2 us (7%)
    ppermute x13, starting transfers between devices, shifted(): return lax.ppermute(value, axis, [(i, (i + by) % n) for i in range(n)])  46.6 us
    all_to_all x5, starting transfers between devices, exchanged(): return lax.all_to_all(value, axis, split_axis=0, concat_axis=0, tiled=True)  31.8 us
    all_to_all x5, waiting for transfers between devices, exchanged(): return lax.all_to_all(value, axis, split_axis=0, concat_axis=0, tiled=True)  29 us
    all_to_all x1, blocking collectives, exchanged(): return lax.all_to_all(value, axis, split_axis=0, concat_axis=0, tiled=True)  22.3 us
    dot_general x13, matrix products, dot(): lax.dot_general(a, b, (((ca,), (cb,)), ((), ())), preferred_element_type=...  14.9 us
    unnamed x31, local copies, waits for them, and re-layouts  10.5 us
    ppermute x13, waiting for transfers between devices, shifted(): return lax.ppermute(value, axis, [(i, (i + by) % n) for i in range(n)])  4.51 us
  transfers between devices with their start and end apart: 18, of which 7 were waited for; matrix products, arithmetic and copies ran while one was open for 14% of the time, Pallas kernels for 0%

profile of v8, /device:TPU:1, one launch (start us, length us, event | category | flops | bytes accessed | tf_op | source)
XLA Modules:
  0.0 182.1 jit_solution(4438515399929252373)
XLA Ops:
  0.6 1.0 constant_dynamic-slice_fusion
  1.7 1.6 pad_maximum_fusion.1
  3.3 3.9 %collective-permute-start = (bf16[640,256]{1,0:T(8,128)(2,1)}, bf16[640,256]{1,0:T(8,128)(2,1)S(1)}, u32[]{:S(2)}, u32[]{:S(2)}) collective-permute-start(bf16[640,256]{1,0:T(8,128)(2,1)} %pad_maximum_fusion.1), channel_id=1, source_target_pairs={{0,16},{16,32},{32,48},{48,0},{1,17},{17,33},{33,49},{49,1},{2,18}... | collective-permute-start | bytes 983048 | tf_op jit(solution)/shard_map/ppermute | solution.py:20
  7.2 1.0 multiply_reduce_fusion.2
  8.3 1.0 maximum_maximum_fusion
  9.3 1.1 broadcast_in_dim.19
  10.3 10.0 %all-to-all-start = ((bf16[8,136,512]{2,1,0:T(8,128)(2,1)}), bf16[8,136,512]{2,1,0:T(8,128)(2,1)S(1)}, u32[]{:S(2)}, u32[]{:S(2)}) async-start(bf16[8,136,512]{2,1,0:T(8,128)(2,1)} %broadcast_in_dim.19), calls=%async_computation | async-start | bytes 2228224 | tf_op jit(solution)/shard_map/all_to_all | solution.py:24
  20.4 3.4 %collective-permute-start.1 = (bf16[640,256]{1,0:T(8,128)(2,1)}, bf16[640,256]{1,0:T(8,128)(2,1)S(1)}, u32[]{:S(2)}, u32[]{:S(2)}) collective-permute-start(bf16[640,256]{1,0:T(8,128)(2,1)} %pad_maximum_fusion.1), channel_id=1, source_target_pairs={{0,48},{16,0},{32,16},{48,32},{1,49},{17,1},{33,17},{49,33},{2,50}... | collective-permute-start | bytes 983048 | tf_op jit(solution)/shard_map/ppermute | solution.py:20
  23.7 3.4 %collective-permute-start.2 = (bf16[640,256]{1,0:T(8,128)(2,1)}, bf16[640,256]{1,0:T(8,128)(2,1)S(1)}, u32[]{:S(2)}, u32[]{:S(2)}) collective-permute-start(bf16[640,256]{1,0:T(8,128)(2,1)} %pad_maximum_fusion.1), channel_id=1, source_target_pairs={{0,32},{16,48},{32,0},{48,16},{1,33},{17,49},{33,1},{49,17},{2,34}... | collective-permute-start | bytes 983048 | tf_op jit(solution)/shard_map/ppermute | solution.py:20
  27.3 4.1 %copy.162 = bf16[256,4096]{0,1:T(8,128)(2,1)} copy(bf16[256,4096]{1,0:T(8,128)(2,1)} %param.10) | data formatting | bytes 4194304 | tf_op args[2]
  31.4 1.9 %broadcast_select_fusion = (bf16[256,8,1,1,64]{0,4,3,2,1:T(8,128)(2,1)}, bf16[256,8,1,1,64]{0,4,3,2,1:T(8,128)(2,1)}) fusion(pred[]{:T(512)S(6)} %eq.2, bf16[256,8,2,4,64]{0,4,3,2,1:T(8,128)(2,1)} %bitcast.88, s32[]{:T(128)S(6)} %select_n.73, s32[]{:T(128)S(6)} %add.125), kind=kLoop, calls=%fused_computation.39 | loop fusion | flops 262144 | bytes 1048585 | tf_op jit(solution)/shard_map/jit(_where)/select_n | solution.py:81
  33.4 1.7 collective-permute-done.2
  35.1 5.9 %collective-permute-start.3 = (bf16[2048,256]{1,0:T(8,128)(2,1)S(1)}, bf16[2048,256]{1,0:T(8,128)(2,1)}, u32[]{:S(2)}, u32[]{:S(2)}) collective-permute-start(bf16[2048,256]{1,0:T(8,128)(2,1)S(1)} %slice_dynamic-update-slice_fusion), channel_id=1, source_target_pairs={{0,1},{1,0},{2,3},{3,2},{4,5},{5,4},{6,7},{7,6},{8,9},{9,8},{10,11... | collective-permute-start | bytes 3145736 | tf_op jit(solution)/shard_map/ppermute | solution.py:20
  41.6 9.4 %all-to-all-done = bf16[8,136,512]{2,1,0:T(8,128)(2,1)S(1)} async-done(((bf16[8,136,512]{2,1,0:T(8,128)(2,1)}), bf16[8,136,512]{2,1,0:T(8,128)(2,1)S(1)}, u32[]{:S(2)}, u32[]{:S(2)}) %all-to-all-start) | async-done | bytes 1114144 | tf_op jit(solution)/shard_map/all_to_all | solution.py:24
  51.9 1.8 multiply_reduce_fusion
  53.7 3.1 %fusion.2 = (f32[1024]{0:T(1024)S(1)}, f32[1024]{0:T(1024)S(1)}, bf16[1024,1024]{1,0:T(8,128)(2,1)}, bf16[1024,1024]{1,0:T(8,128)(2,1)}) fusion(f32[1024,1024]{1,0:T(8,128)S(1)} %get-tuple-element.96, f32[1024]{0:T(1024)S(1)} %max.14, f32[1024,1024]{1,0:T(8,128)S(1)} %get-tuple-element.94), kind=kLoop, calls=%fused_computation.8 | loop fusion | flops 8386560 | bytes 12595200 | tf_op jit(solution)/shard_map/reduce_sum | solution.py:103
  57.4 3.4 %all-to-all-start.1 = ((f32[8,16,128]{2,1,0:T(8,128)}), f32[8,16,128]{2,1,0:T(8,128)S(1)}, u32[]{:S(2)}, u32[]{:S(2)}) async-start(f32[8,16,128]{2,1,0:T(8,128)} %broadcast_in_dim.20), calls=%async_computation.1 | async-start | bytes 131072 | tf_op jit(solution)/shard_map/all_to_all | solution.py:24
  60.8 2.4 %multiply_convert_fusion.1 = bf16[1024,1024]{1,0:T(8,128)(2,1)S(1)} fusion(bf16[1024,1024]{1,0:T(8,128)(2,1)} %get-tuple-element.20, bf16[1024,256]{1,0:T(8,128)(2,1)S(1)} %bitcast.108, f32[1024]{0:T(1024)S(1)} %bitcast.119, bf16[2048,256]{1,0:T(8,128)(2,1)S(1)} %slice_dynamic-update-slice_fusion), kind=kOutput, calls=%fused_computation.1 | convolution fusion | flops 542113792 | bytes 5246976 | tf_op jit(solution)/shard_map/dot_general | solution.py:33
  63.9 1.6 copy-done.1
  65.5 1.9 %multiply_convert_fusion = bf16[1024,1024]{1,0:T(8,128)(2,1)S(1)} fusion(bf16[1024,1024]{1,0:T(8,128)(2,1)S(1)} %copy-done.1, bf16[1024,256]{1,0:T(8,128)(2,1)S(1)} %bitcast.109, f32[1024]{0:T(1024)S(1)} %bitcast.120, bf16[2048,256]{1,0:T(8,128)(2,1)} %collective-permute-done.3), kind=kOutput, calls=%fused_computation | convolution fusion | flops 542113792 | bytes 5246976 | tf_op jit(solution)/shard_map/dot_general | solution.py:33
  67.4 1.3 copy-done.5
  68.8 1.8 convolution_add_fusion
  70.9 1.0 copy.164
  73.9 0.8 convolution_convert_fusion.2
  74.8 1.0 pad_maximum_fusion
  75.8 2.4 %collective-permute-start.4 = (bf16[1024,512]{1,0:T(8,128)(2,1)}, bf16[1024,512]{1,0:T(8,128)(2,1)}, u32[]{:S(2)}, u32[]{:S(2)}) collective-permute-start(bf16[1024,512]{1,0:T(8,128)(2,1)} %pad_maximum_fusion), channel_id=1, source_target_pairs={{0,1},{1,0},{2,3},{3,2},{4,5},{5,4},{6,7},{7,6},{8,9},{9,8},{10,11... | collective-permute-start | bytes 3145736 | tf_op jit(solution)/shard_map/ppermute | solution.py:20
  78.4 9.4 %all-to-all-start.2 = ((bf16[32,64,128]{2,1,0:T(8,128)(2,1)}), bf16[32,64,128]{2,1,0:T(8,128)(2,1)S(1)}, u32[]{:S(2)}, u32[]{:S(2)}) async-start(bf16[32,64,128]{2,1,0:T(8,128)(2,1)} %bitcast.15), calls=%async_computation.2 | async-start | bytes 1048576 | tf_op jit(solution)/shard_map/all_to_all | solution.py:24
  87.8 2.0 %fusion.18 = f32[1024,256]{1,0:T(8,128)S(1)} fusion(bf16[1024,1024]{1,0:T(8,128)(2,1)S(1)} %copy-done, bf16[1024,256]{1,0:T(8,128)(2,1)} %bitcast.111, f32[1024]{0:T(1024)S(1)} %fusion.20), kind=kOutput, calls=%fused_computation.42 | convolution fusion | flops 537657344 | bytes 3674112 | tf_op jit(solution)/shard_map/dot_general | solution.py:33
  89.8 2.2 %collective-permute-start.5 = (bf16[512,256]{0,1:T(8,128)(2,1)S(1)}, bf16[512,256]{0,1:T(8,128)(2,1)S(1)}, u32[]{:S(2)}, u32[]{:S(2)}) collective-permute-start(bf16[512,256]{0,1:T(8,128)(2,1)S(1)} %constant_dynamic-update-slice_fusion), channel_id=1, source_target_pairs={{0,1},{1,0},{2,3},{3,2},{4,5},{5,4},{6,7},{7,6},{8,9},{9,8},{10,11... | collective-permute-start | bytes 786440 | tf_op jit(solution)/shard_map/ppermute | solution.py:20
  92.1 0.8 fusion.17
  93.5 1.5 fusion.4
  95.0 9.6 %all-to-all-done.2 = bf16[32,64,128]{2,1,0:T(8,128)(2,1)S(1)} async-done(((bf16[32,64,128]{2,1,0:T(8,128)(2,1)}), bf16[32,64,128]{2,1,0:T(8,128)(2,1)S(1)}, u32[]{:S(2)}, u32[]{:S(2)}) %all-to-all-start.2) | async-done | bytes 524320 | tf_op jit(solution)/shard_map/all_to_all | solution.py:24
  104.8 22.3 %all_to_all.30 = bf16[8,72,512]{2,1,0:T(8,128)(2,1)S(1)} all-to-all(bf16[8,72,512]{2,1,0:T(8,128)(2,1)S(1)} %broadcast_in_dim.23), channel_id=1, replica_groups=mesh['z'=8,'x'=4,'y'=8,'c'=2] {'y'}, dimensions={0} | all-to-all | bytes 1179648 | tf_op jit(solution)/shard_map/all_to_all | solution.py:24
  127.9 0.9 copy.175
  128.7 6.2 %collective-permute-start.6 = (bf16[512,512]{1,0:T(8,128)(2,1)S(1)}, bf16[512,512]{1,0:T(8,128)(2,1)S(1)}, u32[]{:S(2)}, u32[]{:S(2)}) collective-permute-start(bf16[512,512]{1,0:T(8,128)(2,1)S(1)} %bitcast.86), channel_id=1, source_target_pairs={{0,1},{1,0},{2,3},{3,2},{4,5},{5,4},{6,7},{7,6},{8,9},{9,8},{10,11... | collective-permute-start | bytes 1572872 | tf_op jit(solution)/shard_map/ppermute | solution.py:20
  135.0 5.6 %all-to-all-start.4 = ((bf16[64,8,512]{2,1,0:T(8,128)(2,1)}), bf16[64,8,512]{2,1,0:T(8,128)(2,1)S(1)}, u32[]{:S(2)}, u32[]{:S(2)}) async-start(bf16[64,8,512]{2,1,0:T(8,128)(2,1)} %bitcast.30), calls=%async_computation.4 | async-start | bytes 1048576 | tf_op jit(solution)/shard_map/all_to_all | solution.py:24
  140.7 4.8 %collective-permute-start.10 = (bf16[256,512]{1,0:T(8,128)(2,1)S(1)}, bf16[256,512]{1,0:T(8,128)(2,1)S(1)}, u32[]{:S(2)}, u32[]{:S(2)}) collective-permute-start(bf16[256,512]{1,0:T(8,128)(2,1)S(1)} %get-tuple-element.80), channel_id=1, source_target_pairs={{0,32},{16,48},{32,0},{48,16},{1,33},{17,49},{33,1},{49,17},{2,34}... | collective-permute-start | bytes 786440 | tf_op jit(solution)/shard_map/ppermute | solution.py:20
  145.4 2.8 %collective-permute-start.12 = (bf16[256,512]{1,0:T(8,128)(2,1)S(1)}, bf16[256,512]{1,0:T(8,128)(2,1)S(1)}, u32[]{:S(2)}, u32[]{:S(2)}) collective-permute-start(bf16[256,512]{1,0:T(8,128)(2,1)S(1)} %get-tuple-element.81), channel_id=1, source_target_pairs={{0,48},{16,0},{32,16},{48,32},{1,49},{17,1},{33,17},{49,33},{2,50}... | collective-permute-start | bytes 786440 | tf_op jit(solution)/shard_map/ppermute | solution.py:20
  148.2 2.5 %collective-permute-start.11 = (bf16[256,512]{1,0:T(8,128)(2,1)S(1)}, bf16[256,512]{1,0:T(8,128)(2,1)S(1)}, u32[]{:S(2)}, u32[]{:S(2)}) collective-permute-start(bf16[256,512]{1,0:T(8,128)(2,1)S(1)} %get-tuple-element.82), channel_id=1, source_target_pairs={{0,16},{16,32},{32,48},{48,0},{1,17},{17,33},{33,49},{49,1},{2,18}... | collective-permute-start | bytes 786440 | tf_op jit(solution)/shard_map/ppermute | solution.py:20
  151.5 2.2 %collective-permute-start.7 = (bf16[256,128]{1,0:T(8,128)(2,1)S(1)}, bf16[256,128]{1,0:T(8,128)(2,1)S(1)}, u32[]{:S(2)}, u32[]{:S(2)}) collective-permute-start(bf16[256,128]{1,0:T(8,128)(2,1)S(1)} %get-tuple-element.83), channel_id=1, source_target_pairs={{0,16},{16,32},{32,48},{48,0},{1,17},{17,33},{33,49},{49,1},{2,18}... | collective-permute-start | bytes 196616 | tf_op jit(solution)/shard_map/ppermute | solution.py:20
  153.7 4.9 %collective-permute-start.9 = (bf16[256,128]{1,0:T(8,128)(2,1)S(1)}, bf16[256,128]{1,0:T(8,128)(2,1)S(1)}, u32[]{:S(2)}, u32[]{:S(2)}) collective-permute-start(bf16[256,128]{1,0:T(8,128)(2,1)S(1)} %get-tuple-element.84), channel_id=1, source_target_pairs={{0,32},{16,48},{32,0},{48,16},{1,33},{17,49},{33,1},{49,17},{2,34}... | collective-permute-start | bytes 196616 | tf_op jit(solution)/shard_map/ppermute | solution.py:20
  158.6 2.1 %collective-permute-start.8 = (bf16[256,128]{1,0:T(8,128)(2,1)S(1)}, bf16[256,128]{1,0:T(8,128)(2,1)S(1)}, u32[]{:S(2)}, u32[]{:S(2)}) collective-permute-start(bf16[256,128]{1,0:T(8,128)(2,1)S(1)} %get-tuple-element.85), channel_id=1, source_target_pairs={{0,48},{16,0},{32,16},{48,32},{1,49},{17,1},{33,17},{49,33},{2,50}... | collective-permute-start | bytes 196616 | tf_op jit(solution)/shard_map/ppermute | solution.py:20
  160.7 1.5 collective-permute-done.12
  162.2 0.9 collective-permute-done.11
  163.1 0.8 add_convert_fusion
  163.9 3.4 %all-to-all-start.5 = ((bf16[8,32,512]{2,1,0:T(8,128)(2,1)}), bf16[8,32,512]{2,1,0:T(8,128)(2,1)S(1)}, u32[]{:S(2)}, u32[]{:S(2)}) async-start(bf16[8,32,512]{2,1,0:T(8,128)(2,1)} %bitcast.35), calls=%async_computation.5 | async-start | bytes 524288 | tf_op jit(solution)/shard_map/all_to_all | solution.py:24
  168.6 0.9 reshape.178
  169.5 10.1 %all-to-all-done.5 = bf16[8,32,512]{2,1,0:T(8,128)(2,1)S(1)} async-done(((bf16[8,32,512]{2,1,0:T(8,128)(2,1)}), bf16[8,32,512]{2,1,0:T(8,128)(2,1)S(1)}, u32[]{:S(2)}, u32[]{:S(2)}) %all-to-all-start.5) | async-done | bytes 262176 | tf_op jit(solution)/shard_map/all_to_all | solution.py:24
  (110 shorter events, 11.6 us)
Async XLA Ops:
  3.3 30.1 %collective-permute-start = (bf16[640,256]{1,0:T(8,128)(2,1)}, bf16[640,256]{1,0:T(8,128)(2,1)S(1)}, u32[]{:S(2)}, u32[]{:S(2)}) collective-permute-start(bf16[640,256]{1,0:T(8,128)(2,1)} %pad_maximum_fusion.1), channel_id=1, source_target_pairs={{0,16},{16,32},{32,48},{48,0},{1,17},{17,33},{33,49},{49,1},{2,18}... | collective-permute-start | bytes 983048 | tf_op jit(solution)/shard_map/ppermute | solution.py:20
  10.3 40.6 %all-to-all-start = ((bf16[8,136,512]{2,1,0:T(8,128)(2,1)}), bf16[8,136,512]{2,1,0:T(8,128)(2,1)S(1)}, u32[]{:S(2)}, u32[]{:S(2)}) async-start(bf16[8,136,512]{2,1,0:T(8,128)(2,1)} %broadcast_in_dim.19), calls=%async_computation | async-start | bytes 2228224 | tf_op jit(solution)/shard_map/all_to_all | solution.py:24
  20.4 13.0 %collective-permute-start.1 = (bf16[640,256]{1,0:T(8,128)(2,1)}, bf16[640,256]{1,0:T(8,128)(2,1)S(1)}, u32[]{:S(2)}, u32[]{:S(2)}) collective-permute-start(bf16[640,256]{1,0:T(8,128)(2,1)} %pad_maximum_fusion.1), channel_id=1, source_target_pairs={{0,48},{16,0},{32,16},{48,32},{1,49},{17,1},{33,17},{49,33},{2,50}... | collective-permute-start | bytes 983048 | tf_op jit(solution)/shard_map/ppermute | solution.py:20
  23.7 11.4 %collective-permute-start.2 = (bf16[640,256]{1,0:T(8,128)(2,1)}, bf16[640,256]{1,0:T(8,128)(2,1)S(1)}, u32[]{:S(2)}, u32[]{:S(2)}) collective-permute-start(bf16[640,256]{1,0:T(8,128)(2,1)} %pad_maximum_fusion.1), channel_id=1, source_target_pairs={{0,32},{16,48},{32,0},{48,16},{1,33},{17,49},{33,1},{49,17},{2,34}... | collective-permute-start | bytes 983048 | tf_op jit(solution)/shard_map/ppermute | solution.py:20
  31.4 9.7 %copy-start.11 = (bf16[128,256]{1,0:T(8,128)(2,1)S(1)}, bf16[128,256]{1,0:T(8,128)(2,1)}, u32[]{:S(2)}) copy-start(bf16[128,256]{1,0:T(8,128)(2,1)} %param.8) | copy-start | bytes 196612
  35.1 15.9 %copy-start.10 = (bf16[640,256]{1,0:T(8,128)(2,1)}, bf16[640,256]{1,0:T(8,128)(2,1)S(1)}, u32[]{:S(2)}) copy-start(bf16[640,256]{1,0:T(8,128)(2,1)S(1)} %collective-permute-done.2) | copy-start | bytes 983044
  35.1 16.7 %collective-permute-start.3 = (bf16[2048,256]{1,0:T(8,128)(2,1)S(1)}, bf16[2048,256]{1,0:T(8,128)(2,1)}, u32[]{:S(2)}, u32[]{:S(2)}) collective-permute-start(bf16[2048,256]{1,0:T(8,128)(2,1)S(1)} %slice_dynamic-update-slice_fusion), channel_id=1, source_target_pairs={{0,1},{1,0},{2,3},{3,2},{4,5},{5,4},{6,7},{7,6},{8,9},{9,8},{10,11... | collective-permute-start | bytes 3145736 | tf_op jit(solution)/shard_map/ppermute | solution.py:20
  51.1 20.7 %copy-start.9 = (bf16[8,128,256]{2,1,0:T(8,128)(2,1)}, bf16[8,128,256]{2,1,0:T(8,128)(2,1)S(1)}, u32[]{:S(2)}) copy-start(bf16[8,128,256]{2,1,0:T(8,128)(2,1)S(1)} %get-tuple-element.78) | copy-start | bytes 1572868
  57.4 13.1 %all-to-all-start.1 = ((f32[8,16,128]{2,1,0:T(8,128)}), f32[8,16,128]{2,1,0:T(8,128)S(1)}, u32[]{:S(2)}, u32[]{:S(2)}) async-start(f32[8,16,128]{2,1,0:T(8,128)} %broadcast_in_dim.20), calls=%async_computation.1 | async-start | bytes 131072 | tf_op jit(solution)/shard_map/all_to_all | solution.py:24
  63.2 4.2 %copy-start.3 = (bf16[1024,1024]{1,0:T(8,128)(2,1)}, bf16[1024,1024]{1,0:T(8,128)(2,1)S(1)}, u32[]{:S(2)}) copy-start(bf16[1024,1024]{1,0:T(8,128)(2,1)S(1)} %multiply_convert_fusion.1) | copy-start | bytes 6291460
  63.2 2.3 %copy-start.1 = (bf16[1024,1024]{1,0:T(8,128)(2,1)S(1)}, bf16[1024,1024]{1,0:T(8,128)(2,1)}, u32[]{:S(2)}) copy-start(bf16[1024,1024]{1,0:T(8,128)(2,1)} %get-tuple-element.21) | copy-start | bytes 6291460
  67.4 1.3 copy-start.5
  70.6 1.8 copy-start.2
  72.3 1.6 copy-start.6
  74.8 3.5 %slice-start = ((bf16[640,256]{1,0:T(8,128)(2,1)}), bf16[128,256]{1,0:T(8,128)(2,1)S(1)}, s32[]{:S(2)}) async-start(bf16[640,256]{1,0:T(8,128)(2,1)} %copy-done.10), calls=%async_computation.6 | async-start | bytes 131072 | tf_op jit(solution)/shard_map/slice | solution.py:73
  74.8 13.1 %copy-start = (bf16[1024,1024]{1,0:T(8,128)(2,1)S(1)}, bf16[1024,1024]{1,0:T(8,128)(2,1)}, u32[]{:S(2)}) copy-start(bf16[1024,1024]{1,0:T(8,128)(2,1)} %get-tuple-element.20) | copy-start | bytes 6291460
  75.8 17.7 %collective-permute-start.4 = (bf16[1024,512]{1,0:T(8,128)(2,1)}, bf16[1024,512]{1,0:T(8,128)(2,1)}, u32[]{:S(2)}, u32[]{:S(2)}) collective-permute-start(bf16[1024,512]{1,0:T(8,128)(2,1)} %pad_maximum_fusion), channel_id=1, source_target_pairs={{0,1},{1,0},{2,3},{3,2},{4,5},{5,4},{6,7},{7,6},{8,9},{9,8},{10,11... | collective-permute-start | bytes 3145736 | tf_op jit(solution)/shard_map/ppermute | solution.py:20
  78.4 26.1 %all-to-all-start.2 = ((bf16[32,64,128]{2,1,0:T(8,128)(2,1)}), bf16[32,64,128]{2,1,0:T(8,128)(2,1)S(1)}, u32[]{:S(2)}, u32[]{:S(2)}) async-start(bf16[32,64,128]{2,1,0:T(8,128)(2,1)} %bitcast.15), calls=%async_computation.2 | async-start | bytes 1048576 | tf_op jit(solution)/shard_map/all_to_all | solution.py:24
  87.8 4.2 %copy-start.4 = (bf16[1024,1024]{1,0:T(8,128)(2,1)S(1)}, bf16[1024,1024]{1,0:T(8,128)(2,1)}, u32[]{:S(2)}) copy-start(bf16[1024,1024]{1,0:T(8,128)(2,1)} %copy-done.3) | copy-start | bytes 6291460
  89.8 3.4 %collective-permute-start.5 = (bf16[512,256]{0,1:T(8,128)(2,1)S(1)}, bf16[512,256]{0,1:T(8,128)(2,1)S(1)}, u32[]{:S(2)}, u32[]{:S(2)}) collective-permute-start(bf16[512,256]{0,1:T(8,128)(2,1)S(1)} %constant_dynamic-update-slice_fusion), channel_id=1, source_target_pairs={{0,1},{1,0},{2,3},{3,2},{4,5},{5,4},{6,7},{7,6},{8,9},{9,8},{10,11... | collective-permute-start | bytes 786440 | tf_op jit(solution)/shard_map/ppermute | solution.py:20
  127.3 7.6 %copy-start.12 = (f32[256]{0:T(256)S(1)}, f32[256]{0:T(256)}, u32[]{:S(2)}) copy-start(f32[256]{0:T(256)} %param.9) | copy-start | bytes 3076
  127.8 22.9 %copy-start.8 = (bf16[256,8,1,1,64]{0,4,3,2,1:T(8,128)(2,1)S(1)}, bf16[256,8,1,1,64]{0,4,3,2,1:T(8,128)(2,1)}, u32[]{:S(2)}) copy-start(bf16[256,8,1,1,64]{0,4,3,2,1:T(8,128)(2,1)} %get-tuple-element.77) | copy-start | bytes 786436
  128.7 22.4 %copy-start.7 = (bf16[256,8,1,1,64]{0,4,3,2,1:T(8,128)(2,1)S(1)}, bf16[256,8,1,1,64]{0,4,3,2,1:T(8,128)(2,1)}, u32[]{:S(2)}) copy-start(bf16[256,8,1,1,64]{0,4,3,2,1:T(8,128)(2,1)} %get-tuple-element.76) | copy-start | bytes 786436
  128.7 22.4 %collective-permute-start.6 = (bf16[512,512]{1,0:T(8,128)(2,1)S(1)}, bf16[512,512]{1,0:T(8,128)(2,1)S(1)}, u32[]{:S(2)}, u32[]{:S(2)}) collective-permute-start(bf16[512,512]{1,0:T(8,128)(2,1)S(1)} %bitcast.86), channel_id=1, source_target_pairs={{0,1},{1,0},{2,3},{3,2},{4,5},{5,4},{6,7},{7,6},{8,9},{9,8},{10,11... | collective-permute-start | bytes 1572872 | tf_op jit(solution)/shard_map/ppermute | solution.py:20
  135.0 28.9 %all-to-all-start.4 = ((bf16[64,8,512]{2,1,0:T(8,128)(2,1)}), bf16[64,8,512]{2,1,0:T(8,128)(2,1)S(1)}, u32[]{:S(2)}, u32[]{:S(2)}) async-start(bf16[64,8,512]{2,1,0:T(8,128)(2,1)} %bitcast.30), calls=%async_computation.4 | async-start | bytes 1048576 | tf_op jit(solution)/shard_map/all_to_all | solution.py:24
  140.7 17.9 %collective-permute-start.10 = (bf16[256,512]{1,0:T(8,128)(2,1)S(1)}, bf16[256,512]{1,0:T(8,128)(2,1)S(1)}, u32[]{:S(2)}, u32[]{:S(2)}) collective-permute-start(bf16[256,512]{1,0:T(8,128)(2,1)S(1)} %get-tuple-element.80), channel_id=1, source_target_pairs={{0,32},{16,48},{32,0},{48,16},{1,33},{17,49},{33,1},{49,17},{2,34}... | collective-permute-start | bytes 786440 | tf_op jit(solution)/shard_map/ppermute | solution.py:20
  145.4 16.8 %collective-permute-start.12 = (bf16[256,512]{1,0:T(8,128)(2,1)S(1)}, bf16[256,512]{1,0:T(8,128)(2,1)S(1)}, u32[]{:S(2)}, u32[]{:S(2)}) collective-permute-start(bf16[256,512]{1,0:T(8,128)(2,1)S(1)} %get-tuple-element.81), channel_id=1, source_target_pairs={{0,48},{16,0},{32,16},{48,32},{1,49},{17,1},{33,17},{49,33},{2,50}... | collective-permute-start | bytes 786440 | tf_op jit(solution)/shard_map/ppermute | solution.py:20
  148.2 14.9 %collective-permute-start.11 = (bf16[256,512]{1,0:T(8,128)(2,1)S(1)}, bf16[256,512]{1,0:T(8,128)(2,1)S(1)}, u32[]{:S(2)}, u32[]{:S(2)}) collective-permute-start(bf16[256,512]{1,0:T(8,128)(2,1)S(1)} %get-tuple-element.82), channel_id=1, source_target_pairs={{0,16},{16,32},{32,48},{48,0},{1,17},{17,33},{33,49},{49,1},{2,18}... | collective-permute-start | bytes 786440 | tf_op jit(solution)/shard_map/ppermute | solution.py:20
  151.5 15.9 %collective-permute-start.7 = (bf16[256,128]{1,0:T(8,128)(2,1)S(1)}, bf16[256,128]{1,0:T(8,128)(2,1)S(1)}, u32[]{:S(2)}, u32[]{:S(2)}) collective-permute-start(bf16[256,128]{1,0:T(8,128)(2,1)S(1)} %get-tuple-element.83), channel_id=1, source_target_pairs={{0,16},{16,32},{32,48},{48,0},{1,17},{17,33},{33,49},{49,1},{2,18}... | collective-permute-start | bytes 196616 | tf_op jit(solution)/shard_map/ppermute | solution.py:20
  153.7 13.7 %collective-permute-start.9 = (bf16[256,128]{1,0:T(8,128)(2,1)S(1)}, bf16[256,128]{1,0:T(8,128)(2,1)S(1)}, u32[]{:S(2)}, u32[]{:S(2)}) collective-permute-start(bf16[256,128]{1,0:T(8,128)(2,1)S(1)} %get-tuple-element.84), channel_id=1, source_target_pairs={{0,32},{16,48},{32,0},{48,16},{1,33},{17,49},{33,1},{49,17},{2,34}... | collective-permute-start | bytes 196616 | tf_op jit(solution)/shard_map/ppermute | solution.py:20
  158.6 8.8 %collective-permute-start.8 = (bf16[256,128]{1,0:T(8,128)(2,1)S(1)}, bf16[256,128]{1,0:T(8,128)(2,1)S(1)}, u32[]{:S(2)}, u32[]{:S(2)}) collective-permute-start(bf16[256,128]{1,0:T(8,128)(2,1)S(1)} %get-tuple-element.85), channel_id=1, source_target_pairs={{0,48},{16,0},{32,16},{48,32},{1,49},{17,1},{33,17},{49,33},{2,50}... | collective-permute-start | bytes 196616 | tf_op jit(solution)/shard_map/ppermute | solution.py:20
  163.9 15.6 %all-to-all-start.5 = ((bf16[8,32,512]{2,1,0:T(8,128)(2,1)}), bf16[8,32,512]{2,1,0:T(8,128)(2,1)S(1)}, u32[]{:S(2)}, u32[]{:S(2)}) async-start(bf16[8,32,512]{2,1,0:T(8,128)(2,1)} %bitcast.35), calls=%async_computation.5 | async-start | bytes 524288 | tf_op jit(solution)/shard_map/all_to_all | solution.py:24
